TPU v7x, 32 devices: a whole 2x2x4 slice. The times are simulated.
32 devices in a mesh: kv: 16 (over z, y, x), tp: 2 (over core).
Axes of the slice: x: 2, y: 2, z: 4, core: 2. Of those that a mesh axis runs over, the one named last changes fastest.
Arguments:
- tokens: bfloat16 [6144, 2048], P('kv', 'tp'), may hold values from -12 to 12
- query_weight: bfloat16 [2048, 2048], P(None, 'tp'), may hold values from -0.5 to 0.5
- key_weight: bfloat16 [2048, 1024], P(None, 'tp'), may hold values from -0.5 to 0.5
- value_weight: bfloat16 [2048, 1024], P(None, 'tp'), may hold values from -0.125 to 0.125
- out_weight: bfloat16 [2048, 2048], P(None, 'tp'), may hold values from -0.125 to 0.125
- chosen: int32 [96, 16], P('kv'), may hold values from 0 to 95, as said below
Outputs:
- mixed: bfloat16 [6144, 2048], P('kv', 'tp')
Inputs may be any that keep to these rules, and one draw needn't show every extreme that they name: `chosen`: row b names no block after b; its first entry is b and its next 3 entries are blocks of the same device as block b; entries may repeat. Over the rows of one device, the entries after the first 4 name at most 2 blocks, counting repeats, of any one other device, and some device names exactly 2 of another.
All inputs are finite; a program needn't handle non-finite values.
Results may differ from a plain program's by a relative error of at most 0.0072.
Values may be sent and summed in bfloat16 or wider, within the bound.
No kernel may reach another device: no remote copies, remote signals or barrier semaphores. Data moves between devices by JAX's collectives and lax.ppermute only.
A program may use at most 128 MiB of HBM per device.

v0:
```python
import functools
import math

import jax
import jax.numpy as jnp
from jax import lax
from jax.experimental import pallas as pl
from jax.experimental.pallas import tpu as pltpu
from jax.sharding import PartitionSpec as P


HD = 128
BLK = 64
TOPB = 16
CAP = 2
NEG = float("-inf")
VMEM = pl.BlockSpec(memory_space=pltpu.VMEM)
SMEM = pl.BlockSpec(memory_space=pltpu.SMEM)
ANY = pl.BlockSpec(memory_space=pl.ANY)


def plane_size(devices):
    return max(d for d in range(1, math.isqrt(devices) + 1) if devices % d == 0)


def partner(place, shift, plane):
    if plane & (plane - 1) == 0:
        return place ^ shift
    return (shift - place) % plane


def far(part):
    return pltpu.with_memory_space_constraint(part, pltpu.HBM)


def send(part, pairs):
    return lax.ppermute(part, "kv", pairs)


def spread(part):
    count = lax.axis_size("tp")
    pieces = [part]
    for shift in range(1, count):
        pairs = [(i, (i - shift) % count) for i in range(count)]
        pieces.append(lax.ppermute(part, "tp", pairs))
    return pieces


def split_dot(pieces, weight):
    count = lax.axis_size("tp")
    me = lax.axis_index("tp")
    width = weight.shape[0] // count
    total = None
    for shift, piece in enumerate(pieces):
        rows = lax.dynamic_slice_in_dim(weight, (me + shift) % count * width, width, 0)
        term = jnp.dot(piece, rows, preferred_element_type=jnp.float32)
        total = term if total is None else total + term
    return total.astype(jnp.bfloat16)


def project_kernel(count, first, cols, *refs):
    pieces = refs[:count]
    key_ref, value_ref, out_ref, held, sems = refs[count:]
    width = pieces[0].shape[1]
    me = lax.axis_index("tp")
    copies = []
    for s in range(count):
        at = pl.multiple_of(lax.rem(me + s, count) * width, width)
        for i, ref in enumerate((key_ref, value_ref)):
            copy = pltpu.make_async_copy(
                ref.at[pl.ds(at, width), pl.ds(first, cols)],
                held.at[s, i],
                sems.at[s, i],
            )
            copy.start()
            copies.append(copy)
    totals = [None, None]
    for s in range(count):
        for i in range(2):
            copies[2 * s + i].wait()
            term = jnp.dot(
                pieces[s][...], held[s, i], preferred_element_type=jnp.float32
            )
            totals[i] = term if s == 0 else totals[i] + term
    for i in range(2):
        out_ref[:, i * cols : (i + 1) * cols] = totals[i].astype(jnp.bfloat16)


def project(pieces, key_weight, value_weight, first, cols):
    rows, width = pieces[0].shape
    count = len(pieces)
    return pl.pallas_call(
        functools.partial(project_kernel, count, first, cols),
        out_shape=jax.ShapeDtypeStruct((rows, 2 * cols), jnp.bfloat16),
        in_specs=[VMEM] * count + [ANY, ANY],
        out_specs=VMEM,
        scratch_shapes=[
            pltpu.VMEM((count, 2, width, cols), jnp.bfloat16),
            pltpu.SemaphoreType.DMA((count, 2)),
        ],
        cost_estimate=pl.CostEstimate(
            flops=4 * rows * width * count * cols,
            bytes_accessed=2 * count * width * (rows + 2 * cols) + 4 * rows * cols,
            transcendentals=0,
        ),
        compiler_params=pltpu.CompilerParams(vmem_limit_bytes=16 << 20),
        name="project",
    )(*pieces, far(key_weight), far(value_weight))


def index_kernel(lines, plane, own_blocks, chosen_ref, slots_ref, *refs):
    asks = refs[: plane - 1]
    count, seen, rows = refs[plane - 1 :]
    size = own_blocks * TOPB
    device = lax.axis_index("kv")
    line = lax.div(device, plane)
    place = device - line * plane
    side_base = own_blocks * lines

    def clear(ref):
        def one(i, carry):
            ref[i] = 0
            return carry

        lax.fori_loop(0, ref.shape[0], one, 0)

    clear(count)
    clear(seen)
    clear(rows)

    def entry(e, carry):
        at = lax.div(e, TOPB)
        block = chosen_ref[at, e - at * TOPB]
        holder = lax.div(block, own_blocks)
        within = block - holder * own_blocks
        remote = holder != device
        spot = count[holder]
        count[holder] = spot + jnp.where(remote, 1, 0)
        spot = jnp.minimum(spot, CAP - 1)
        from_line = lax.div(holder, plane)
        from_place = holder - from_line * plane
        if plane & (plane - 1) == 0:
            shift = jnp.bitwise_xor(from_place, place)
        else:
            shift = lax.rem(from_place + place, plane)
        gap = jnp.maximum(line - from_line, 0)
        rows[(shift * lines + from_line) * CAP + spot] = within
        straight = gap * own_blocks + within
        across = side_base + (gap * (plane - 1) + shift - 1) * CAP + spot
        slots_ref[e] = jnp.where(from_place == place, straight, across)
        row = at + 1
        slots_ref[size + e] = jnp.where(seen[block] == row, 1, 0)
        seen[block] = row
        return carry

    lax.fori_loop(0, size, entry, 0)
    for shift, ask in enumerate(asks, 1):
        for i in range(lines * CAP):
            ask[i] = rows[shift * lines * CAP + i]


def index(chosen, lines, plane, own_blocks):
    size = own_blocks * TOPB
    ask = jax.ShapeDtypeStruct((lines * CAP,), jnp.int32)
    outs = pl.pallas_call(
        functools.partial(index_kernel, lines, plane, own_blocks),
        out_shape=[jax.ShapeDtypeStruct((2 * size,), jnp.int32)] + [ask] * (plane - 1),
        in_specs=[SMEM],
        out_specs=[SMEM] * plane,
        scratch_shapes=[
            pltpu.SMEM((lines * plane,), jnp.int32),
            pltpu.SMEM((lines * plane * own_blocks,), jnp.int32),
            pltpu.SMEM((plane * lines * CAP,), jnp.int32),
        ],
        compiler_params=pltpu.CompilerParams(vmem_limit_bytes=1 << 20),
        name="index",
    )(chosen)
    return outs[0], outs[1:]


def pick_kernel(targets, count, step, *refs):
    tables = refs[:targets]
    parts = refs[targets : targets + count]
    outs = refs[targets + count : -1]
    sems = refs[-1]
    line = lax.div(lax.axis_index("kv"), targets + 1)
    row = jnp.maximum(line - step, 0)
    copies = []
    for r, out in enumerate(outs):
        for i in range(CAP):
            block = tables[r][row * CAP + i]
            for t, part in enumerate(parts):
                cols = part.shape[2]
                copies.append(
                    pltpu.make_async_copy(
                        part.at[block],
                        out.at[i, :, pl.ds(t * cols, cols)],
                        sems.at[r, i, t],
                    )
                )
    for copy in copies:
        copy.start()
    for copy in copies:
        copy.wait()


def pick(tables, parts, step):
    targets = len(tables)
    _, rows, cols = parts[0].shape
    shape = jax.ShapeDtypeStruct((CAP, rows, cols * len(parts)), jnp.bfloat16)
    return pl.pallas_call(
        functools.partial(pick_kernel, targets, len(parts), step),
        out_shape=[shape] * targets,
        in_specs=[SMEM] * targets + [ANY] * len(parts),
        out_specs=[VMEM] * targets,
        scratch_shapes=[pltpu.SemaphoreType.DMA((targets, CAP, len(parts)))],
        compiler_params=pltpu.CompilerParams(vmem_limit_bytes=8 << 20),
        name="pick",
    )(*tables, *parts)


def attend_kernel(sizes, offsets, heads, group, first, *refs):
    n = len(sizes)
    slots_ref, q_ref = refs[:2]
    pool_refs = refs[2 : 2 + n]
    out_ref, pool, sems = refs[2 + n :]
    width = heads * HD
    copies = []
    at = 0
    for i, size in enumerate(sizes):
        part = pool_refs[i].at[:, :, pl.ds(offsets[i], 2 * width)]
        copies.append(
            pltpu.make_async_copy(part, pool.at[pl.ds(at, size)], sems.at[i])
        )
        at += size
    for copy in copies:
        copy.start()
    for copy in copies:
        copy.wait()
    blocks = q_ref.shape[0] // BLK
    low = lax.broadcasted_iota(jnp.int32, (1, 2 * BLK), 1) < BLK
    tri_row = lax.broadcasted_iota(jnp.int32, (BLK, HD), 0)
    tri_col = lax.broadcasted_iota(jnp.int32, (BLK, HD), 1)
    tri = jnp.where((tri_col < BLK) & (tri_col > tri_row), NEG, 0.0)
    tri = jnp.concatenate([tri] * group, axis=0)

    def block(b, carry):
        at_row = pl.multiple_of(b * BLK, BLK)
        picks = [slots_ref[b * TOPB + s] for s in range(TOPB)]
        hidden = [
            jnp.where(slots_ref[(blocks + b) * TOPB + s] > 0, NEG, 0.0)
            for s in range(TOPB)
        ]
        bias = jnp.concatenate(
            [jnp.where(low, hidden[s], hidden[s + 1]) for s in range(0, TOPB, 2)], axis=1
        )
        for j in range(heads):
            cols = [(j * group + g) * HD for g in range(group)]
            q = jnp.concatenate(
                [q_ref[pl.ds(at_row, BLK), first + c : first + c + HD] for c in cols],
                axis=0,
            )
            k = jnp.concatenate(
                [pool[p, :, j * HD : (j + 1) * HD] for p in picks], axis=0
            )
            v = jnp.concatenate(
                [pool[p, :, width + j * HD : width + (j + 1) * HD] for p in picks], axis=0
            )
            s = lax.dot_general(
                q, k, (((1,), (1,)), ((), ())), preferred_element_type=jnp.float32
            )
            s = s + bias
            s = jnp.concatenate([s[:, :HD] + tri, s[:, HD:]], axis=1)
            peak = jnp.max(s, axis=1, keepdims=True)
            w = jnp.exp((s - peak) * HD ** (-0.5))
            total = jnp.sum(w, axis=1, keepdims=True)
            o = jnp.dot(w.astype(jnp.bfloat16), v, preferred_element_type=jnp.float32)
            o = (o / total).astype(jnp.bfloat16)
            for g, c in enumerate(cols):
                out_ref[pl.ds(at_row, BLK), c : c + HD] = o[g * BLK : (g + 1) * BLK]
        return carry

    lax.fori_loop(0, blocks, block, 0)


def attend(queries, slots, pools, offsets, heads, group, first):
    rows = queries.shape[0]
    cols = heads * group * HD
    sizes = tuple(p.shape[0] for p in pools)
    return pl.pallas_call(
        functools.partial(attend_kernel, sizes, offsets, heads, group, first),
        out_shape=jax.ShapeDtypeStruct((rows, cols), jnp.bfloat16),
        in_specs=[SMEM, VMEM] + [ANY] * len(pools),
        out_specs=VMEM,
        scratch_shapes=[
            pltpu.VMEM((sum(sizes), BLK, 2 * heads * HD), jnp.bfloat16),
            pltpu.SemaphoreType.DMA((len(sizes),)),
        ],
        cost_estimate=pl.CostEstimate(
            flops=4 * rows * TOPB * BLK * cols,
            bytes_accessed=4 * rows * cols + 4 * sum(sizes) * BLK * heads * HD,
            transcendentals=rows * TOPB * BLK * cols // HD,
        ),
        compiler_params=pltpu.CompilerParams(vmem_limit_bytes=24 << 20),
        name="attend",
    )(slots, queries, *pools)


def local(tokens, query_weight, key_weight, value_weight, out_weight, chosen):
    tok_rows = tokens.shape[0]
    key_heads = key_weight.shape[1] // HD
    group = query_weight.shape[1] // HD // key_heads
    own_blocks = tok_rows // BLK
    devices = lax.axis_size("kv")
    plane = plane_size(devices)
    lines = devices // plane
    tp = lax.axis_size("tp")
    streams = 2 if key_heads % 2 == 0 else 1
    heads = key_heads // streams
    cols = heads * HD

    section = spread(tokens)
    up = [(d, (d + plane) % devices) for d in range(devices)]
    swaps = [
        [
            (l * plane + c, l * plane + partner(c, shift, plane))
            for l in range(lines)
            for c in range(plane)
        ]
        for shift in range(1, plane)
    ]

    own = []
    line_parts = [[] for _ in range(streams)]
    for t in range(streams):
        if t > 0:
            section, _ = lax.optimization_barrier((section, own[-1]))
        pair = project(section, key_weight, value_weight, t * cols, cols)
        own.append(pair.reshape(own_blocks, BLK, 2 * cols))
        if lines > 1:
            line_parts[t].append(send(own[t], up))
    chosen, _ = lax.optimization_barrier((chosen, own[-1]))
    slots, asks = index(chosen, lines, plane, own_blocks)
    asked = []
    for shift in range(1, plane):
        asked.append(send(asks[shift - 1], swaps[shift - 1]))

    side_parts = [[] for _ in range(streams)]
    offsets = [[] for _ in range(streams)]
    queries = None
    held = own
    for step in range(lines):
        last = step == lines - 1
        split = step >= lines - 2
        batches = [[t] for t in range(streams)] if split else [list(range(streams))]
        if last and queries is not None:
            held[0], queries = lax.optimization_barrier((held[0], queries))
        for batch in batches:
            if plane == 1:
                continue
            picked = pick(asked, [held[t] for t in batch], step)
            for shift in range(1, plane):
                got = send(picked[shift - 1], swaps[shift - 1])
                for i, t in enumerate(batch):
                    side_parts[t].append(got)
                    offsets[t].append(i * 2 * cols)
        if not last:
            held = [line_parts[t][-1] for t in range(streams)]
        if step + 1 < lines - 1:
            for t in range(streams):
                line_parts[t].append(send(held[t], up))
        if queries is None:
            queries = split_dot(section, query_weight)
    total = None
    me = lax.axis_index("tp")
    share = group * cols
    for t in range(streams):
        pools = [own[t]] + line_parts[t] + side_parts[t]
        shifts = (0,) * (1 + len(line_parts[t])) + tuple(offsets[t])
        done = attend(queries, slots, pools, shifts, heads, group, t * share)
        for shift, piece in enumerate(spread(done)):
            at = ((me + shift) % tp * streams + t) * share
            rows = lax.dynamic_slice_in_dim(out_weight, at, share, 0)
            term = jnp.dot(piece, rows, preferred_element_type=jnp.float32)
            total = term if total is None else total + term
    return total.astype(jnp.bfloat16)


def solution(mesh):
    return jax.shard_map(
        local,
        mesh=mesh,
        in_specs=(
            P("kv", "tp"),
            P(None, "tp"),
            P(None, "tp"),
            P(None, "tp"),
            P(None, "tp"),
            P("kv", None),
        ),
        out_specs=P("kv", "tp"),
        check_vma=False,
    )
```

profile of v0, /device:TPU:23, one launch (start us, length us, event | category | flops | bytes accessed | tf_op | source)
XLA Modules:
  0.0 117.8 jit_solution(5510506689393348865)
XLA Ops:
  0.0 0.7 collective-permute-start
  0.7 2.1 %collective-permute-done.refs_1_ = bf16[384,1024]{1,0:T(8,128)(2,1)S(1)} collective-permute-done((bf16[384,1024]{1,0:T(8,128)(2,1)}, bf16[384,1024]{1,0:T(8,128)(2,1)S(1)}, u32[]{:S(2)}, u32[]{:S(2)}) %collective-permute-start) | collective-permute-done | bytes 786464 | tf_op jit(solution)/shard_map/ppermute | solution.py:45
  2.8 1.1 copy-done
  3.9 3.3 %project.2 = bf16[384,512]{1,0:T(8,128)(2,1)S(1)} custom-call(bf16[384,1024]{1,0:T(8,128)(2,1)S(1)} %copy-done, bf16[384,1024]{1,0:T(8,128)(2,1)S(1)} %collective-permute-done.refs_1_, bf16[2048,512]{1,0:T(8,128)(2,1)} %refs_2_.3, bf16[2048,512]{1,0:T(8,128)(2,1)} %refs_3_.3), custom_call_target="tpu_custom_call" | custom-call | flops 805306368 | bytes 4063232 | tf_op jit(solution)/shard_map/project/pallas_call | solution.py:92
  7.3 1.3 %collective-permute-start.1 = (bf16[6,64,512]{2,1,0:T(8,128)(2,1)S(1)}, bf16[6,64,512]{2,1,0:T(8,128)(2,1)S(1)}, u32[]{:S(2)}, u32[]{:S(2)}) collective-permute-start(bf16[6,64,512]{2,1,0:T(8,128)(2,1)S(1)} %bitcast.11), channel_id=1, source_target_pairs={{0,8},{2,10},{4,12},{6,14},{8,16},{10,18},{12,20},{14,22},{16,24},... | collective-permute-start | bytes 1179656 | tf_op jit(solution)/shard_map/ppermute | solution.py:37
  8.6 3.3 %project.3 = bf16[384,512]{1,0:T(8,128)(2,1)S(1)} custom-call(bf16[384,1024]{1,0:T(8,128)(2,1)S(1)} %copy-done, bf16[384,1024]{1,0:T(8,128)(2,1)S(1)} %collective-permute-done.refs_1_, bf16[2048,512]{1,0:T(8,128)(2,1)} %refs_2_.3, bf16[2048,512]{1,0:T(8,128)(2,1)} %refs_3_.3), custom_call_target="tpu_custom_call" | custom-call | flops 805306368 | bytes 4063232 | tf_op jit(solution)/shard_map/project/pallas_call | solution.py:92
  12.0 5.6 %collective-permute-done.1.refs_3_ = bf16[6,64,512]{2,1,0:T(8,128)(2,1)S(1)} collective-permute-done((bf16[6,64,512]{2,1,0:T(8,128)(2,1)S(1)}, bf16[6,64,512]{2,1,0:T(8,128)(2,1)S(1)}, u32[]{:S(2)}, u32[]{:S(2)}) %collective-permute-start.1) | collective-permute-done | bytes 393248 | tf_op jit(solution)/shard_map/ppermute | solution.py:37
  17.6 1.3 %collective-permute-start.2 = (bf16[6,64,512]{2,1,0:T(8,128)(2,1)S(1)}, bf16[6,64,512]{2,1,0:T(8,128)(2,1)S(1)}, u32[]{:S(2)}, u32[]{:S(2)}) collective-permute-start(bf16[6,64,512]{2,1,0:T(8,128)(2,1)S(1)} %collective-permute-done.1.refs_3_), channel_id=1, source_target_pairs={{0,8},{2,10},{4,12},{6,14},{8,16},{10,18},{12,20},{14,22},{16,24},... | collective-permute-start | bytes 1179656 | tf_op jit(solution)/shard_map/ppermute | solution.py:37
  18.9 7.1 %collective-permute-done.10.refs_4_.refs_3_ = bf16[6,64,512]{2,1,0:T(8,128)(2,1)S(1)} collective-permute-done((bf16[6,64,512]{2,1,0:T(8,128)(2,1)S(1)}, bf16[6,64,512]{2,1,0:T(8,128)(2,1)S(1)}, u32[]{:S(2)}, u32[]{:S(2)}) %collective-permute-start.10) | collective-permute-done | bytes 393248 | tf_op jit(solution)/shard_map/ppermute | solution.py:37
  26.1 1.3 %collective-permute-start.21 = (bf16[6,64,512]{2,1,0:T(8,128)(2,1)S(1)}, bf16[6,64,512]{2,1,0:T(8,128)(2,1)S(1)}, u32[]{:S(2)}, u32[]{:S(2)}) collective-permute-start(bf16[6,64,512]{2,1,0:T(8,128)(2,1)S(1)} %collective-permute-done.10.refs_4_.refs_3_), channel_id=1, source_target_pairs={{0,8},{2,10},{4,12},{6,14},{8,16},{10,18},{12,20},{14,22},{16,24},... | collective-permute-start | bytes 1179656 | tf_op jit(solution)/shard_map/ppermute | solution.py:37
  27.4 5.0 %index.1 = (s32[192]{0:T(256)S(1)}, s32[8]{0:T(128)S(1)}, s32[8]{0:T(128)S(1)}, s32[8]{0:T(128)S(1)}) custom-call(s32[6,16]{1,0:T(8,128)S(1)} %copy-done.20), custom_call_target="tpu_custom_call" | custom-call | tf_op jit(solution)/shard_map/index/pallas_call | solution.py:165
  32.9 2.2 %collective-permute-start.6 = (s32[8]{0:T(128)S(1)}, s32[8]{0:T(128)S(1)}, u32[]{:S(2)}, u32[]{:S(2)}) collective-permute-start(s32[8]{0:T(128)S(1)} %get-tuple-element.39), channel_id=1, source_target_pairs={{0,6},{2,4},{4,2},{6,0},{8,14},{10,12},{12,10},{14,8},{16,22},{18,... | collective-permute-start | bytes 104 | tf_op jit(solution)/shard_map/ppermute | solution.py:37
  35.4 0.8 collective-permute-done.6.refs_2_
  36.2 1.5 %pick.6 = (bf16[2,64,1024]{2,1,0:T(8,128)(2,1)}, bf16[2,64,1024]{2,1,0:T(8,128)(2,1)S(1)}, bf16[2,64,1024]{2,1,0:T(8,128)(2,1)S(1)}) custom-call(s32[8]{0:T(128)S(1)} %collective-permute-done.4.refs_0_, s32[8]{0:T(128)S(1)} %collective-permute-done.5.refs_1_, s32[8]{0:T(128)S(1)} %collective-permute-done.6.refs_2_, bf16[6,64,512]{2,1,0:T(8,128)(2,1)S(1)} %bitcast.12, ...), custom_call_target="tpu_custom_call" | custom-call | tf_op jit(solution)/shard_map/pick/pallas_call | solution.py:211
  37.7 1.3 %collective-permute-start.7 = (bf16[2,64,1024]{2,1,0:T(8,128)(2,1)}, bf16[2,64,1024]{2,1,0:T(8,128)(2,1)}, u32[]{:S(2)}, u32[]{:S(2)}) collective-permute-start(bf16[2,64,1024]{2,1,0:T(8,128)(2,1)} %get-tuple-element.40), channel_id=1, source_target_pairs={{0,2},{2,0},{4,6},{6,4},{8,10},{10,8},{12,14},{14,12},{16,18},{18,... | collective-permute-start | bytes 786440 | tf_op jit(solution)/shard_map/ppermute | solution.py:37
  39.0 1.9 %collective-permute-start.3 = (bf16[6,64,512]{2,1,0:T(8,128)(2,1)S(1)}, bf16[6,64,512]{2,1,0:T(8,128)(2,1)S(1)}, u32[]{:S(2)}, u32[]{:S(2)}) collective-permute-start(bf16[6,64,512]{2,1,0:T(8,128)(2,1)S(1)} %collective-permute-done.2.refs_3_.refs_4_), channel_id=1, source_target_pairs={{0,8},{2,10},{4,12},{6,14},{8,16},{10,18},{12,20},{14,22},{16,24},... | collective-permute-start | bytes 1179656 | tf_op jit(solution)/shard_map/ppermute | solution.py:37
  41.0 1.2 %collective-permute-start.8 = (bf16[2,64,1024]{2,1,0:T(8,128)(2,1)}, bf16[2,64,1024]{2,1,0:T(8,128)(2,1)S(1)}, u32[]{:S(2)}, u32[]{:S(2)}) collective-permute-start(bf16[2,64,1024]{2,1,0:T(8,128)(2,1)} %copy-done.22), channel_id=1, source_target_pairs={{0,4},{2,6},{4,0},{6,2},{8,12},{10,14},{12,8},{14,10},{16,20},{18,... | collective-permute-start | bytes 786440 | tf_op jit(solution)/shard_map/ppermute | solution.py:37
  42.8 0.8 pick.7
  43.7 1.1 collective-permute-start.11
  44.8 1.1 collective-permute-start.12
  45.8 3.0 %fusion = f32[384,1024]{1,0:T(8,128)S(1)} fusion(bf16[384,1024]{1,0:T(8,128)(2,1)S(1)} %collective-permute-done.refs_1_, bf16[2048,1024]{1,0:T(8,128)(2,1)} %param.7, s32[]{:T(128)S(6)} %select_n.36), kind=kOutput, calls=%fused_computation | convolution fusion | flops 805306368 | bytes 4456452 | tf_op jit(solution)/shard_map/dot_general | solution.py:56
  48.8 1.1 pick.8
  50.0 1.8 %pick.10 = (bf16[2,64,512]{2,1,0:T(8,128)(2,1)S(1)}, bf16[2,64,512]{2,1,0:T(8,128)(2,1)S(1)}, bf16[2,64,512]{2,1,0:T(8,128)(2,1)}) custom-call(s32[8]{0:T(128)S(1)} %collective-permute-done.4.refs_0_, s32[8]{0:T(128)S(1)} %collective-permute-done.5.refs_1_, s32[8]{0:T(128)S(1)} %collective-permute-done.6.refs_2_, ...), custom_call_target="tpu_custom_call" | custom-call | tf_op jit(solution)/shard_map/pick/pallas_call | solution.py:211
  52.2 1.1 collective-permute-start.23
  53.2 2.9 %collective-permute-done.11.refs_9_ = bf16[2,64,1024]{2,1,0:T(8,128)(2,1)S(1)} collective-permute-done((bf16[2,64,1024]{2,1,0:T(8,128)(2,1)S(1)}, bf16[2,64,1024]{2,1,0:T(8,128)(2,1)S(1)}, u32[]{:S(2)}, u32[]{:S(2)}) %collective-permute-start.11) | collective-permute-done | bytes 262176 | tf_op jit(solution)/shard_map/ppermute | solution.py:37
  56.2 1.8 %collective-permute-done.12.refs_10_ = bf16[2,64,1024]{2,1,0:T(8,128)(2,1)S(1)} collective-permute-done((bf16[2,64,1024]{2,1,0:T(8,128)(2,1)S(1)}, bf16[2,64,1024]{2,1,0:T(8,128)(2,1)S(1)}, u32[]{:S(2)}, u32[]{:S(2)}) %collective-permute-start.12) | collective-permute-done | bytes 262176 | tf_op jit(solution)/shard_map/ppermute | solution.py:37
  58.1 2.7 %collective-permute-start.15 = (bf16[2,64,512]{2,1,0:T(8,128)(2,1)S(1)}, bf16[2,64,512]{2,1,0:T(8,128)(2,1)S(1)}, u32[]{:S(2)}, u32[]{:S(2)}) collective-permute-start(bf16[2,64,512]{2,1,0:T(8,128)(2,1)S(1)} %get-tuple-element.47), channel_id=1, source_target_pairs={{0,4},{2,6},{4,0},{6,2},{8,12},{10,14},{12,8},{14,10},{16,20},{18,... | collective-permute-start | bytes 393224 | tf_op jit(solution)/shard_map/ppermute | solution.py:37
  60.8 1.7 %collective-permute-start.22 = (bf16[6,64,512]{2,1,0:T(8,128)(2,1)S(1)}, bf16[6,64,512]{2,1,0:T(8,128)(2,1)S(1)}, u32[]{:S(2)}, u32[]{:S(2)}) collective-permute-start(bf16[6,64,512]{2,1,0:T(8,128)(2,1)S(1)} %collective-permute-done.21.refs_3_.refs_4_), channel_id=1, source_target_pairs={{0,8},{2,10},{4,12},{6,14},{8,16},{10,18},{12,20},{14,22},{16,24},... | collective-permute-start | bytes 1179656 | tf_op jit(solution)/shard_map/ppermute | solution.py:37
  62.4 1.0 add_convert_fusion.1.refs_1_
  63.4 1.1 pick.9
  64.6 0.8 collective-permute-start.16
  65.9 1.6 %collective-permute-start.18 = (bf16[2,64,512]{2,1,0:T(8,128)(2,1)S(1)}, bf16[2,64,512]{2,1,0:T(8,128)(2,1)S(1)}, u32[]{:S(2)}, u32[]{:S(2)}) collective-permute-start(bf16[2,64,512]{2,1,0:T(8,128)(2,1)S(1)} %get-tuple-element.51), channel_id=1, source_target_pairs={{0,4},{2,6},{4,0},{6,2},{8,12},{10,14},{12,8},{14,10},{16,20},{18,... | collective-permute-start | bytes 393224 | tf_op jit(solution)/shard_map/ppermute | solution.py:37
  67.6 2.4 %collective-permute-start.19 = (bf16[2,64,512]{2,1,0:T(8,128)(2,1)S(1)}, bf16[2,64,512]{2,1,0:T(8,128)(2,1)S(1)}, u32[]{:S(2)}, u32[]{:S(2)}) collective-permute-start(bf16[2,64,512]{2,1,0:T(8,128)(2,1)S(1)} %get-tuple-element.52), channel_id=1, source_target_pairs={{0,6},{2,4},{4,2},{6,0},{8,14},{10,12},{12,10},{14,8},{16,22},{18,... | collective-permute-start | bytes 393224 | tf_op jit(solution)/shard_map/ppermute | solution.py:37
  70.0 1.9 %pick.11 = (bf16[2,64,512]{2,1,0:T(8,128)(2,1)}, bf16[2,64,512]{2,1,0:T(8,128)(2,1)}, bf16[2,64,512]{2,1,0:T(8,128)(2,1)}) custom-call(s32[8]{0:T(128)S(1)} %collective-permute-done.4.refs_0_, s32[8]{0:T(128)S(1)} %collective-permute-done.5.refs_1_, s32[8]{0:T(128)S(1)} %collective-permute-done.6.refs_2_, ...), custom_call_target="tpu_custom_call" | custom-call | tf_op jit(solution)/shard_map/pick/pallas_call | solution.py:211
  71.9 2.1 %collective-permute-start.25 = (bf16[2,64,512]{2,1,0:T(8,128)(2,1)}, bf16[2,64,512]{2,1,0:T(8,128)(2,1)}, u32[]{:S(2)}, u32[]{:S(2)}) collective-permute-start(bf16[2,64,512]{2,1,0:T(8,128)(2,1)} %get-tuple-element.55), channel_id=1, source_target_pairs={{0,6},{2,4},{4,2},{6,0},{8,14},{10,12},{12,10},{14,8},{16,22},{18,... | collective-permute-start | bytes 393224 | tf_op jit(solution)/shard_map/ppermute | solution.py:37
  75.3 1.4 %collective-permute-start.28 = (bf16[2,64,512]{2,1,0:T(8,128)(2,1)}, bf16[2,64,512]{2,1,0:T(8,128)(2,1)}, u32[]{:S(2)}, u32[]{:S(2)}) collective-permute-start(bf16[2,64,512]{2,1,0:T(8,128)(2,1)} %get-tuple-element.58), channel_id=1, source_target_pairs={{0,6},{2,4},{4,2},{6,0},{8,14},{10,12},{12,10},{14,8},{16,22},{18,... | collective-permute-start | bytes 393224 | tf_op jit(solution)/shard_map/ppermute | solution.py:37
  76.7 8.0 %attend.2 = bf16[384,512]{1,0:T(8,128)(2,1)S(1)} custom-call(s32[192]{0:T(256)S(1)} %get-tuple-element.35.refs_0_, bf16[384,1024]{1,0:T(8,128)(2,1)S(1)} %add_convert_fusion.1.refs_1_, bf16[6,64,512]{2,1,0:T(8,128)(2,1)S(1)} %bitcast.13, bf16[6,64,512]{2,1,0:T(8,128)(2,1)S(1)} %copy-done.5, bf16[6,64,512]{2,1,0:T(8,128)(2,1)S(1)} %collective-permute-done.2.refs_3_.refs_4_, ...), custom_call_target="tpu_custom_call" | custom-call | flops 805306368 | bytes 3932160 | tf_op jit(solution)/shard_map/attend/pallas_call | solution.py:290
  85.4 12.5 %collective-permute-start.20 = (bf16[384,512]{1,0:T(8,128)(2,1)S(1)}, bf16[384,512]{1,0:T(8,128)(2,1)S(1)}, u32[]{:S(2)}, u32[]{:S(2)}) collective-permute-start(bf16[384,512]{1,0:T(8,128)(2,1)S(1)} %attend.2), channel_id=1, source_target_pairs={{0,1},{1,0},{2,3},{3,2},{4,5},{5,4},{6,7},{7,6},{8,9},{9,8},{10,11... | collective-permute-start | bytes 1179656 | tf_op jit(solution)/shard_map/ppermute | solution.py:45
  97.9 1.0 copy-done.3
  98.9 0.9 copy-done.7
  99.8 0.9 copy-done.9
  100.8 0.9 copy-done.11
  101.7 0.9 copy-done.13
  102.7 0.9 copy-done.15
  103.6 0.9 copy-done.17
  104.5 0.9 copy-done.19
  105.4 8.4 %attend.3 = bf16[384,512]{1,0:T(8,128)(2,1)S(1)} custom-call(s32[192]{0:T(256)S(1)} %get-tuple-element.35.refs_0_, bf16[384,1024]{1,0:T(8,128)(2,1)S(1)} %add_convert_fusion.1.refs_1_, bf16[6,64,512]{2,1,0:T(8,128)(2,1)S(1)} %bitcast.10, bf16[6,64,512]{2,1,0:T(8,128)(2,1)S(1)} %copy-done.3, bf16[6,64,512]{2,1,0:T(8,128)(2,1)S(1)} %collective-permute-done.21.refs_3_.refs_4_, ...), custom_call_target="tpu_custom_call" | custom-call | flops 805306368 | bytes 3932160 | tf_op jit(solution)/shard_map/attend/pallas_call | solution.py:290
  116.2 1.6 %add_convert_fusion = bf16[384,1024]{1,0:T(8,128)(2,1)} fusion(f32[384,1024]{1,0:T(8,128)S(1)} %fusion.6, f32[384,1024]{1,0:T(8,128)S(1)} %fusion.14, f32[384,1024]{1,0:T(8,128)S(1)} %fusion.12, bf16[384,512]{1,0:T(8,128)(2,1)S(1)} %attend.3, bf16[2048,1024]{1,0:T(8,128)(2,1)S(1)} %copy-done.23, s32[]{:T(128)S(6)} %select_n.37), kind=kOutput, calls=%fused_computation.4 | convolution fusion | flops 404226048 | bytes 6946820 | tf_op jit(solution)/shard_map/dot_general | solution.py:384
  (79 shorter events, 6.9 us)
Async XLA Ops:
  0.0 2.8 %collective-permute-start = (bf16[384,1024]{1,0:T(8,128)(2,1)}, bf16[384,1024]{1,0:T(8,128)(2,1)S(1)}, u32[]{:S(2)}, u32[]{:S(2)}) collective-permute-start(bf16[384,1024]{1,0:T(8,128)(2,1)} %refs_0_.2), channel_id=1, source_target_pairs={{0,1},{1,0},{2,3},{3,2},{4,5},{5,4},{6,7},{7,6},{8,9},{9,8},{10,11... | collective-permute-start | bytes 2359304 | tf_op jit(solution)/shard_map/ppermute | solution.py:45
  2.8 1.1 copy-start
  7.3 20.1 %copy-start.20 = (s32[6,16]{1,0:T(8,128)S(1)}, s32[6,16]{1,0:T(8,128)}, u32[]{:S(2)}) copy-start(s32[6,16]{1,0:T(8,128)} %chosen_ref) | copy-start | bytes 1156
  7.3 10.4 %collective-permute-start.1 = (bf16[6,64,512]{2,1,0:T(8,128)(2,1)S(1)}, bf16[6,64,512]{2,1,0:T(8,128)(2,1)S(1)}, u32[]{:S(2)}, u32[]{:S(2)}) collective-permute-start(bf16[6,64,512]{2,1,0:T(8,128)(2,1)S(1)} %bitcast.11), channel_id=1, source_target_pairs={{0,8},{2,10},{4,12},{6,14},{8,16},{10,18},{12,20},{14,22},{16,24},... | collective-permute-start | bytes 1179656 | tf_op jit(solution)/shard_map/ppermute | solution.py:37
  11.9 14.1 %collective-permute-start.10 = (bf16[6,64,512]{2,1,0:T(8,128)(2,1)S(1)}, bf16[6,64,512]{2,1,0:T(8,128)(2,1)S(1)}, u32[]{:S(2)}, u32[]{:S(2)}) collective-permute-start(bf16[6,64,512]{2,1,0:T(8,128)(2,1)S(1)} %bitcast.8), channel_id=1, source_target_pairs={{0,8},{2,10},{4,12},{6,14},{8,16},{10,18},{12,20},{14,22},{16,24},... | collective-permute-start | bytes 1179656 | tf_op jit(solution)/shard_map/ppermute | solution.py:37
  17.6 31.2 %copy-start.4 = (bf16[6,64,512]{2,1,0:T(8,128)(2,1)}, bf16[6,64,512]{2,1,0:T(8,128)(2,1)S(1)}, u32[]{:S(2)}) copy-start(bf16[6,64,512]{2,1,0:T(8,128)(2,1)S(1)} %collective-permute-done.1.refs_3_) | copy-start | bytes 1179652
  17.6 21.4 %collective-permute-start.2 = (bf16[6,64,512]{2,1,0:T(8,128)(2,1)S(1)}, bf16[6,64,512]{2,1,0:T(8,128)(2,1)S(1)}, u32[]{:S(2)}, u32[]{:S(2)}) collective-permute-start(bf16[6,64,512]{2,1,0:T(8,128)(2,1)S(1)} %collective-permute-done.1.refs_3_), channel_id=1, source_target_pairs={{0,8},{2,10},{4,12},{6,14},{8,16},{10,18},{12,20},{14,22},{16,24},... | collective-permute-start | bytes 1179656 | tf_op jit(solution)/shard_map/ppermute | solution.py:37
  26.1 22.8 %copy-start.2 = (bf16[6,64,512]{2,1,0:T(8,128)(2,1)}, bf16[6,64,512]{2,1,0:T(8,128)(2,1)S(1)}, u32[]{:S(2)}) copy-start(bf16[6,64,512]{2,1,0:T(8,128)(2,1)S(1)} %collective-permute-done.10.refs_4_.refs_3_) | copy-start | bytes 1179652
  26.1 18.7 %collective-permute-start.21 = (bf16[6,64,512]{2,1,0:T(8,128)(2,1)S(1)}, bf16[6,64,512]{2,1,0:T(8,128)(2,1)S(1)}, u32[]{:S(2)}, u32[]{:S(2)}) collective-permute-start(bf16[6,64,512]{2,1,0:T(8,128)(2,1)S(1)} %collective-permute-done.10.refs_4_.refs_3_), channel_id=1, source_target_pairs={{0,8},{2,10},{4,12},{6,14},{8,16},{10,18},{12,20},{14,22},{16,24},... | collective-permute-start | bytes 1179656 | tf_op jit(solution)/shard_map/ppermute | solution.py:37
  32.3 2.8 %collective-permute-start.4 = (s32[8]{0:T(128)S(1)}, s32[8]{0:T(128)S(1)}, u32[]{:S(2)}, u32[]{:S(2)}) collective-permute-start(s32[8]{0:T(128)S(1)} %get-tuple-element.37), channel_id=1, source_target_pairs={{0,2},{2,0},{4,6},{6,4},{8,10},{10,8},{12,14},{14,12},{16,18},{18,... | collective-permute-start | bytes 104 | tf_op jit(solution)/shard_map/ppermute | solution.py:37
  32.7 2.7 %collective-permute-start.5 = (s32[8]{0:T(128)S(1)}, s32[8]{0:T(128)S(1)}, u32[]{:S(2)}, u32[]{:S(2)}) collective-permute-start(s32[8]{0:T(128)S(1)} %get-tuple-element.38), channel_id=1, source_target_pairs={{0,4},{2,6},{4,0},{6,2},{8,12},{10,14},{12,8},{14,10},{16,20},{18,... | collective-permute-start | bytes 104 | tf_op jit(solution)/shard_map/ppermute | solution.py:37
  32.9 3.3 %collective-permute-start.6 = (s32[8]{0:T(128)S(1)}, s32[8]{0:T(128)S(1)}, u32[]{:S(2)}, u32[]{:S(2)}) collective-permute-start(s32[8]{0:T(128)S(1)} %get-tuple-element.39), channel_id=1, source_target_pairs={{0,6},{2,4},{4,2},{6,0},{8,14},{10,12},{12,10},{14,8},{16,22},{18,... | collective-permute-start | bytes 104 | tf_op jit(solution)/shard_map/ppermute | solution.py:37
  37.7 1.3 %copy-start.21 = (bf16[2,64,1024]{2,1,0:T(8,128)(2,1)}, bf16[2,64,1024]{2,1,0:T(8,128)(2,1)S(1)}, u32[]{:S(2)}) copy-start(bf16[2,64,1024]{2,1,0:T(8,128)(2,1)S(1)} %get-tuple-element.42) | copy-start | bytes 786436
  37.7 1.3 %copy-start.22 = (bf16[2,64,1024]{2,1,0:T(8,128)(2,1)}, bf16[2,64,1024]{2,1,0:T(8,128)(2,1)S(1)}, u32[]{:S(2)}) copy-start(bf16[2,64,1024]{2,1,0:T(8,128)(2,1)S(1)} %get-tuple-element.41) | copy-start | bytes 786436
  37.7 5.9 %collective-permute-start.7 = (bf16[2,64,1024]{2,1,0:T(8,128)(2,1)}, bf16[2,64,1024]{2,1,0:T(8,128)(2,1)}, u32[]{:S(2)}, u32[]{:S(2)}) collective-permute-start(bf16[2,64,1024]{2,1,0:T(8,128)(2,1)} %get-tuple-element.40), channel_id=1, source_target_pairs={{0,2},{2,0},{4,6},{6,4},{8,10},{10,8},{12,14},{14,12},{16,18},{18,... | collective-permute-start | bytes 786440 | tf_op jit(solution)/shard_map/ppermute | solution.py:37
  39.0 21.7 %collective-permute-start.3 = (bf16[6,64,512]{2,1,0:T(8,128)(2,1)S(1)}, bf16[6,64,512]{2,1,0:T(8,128)(2,1)S(1)}, u32[]{:S(2)}, u32[]{:S(2)}) collective-permute-start(bf16[6,64,512]{2,1,0:T(8,128)(2,1)S(1)} %collective-permute-done.2.refs_3_.refs_4_), channel_id=1, source_target_pairs={{0,8},{2,10},{4,12},{6,14},{8,16},{10,18},{12,20},{14,22},{16,24},... | collective-permute-start | bytes 1179656 | tf_op jit(solution)/shard_map/ppermute | solution.py:37
  41.0 10.8 %collective-permute-start.8 = (bf16[2,64,1024]{2,1,0:T(8,128)(2,1)}, bf16[2,64,1024]{2,1,0:T(8,128)(2,1)S(1)}, u32[]{:S(2)}, u32[]{:S(2)}) collective-permute-start(bf16[2,64,1024]{2,1,0:T(8,128)(2,1)} %copy-done.22), channel_id=1, source_target_pairs={{0,4},{2,6},{4,0},{6,2},{8,12},{10,14},{12,8},{14,10},{16,20},{18,... | collective-permute-start | bytes 786440 | tf_op jit(solution)/shard_map/ppermute | solution.py:37
  42.2 10.0 %collective-permute-start.9 = (bf16[2,64,1024]{2,1,0:T(8,128)(2,1)}, bf16[2,64,1024]{2,1,0:T(8,128)(2,1)S(1)}, u32[]{:S(2)}, u32[]{:S(2)}) collective-permute-start(bf16[2,64,1024]{2,1,0:T(8,128)(2,1)} %copy-done.21), channel_id=1, source_target_pairs={{0,6},{2,4},{4,2},{6,0},{8,14},{10,12},{12,10},{14,8},{16,22},{18,... | collective-permute-start | bytes 786440 | tf_op jit(solution)/shard_map/ppermute | solution.py:37
  43.7 12.4 %collective-permute-start.11 = (bf16[2,64,1024]{2,1,0:T(8,128)(2,1)S(1)}, bf16[2,64,1024]{2,1,0:T(8,128)(2,1)S(1)}, u32[]{:S(2)}, u32[]{:S(2)}) collective-permute-start(bf16[2,64,1024]{2,1,0:T(8,128)(2,1)S(1)} %get-tuple-element.43), channel_id=1, source_target_pairs={{0,2},{2,0},{4,6},{6,4},{8,10},{10,8},{12,14},{14,12},{16,18},{18,... | collective-permute-start | bytes 786440 | tf_op jit(solution)/shard_map/ppermute | solution.py:37
  44.8 17.7 %copy-start.1 = (bf16[384,1024]{1,0:T(8,128)(2,1)S(1)}, bf16[384,1024]{1,0:T(8,128)(2,1)}, u32[]{:S(2)}) copy-start(bf16[384,1024]{1,0:T(8,128)(2,1)} %refs_0_.2) | copy-start | bytes 2359300
  44.8 17.7 %copy-start.24 = (bf16[2048,1024]{1,0:T(8,128)(2,1)S(1)}, bf16[2048,1024]{1,0:T(8,128)(2,1)}, u32[]{:S(2)}) copy-start(bf16[2048,1024]{1,0:T(8,128)(2,1)} %param.7) | copy-start | bytes 12582916
  44.8 13.3 %collective-permute-start.12 = (bf16[2,64,1024]{2,1,0:T(8,128)(2,1)S(1)}, bf16[2,64,1024]{2,1,0:T(8,128)(2,1)S(1)}, u32[]{:S(2)}, u32[]{:S(2)}) collective-permute-start(bf16[2,64,1024]{2,1,0:T(8,128)(2,1)S(1)} %get-tuple-element.44), channel_id=1, source_target_pairs={{0,4},{2,6},{4,0},{6,2},{8,12},{10,14},{12,8},{14,10},{16,20},{18,... | collective-permute-start | bytes 786440 | tf_op jit(solution)/shard_map/ppermute | solution.py:37
  51.8 24.9 %copy-start.6 = (bf16[2,64,1024]{2,1,0:T(8,128)(2,1)}, bf16[2,64,1024]{2,1,0:T(8,128)(2,1)S(1)}, u32[]{:S(2)}) copy-start(bf16[2,64,1024]{2,1,0:T(8,128)(2,1)S(1)} %collective-permute-done.8.refs_7_) | copy-start | bytes 786436
  51.8 12.8 %collective-permute-start.13 = (bf16[2,64,1024]{2,1,0:T(8,128)(2,1)S(1)}, bf16[2,64,1024]{2,1,0:T(8,128)(2,1)S(1)}, u32[]{:S(2)}, u32[]{:S(2)}) collective-permute-start(bf16[2,64,1024]{2,1,0:T(8,128)(2,1)S(1)} %get-tuple-element.45), channel_id=1, source_target_pairs={{0,6},{2,4},{4,2},{6,0},{8,14},{10,12},{12,10},{14,8},{16,22},{18,... | collective-permute-start | bytes 786440 | tf_op jit(solution)/shard_map/ppermute | solution.py:37
  52.2 24.5 %copy-start.8 = (bf16[2,64,1024]{2,1,0:T(8,128)(2,1)}, bf16[2,64,1024]{2,1,0:T(8,128)(2,1)S(1)}, u32[]{:S(2)}) copy-start(bf16[2,64,1024]{2,1,0:T(8,128)(2,1)S(1)} %collective-permute-done.9.refs_8_) | copy-start | bytes 786436
  52.2 13.3 %collective-permute-start.23 = (bf16[2,64,512]{2,1,0:T(8,128)(2,1)S(1)}, bf16[2,64,512]{2,1,0:T(8,128)(2,1)S(1)}, u32[]{:S(2)}, u32[]{:S(2)}) collective-permute-start(bf16[2,64,512]{2,1,0:T(8,128)(2,1)S(1)} %get-tuple-element.53), channel_id=1, source_target_pairs={{0,2},{2,0},{4,6},{6,4},{8,10},{10,8},{12,14},{14,12},{16,18},{18,... | collective-permute-start | bytes 393224 | tf_op jit(solution)/shard_map/ppermute | solution.py:37
  56.1 20.6 %copy-start.10 = (bf16[2,64,1024]{2,1,0:T(8,128)(2,1)}, bf16[2,64,1024]{2,1,0:T(8,128)(2,1)S(1)}, u32[]{:S(2)}) copy-start(bf16[2,64,1024]{2,1,0:T(8,128)(2,1)S(1)} %collective-permute-done.11.refs_9_) | copy-start | bytes 786436
  56.1 9.8 %collective-permute-start.14 = (bf16[2,64,512]{2,1,0:T(8,128)(2,1)S(1)}, bf16[2,64,512]{2,1,0:T(8,128)(2,1)S(1)}, u32[]{:S(2)}, u32[]{:S(2)}) collective-permute-start(bf16[2,64,512]{2,1,0:T(8,128)(2,1)S(1)} %get-tuple-element.46), channel_id=1, source_target_pairs={{0,2},{2,0},{4,6},{6,4},{8,10},{10,8},{12,14},{14,12},{16,18},{18,... | collective-permute-start | bytes 393224 | tf_op jit(solution)/shard_map/ppermute | solution.py:37
  58.1 18.6 %copy-start.12 = (bf16[2,64,1024]{2,1,0:T(8,128)(2,1)}, bf16[2,64,1024]{2,1,0:T(8,128)(2,1)S(1)}, u32[]{:S(2)}) copy-start(bf16[2,64,1024]{2,1,0:T(8,128)(2,1)S(1)} %collective-permute-done.12.refs_10_) | copy-start | bytes 786436
  58.1 18.6 %copy-start.5 = (bf16[6,64,512]{2,1,0:T(8,128)(2,1)S(1)}, bf16[6,64,512]{2,1,0:T(8,128)(2,1)}, u32[]{:S(2)}) copy-start(bf16[6,64,512]{2,1,0:T(8,128)(2,1)} %copy-done.4) | copy-start | bytes 1179652
  58.1 9.5 %collective-permute-start.15 = (bf16[2,64,512]{2,1,0:T(8,128)(2,1)S(1)}, bf16[2,64,512]{2,1,0:T(8,128)(2,1)S(1)}, u32[]{:S(2)}, u32[]{:S(2)}) collective-permute-start(bf16[2,64,512]{2,1,0:T(8,128)(2,1)S(1)} %get-tuple-element.47), channel_id=1, source_target_pairs={{0,4},{2,6},{4,0},{6,2},{8,12},{10,14},{12,8},{14,10},{16,20},{18,... | collective-permute-start | bytes 393224 | tf_op jit(solution)/shard_map/ppermute | solution.py:37
  60.8 9.2 %collective-permute-start.22 = (bf16[6,64,512]{2,1,0:T(8,128)(2,1)S(1)}, bf16[6,64,512]{2,1,0:T(8,128)(2,1)S(1)}, u32[]{:S(2)}, u32[]{:S(2)}) collective-permute-start(bf16[6,64,512]{2,1,0:T(8,128)(2,1)S(1)} %collective-permute-done.21.refs_3_.refs_4_), channel_id=1, source_target_pairs={{0,8},{2,10},{4,12},{6,14},{8,16},{10,18},{12,20},{14,22},{16,24},... | collective-permute-start | bytes 1179656 | tf_op jit(solution)/shard_map/ppermute | solution.py:37
  64.6 20.1 %copy-start.14 = (bf16[2,64,1024]{2,1,0:T(8,128)(2,1)}, bf16[2,64,1024]{2,1,0:T(8,128)(2,1)S(1)}, u32[]{:S(2)}) copy-start(bf16[2,64,1024]{2,1,0:T(8,128)(2,1)S(1)} %collective-permute-done.13.refs_11_) | copy-start | bytes 786436
  64.6 7.3 %collective-permute-start.16 = (bf16[2,64,512]{2,1,0:T(8,128)(2,1)S(1)}, bf16[2,64,512]{2,1,0:T(8,128)(2,1)S(1)}, u32[]{:S(2)}, u32[]{:S(2)}) collective-permute-start(bf16[2,64,512]{2,1,0:T(8,128)(2,1)S(1)} %get-tuple-element.48), channel_id=1, source_target_pairs={{0,6},{2,4},{4,2},{6,0},{8,14},{10,12},{12,10},{14,8},{16,22},{18,... | collective-permute-start | bytes 393224 | tf_op jit(solution)/shard_map/ppermute | solution.py:37
  65.5 19.2 %copy-start.16 = (bf16[2,64,512]{2,1,0:T(8,128)(2,1)}, bf16[2,64,512]{2,1,0:T(8,128)(2,1)S(1)}, u32[]{:S(2)}) copy-start(bf16[2,64,512]{2,1,0:T(8,128)(2,1)S(1)} %collective-permute-done.23.refs_12_) | copy-start | bytes 393220
  65.5 8.6 %collective-permute-start.17 = (bf16[2,64,512]{2,1,0:T(8,128)(2,1)S(1)}, bf16[2,64,512]{2,1,0:T(8,128)(2,1)S(1)}, u32[]{:S(2)}, u32[]{:S(2)}) collective-permute-start(bf16[2,64,512]{2,1,0:T(8,128)(2,1)S(1)} %get-tuple-element.50), channel_id=1, source_target_pairs={{0,2},{2,0},{4,6},{6,4},{8,10},{10,8},{12,14},{14,12},{16,18},{18,... | collective-permute-start | bytes 393224 | tf_op jit(solution)/shard_map/ppermute | solution.py:37
  65.9 8.7 %collective-permute-start.18 = (bf16[2,64,512]{2,1,0:T(8,128)(2,1)S(1)}, bf16[2,64,512]{2,1,0:T(8,128)(2,1)S(1)}, u32[]{:S(2)}, u32[]{:S(2)}) collective-permute-start(bf16[2,64,512]{2,1,0:T(8,128)(2,1)S(1)} %get-tuple-element.51), channel_id=1, source_target_pairs={{0,4},{2,6},{4,0},{6,2},{8,12},{10,14},{12,8},{14,10},{16,20},{18,... | collective-permute-start | bytes 393224 | tf_op jit(solution)/shard_map/ppermute | solution.py:37
  67.6 7.7 %collective-permute-start.19 = (bf16[2,64,512]{2,1,0:T(8,128)(2,1)S(1)}, bf16[2,64,512]{2,1,0:T(8,128)(2,1)S(1)}, u32[]{:S(2)}, u32[]{:S(2)}) collective-permute-start(bf16[2,64,512]{2,1,0:T(8,128)(2,1)S(1)} %get-tuple-element.52), channel_id=1, source_target_pairs={{0,6},{2,4},{4,2},{6,0},{8,14},{10,12},{12,10},{14,8},{16,22},{18,... | collective-permute-start | bytes 393224 | tf_op jit(solution)/shard_map/ppermute | solution.py:37
  70.0 14.7 %collective-permute-start.24 = (bf16[2,64,512]{2,1,0:T(8,128)(2,1)S(1)}, bf16[2,64,512]{2,1,0:T(8,128)(2,1)S(1)}, u32[]{:S(2)}, u32[]{:S(2)}) collective-permute-start(bf16[2,64,512]{2,1,0:T(8,128)(2,1)S(1)} %get-tuple-element.54), channel_id=1, source_target_pairs={{0,4},{2,6},{4,0},{6,2},{8,12},{10,14},{12,8},{14,10},{16,20},{18,... | collective-permute-start | bytes 393224 | tf_op jit(solution)/shard_map/ppermute | solution.py:37
  71.9 25.9 %collective-permute-start.25 = (bf16[2,64,512]{2,1,0:T(8,128)(2,1)}, bf16[2,64,512]{2,1,0:T(8,128)(2,1)}, u32[]{:S(2)}, u32[]{:S(2)}) collective-permute-start(bf16[2,64,512]{2,1,0:T(8,128)(2,1)} %get-tuple-element.55), channel_id=1, source_target_pairs={{0,6},{2,4},{4,2},{6,0},{8,14},{10,12},{12,10},{14,8},{16,22},{18,... | collective-permute-start | bytes 393224 | tf_op jit(solution)/shard_map/ppermute | solution.py:37
  74.0 23.8 %collective-permute-start.26 = (bf16[2,64,512]{2,1,0:T(8,128)(2,1)}, bf16[2,64,512]{2,1,0:T(8,128)(2,1)}, u32[]{:S(2)}, u32[]{:S(2)}) collective-permute-start(bf16[2,64,512]{2,1,0:T(8,128)(2,1)} %get-tuple-element.56), channel_id=1, source_target_pairs={{0,2},{2,0},{4,6},{6,4},{8,10},{10,8},{12,14},{14,12},{16,18},{18,... | collective-permute-start | bytes 393224 | tf_op jit(solution)/shard_map/ppermute | solution.py:37
  74.6 23.2 %collective-permute-start.27 = (bf16[2,64,512]{2,1,0:T(8,128)(2,1)}, bf16[2,64,512]{2,1,0:T(8,128)(2,1)}, u32[]{:S(2)}, u32[]{:S(2)}) collective-permute-start(bf16[2,64,512]{2,1,0:T(8,128)(2,1)} %get-tuple-element.57), channel_id=1, source_target_pairs={{0,4},{2,6},{4,0},{6,2},{8,12},{10,14},{12,8},{14,10},{16,20},{18,... | collective-permute-start | bytes 393224 | tf_op jit(solution)/shard_map/ppermute | solution.py:37
  75.3 22.6 %collective-permute-start.28 = (bf16[2,64,512]{2,1,0:T(8,128)(2,1)}, bf16[2,64,512]{2,1,0:T(8,128)(2,1)}, u32[]{:S(2)}, u32[]{:S(2)}) collective-permute-start(bf16[2,64,512]{2,1,0:T(8,128)(2,1)} %get-tuple-element.58), channel_id=1, source_target_pairs={{0,6},{2,4},{4,2},{6,0},{8,14},{10,12},{12,10},{14,8},{16,22},{18,... | collective-permute-start | bytes 393224 | tf_op jit(solution)/shard_map/ppermute | solution.py:37
  85.4 29.2 %collective-permute-start.20 = (bf16[384,512]{1,0:T(8,128)(2,1)S(1)}, bf16[384,512]{1,0:T(8,128)(2,1)S(1)}, u32[]{:S(2)}, u32[]{:S(2)}) collective-permute-start(bf16[384,512]{1,0:T(8,128)(2,1)S(1)} %attend.2), channel_id=1, source_target_pairs={{0,1},{1,0},{2,3},{3,2},{4,5},{5,4},{6,7},{7,6},{8,9},{9,8},{10,11... | collective-permute-start | bytes 1179656 | tf_op jit(solution)/shard_map/ppermute | solution.py:45
  97.9 1.0 copy-start.3
  98.9 0.9 copy-start.7
  105.4 8.5 %copy-start.23 = (bf16[2048,1024]{1,0:T(8,128)(2,1)S(1)}, bf16[2048,1024]{1,0:T(8,128)(2,1)}, u32[]{:S(2)}) copy-start(bf16[2048,1024]{1,0:T(8,128)(2,1)} %param.10) | copy-start | bytes 12582916
  113.8 1.8 %collective-permute-start.29 = (bf16[384,512]{1,0:T(8,128)(2,1)S(1)}, bf16[384,512]{1,0:T(8,128)(2,1)S(1)}, u32[]{:S(2)}, u32[]{:S(2)}) collective-permute-start(bf16[384,512]{1,0:T(8,128)(2,1)S(1)} %attend.3), channel_id=1, source_target_pairs={{0,1},{1,0},{2,3},{3,2},{4,5},{5,4},{6,7},{7,6},{8,9},{9,8},{10,11... | collective-permute-start | bytes 1179656 | tf_op jit(solution)/shard_map/ppermute | solution.py:45
  (7 other events, 6.3 us)
where the time goes:
time: 118 us
  starting transfers between devices  42.9 us (36%)
  Pallas kernels  36.3 us (31%)
  waiting for transfers between devices  21.4 us (18%)
  local copies, waits for them, and re-layouts  9.39 us (8%)
  matrix products  7.38 us (6%)
    ppermute x27, starting transfers between devices, send(): return lax.ppermute(part, 'kv', pairs)  29.7 us
    ppermute x27, waiting for transfers between devices, send(): return lax.ppermute(part, 'kv', pairs)  18.8 us
    pallas_call x2, Pallas kernels, attend(): pl.pallas_call(functools.partial(attend_kernel, sizes, offsets, heads, gr...  16.4 us
    ppermute x3, starting transfers between devices, spread(): pieces.append(lax.ppermute(part, 'tp', pairs))  13.2 us
    unnamed x50, local copies, waits for them, and re-layouts  9.39 us
    pallas_call x6, Pallas kernels, pick(): pl.pallas_call(functools.partial(pick_kernel, targets, len(parts), step),...  8.33 us
    pallas_call x2, Pallas kernels, project(): pl.pallas_call(functools.partial(project_kernel, count, first, cols), out...  6.63 us
    pallas_call x1, Pallas kernels, index(): pl.pallas_call(functools.partial(index_kernel, lines, plane, own_blocks),...  4.97 us
  transfers between devices with their start and end apart: 30, of which 10 were waited for; matrix products, arithmetic and copies ran while one was open for 4% of the time, Pallas kernels for 28%

commit v1 on v0

--- a/solution.py
+++ b/solution.py
@@ -29,6 +29,10 @@
     return (shift - place) % plane
 
 
+def near(part):
+    return pltpu.with_memory_space_constraint(part, pltpu.VMEM)
+
+
 def far(part):
     return pltpu.with_memory_space_constraint(part, pltpu.HBM)
 
@@ -46,27 +50,16 @@
     return pieces
 
 
-def split_dot(pieces, weight):
-    count = lax.axis_size("tp")
-    me = lax.axis_index("tp")
-    width = weight.shape[0] // count
-    total = None
-    for shift, piece in enumerate(pieces):
-        rows = lax.dynamic_slice_in_dim(weight, (me + shift) % count * width, width, 0)
-        term = jnp.dot(piece, rows, preferred_element_type=jnp.float32)
-        total = term if total is None else total + term
-    return total.astype(jnp.bfloat16)
-
-
-def project_kernel(count, first, cols, *refs):
+def project_kernel(count, kinds, first, cols, *refs):
     pieces = refs[:count]
-    key_ref, value_ref, out_ref, held, sems = refs[count:]
+    weights = refs[count : count + kinds]
+    out_ref, held, sems = refs[count + kinds :]
     width = pieces[0].shape[1]
     me = lax.axis_index("tp")
     copies = []
     for s in range(count):
         at = pl.multiple_of(lax.rem(me + s, count) * width, width)
-        for i, ref in enumerate((key_ref, value_ref)):
+        for i, ref in enumerate(weights):
             copy = pltpu.make_async_copy(
                 ref.at[pl.ds(at, width), pl.ds(first, cols)],
                 held.at[s, i],
@@ -74,38 +67,77 @@
             )
             copy.start()
             copies.append(copy)
-    totals = [None, None]
+    totals = [None] * kinds
     for s in range(count):
-        for i in range(2):
-            copies[2 * s + i].wait()
+        for i in range(kinds):
+            copies[kinds * s + i].wait()
             term = jnp.dot(
                 pieces[s][...], held[s, i], preferred_element_type=jnp.float32
             )
             totals[i] = term if s == 0 else totals[i] + term
-    for i in range(2):
+    for i in range(kinds):
         out_ref[:, i * cols : (i + 1) * cols] = totals[i].astype(jnp.bfloat16)
 
 
-def project(pieces, key_weight, value_weight, first, cols):
+def project(pieces, weights, first, cols):
     rows, width = pieces[0].shape
-    count = len(pieces)
+    count, kinds = len(pieces), len(weights)
     return pl.pallas_call(
-        functools.partial(project_kernel, count, first, cols),
-        out_shape=jax.ShapeDtypeStruct((rows, 2 * cols), jnp.bfloat16),
-        in_specs=[VMEM] * count + [ANY, ANY],
+        functools.partial(project_kernel, count, kinds, first, cols),
+        out_shape=jax.ShapeDtypeStruct((rows, kinds * cols), jnp.bfloat16),
+        in_specs=[VMEM] * count + [ANY] * kinds,
         out_specs=VMEM,
         scratch_shapes=[
-            pltpu.VMEM((count, 2, width, cols), jnp.bfloat16),
-            pltpu.SemaphoreType.DMA((count, 2)),
+            pltpu.VMEM((count, kinds, width, cols), jnp.bfloat16),
+            pltpu.SemaphoreType.DMA((count, kinds)),
         ],
         cost_estimate=pl.CostEstimate(
-            flops=4 * rows * width * count * cols,
-            bytes_accessed=2 * count * width * (rows + 2 * cols) + 4 * rows * cols,
+            flops=2 * kinds * rows * width * count * cols,
+            bytes_accessed=2 * count * width * (rows + kinds * cols),
             transcendentals=0,
         ),
         compiler_params=pltpu.CompilerParams(vmem_limit_bytes=16 << 20),
         name="project",
-    )(*pieces, far(key_weight), far(value_weight))
+    )(*pieces, *[far(weight) for weight in weights])
+
+
+def mix_kernel(streams, *refs):
+    pieces = refs[:-2]
+    weight_ref, out_ref = refs[-2:]
+    count = len(pieces) // streams
+    width = pieces[0].shape[1]
+    step = min(2 * HD, out_ref.shape[1])
+    me = lax.axis_index("tp")
+    starts = [
+        pl.multiple_of((lax.rem(me + s, count) * streams + t) * width, width)
+        for t in range(streams)
+        for s in range(count)
+    ]
+    for col in range(0, out_ref.shape[1], step):
+        total = None
+        for at, piece in zip(starts, pieces):
+            rows = weight_ref[pl.ds(at, width), col : col + step]
+            term = jnp.dot(piece[...], rows, preferred_element_type=jnp.float32)
+            total = term if total is None else total + term
+        out_ref[:, col : col + step] = total.astype(jnp.bfloat16)
+
+
+def mix(pieces, weight, streams):
+    rows, _ = pieces[0].shape
+    depth, cols = weight.shape
+    return pl.pallas_call(
+        functools.partial(mix_kernel, streams),
+        out_shape=jax.ShapeDtypeStruct((rows, cols), jnp.bfloat16),
+        in_specs=[VMEM] * (len(pieces) + 1),
+        out_specs=VMEM,
+        cost_estimate=pl.CostEstimate(
+            flops=2 * rows * depth * cols,
+            bytes_accessed=2 * (rows * depth + depth * cols + rows * cols),
+            transcendentals=0,
+        ),
+        compiler_params=pltpu.CompilerParams(vmem_limit_bytes=16 << 20),
+        name="mix",
+    )(*pieces, near(weight))
 
 
 def index_kernel(lines, plane, own_blocks, chosen_ref, slots_ref, *refs):
@@ -226,25 +258,30 @@
     out_ref, pool, sems = refs[2 + n :]
     width = heads * HD
     copies = []
-    at = 0
-    for i, size in enumerate(sizes):
-        part = pool_refs[i].at[:, :, pl.ds(offsets[i], 2 * width)]
-        copies.append(
-            pltpu.make_async_copy(part, pool.at[pl.ds(at, size)], sems.at[i])
-        )
-        at += size
+    for j in range(heads):
+        at = 0
+        for i, size in enumerate(sizes):
+            for kind in range(2):
+                col = offsets[i] + kind * width + j * HD
+                copies.append(
+                    pltpu.make_async_copy(
+                        pool_refs[i].at[:, :, pl.ds(col, HD)],
+                        pool.at[j, kind, pl.ds(at, size)],
+                        sems.at[j, kind, i],
+                    )
+                )
+            at += size
     for copy in copies:
         copy.start()
-    for copy in copies:
-        copy.wait()
     blocks = q_ref.shape[0] // BLK
     low = lax.broadcasted_iota(jnp.int32, (1, 2 * BLK), 1) < BLK
     tri_row = lax.broadcasted_iota(jnp.int32, (BLK, HD), 0)
     tri_col = lax.broadcasted_iota(jnp.int32, (BLK, HD), 1)
     tri = jnp.where((tri_col < BLK) & (tri_col > tri_row), NEG, 0.0)
     tri = jnp.concatenate([tri] * group, axis=0)
-
-    def block(b, carry):
+    ones = jnp.ones((TOPB * BLK, HD), jnp.bfloat16)
+
+    def block(j, b, carry):
         at_row = pl.multiple_of(b * BLK, BLK)
         picks = [slots_ref[b * TOPB + s] for s in range(TOPB)]
         hidden = [
@@ -254,33 +291,31 @@
         bias = jnp.concatenate(
             [jnp.where(low, hidden[s], hidden[s + 1]) for s in range(0, TOPB, 2)], axis=1
         )
-        for j in range(heads):
-            cols = [(j * group + g) * HD for g in range(group)]
-            q = jnp.concatenate(
-                [q_ref[pl.ds(at_row, BLK), first + c : first + c + HD] for c in cols],
-                axis=0,
-            )
-            k = jnp.concatenate(
-                [pool[p, :, j * HD : (j + 1) * HD] for p in picks], axis=0
-            )
-            v = jnp.concatenate(
-                [pool[p, :, width + j * HD : width + (j + 1) * HD] for p in picks], axis=0
-            )
-            s = lax.dot_general(
-                q, k, (((1,), (1,)), ((), ())), preferred_element_type=jnp.float32
-            )
-            s = s + bias
-            s = jnp.concatenate([s[:, :HD] + tri, s[:, HD:]], axis=1)
-            peak = jnp.max(s, axis=1, keepdims=True)
-            w = jnp.exp((s - peak) * HD ** (-0.5))
-            total = jnp.sum(w, axis=1, keepdims=True)
-            o = jnp.dot(w.astype(jnp.bfloat16), v, preferred_element_type=jnp.float32)
-            o = (o / total).astype(jnp.bfloat16)
-            for g, c in enumerate(cols):
-                out_ref[pl.ds(at_row, BLK), c : c + HD] = o[g * BLK : (g + 1) * BLK]
+        cols = [(j * group + g) * HD for g in range(group)]
+        q = jnp.concatenate(
+            [q_ref[pl.ds(at_row, BLK), first + c : first + c + HD] for c in cols], axis=0
+        )
+        k = jnp.concatenate([pool[j, 0, p] for p in picks], axis=0)
+        v = jnp.concatenate([pool[j, 1, p] for p in picks], axis=0)
+        s = lax.dot_general(
+            q, k, (((1,), (1,)), ((), ())), preferred_element_type=jnp.float32
+        )
+        s = s + bias
+        s = jnp.concatenate([s[:, :HD] + tri, s[:, HD:]], axis=1)
+        peak = jnp.max(s, axis=1, keepdims=True)
+        w = jnp.exp2((s - peak) * (HD ** (-0.5) * math.log2(math.e)))
+        v = jnp.concatenate([v, ones], axis=1)
+        o = jnp.dot(w.astype(jnp.bfloat16), v, preferred_element_type=jnp.float32)
+        o = (o[:, :HD] / o[:, HD:]).astype(jnp.bfloat16)
+        for g, c in enumerate(cols):
+            out_ref[pl.ds(at_row, BLK), c : c + HD] = o[g * BLK : (g + 1) * BLK]
         return carry
 
-    lax.fori_loop(0, blocks, block, 0)
+    each = 2 * n
+    for j in range(heads):
+        for copy in copies[j * each : (j + 1) * each]:
+            copy.wait()
+        lax.fori_loop(0, blocks, functools.partial(block, j), 0, unroll=blocks)
 
 
 def attend(queries, slots, pools, offsets, heads, group, first):
@@ -293,15 +328,15 @@
         in_specs=[SMEM, VMEM] + [ANY] * len(pools),
         out_specs=VMEM,
         scratch_shapes=[
-            pltpu.VMEM((sum(sizes), BLK, 2 * heads * HD), jnp.bfloat16),
-            pltpu.SemaphoreType.DMA((len(sizes),)),
+            pltpu.VMEM((heads, 2, sum(sizes), BLK, HD), jnp.bfloat16),
+            pltpu.SemaphoreType.DMA((heads, 2, len(sizes))),
         ],
         cost_estimate=pl.CostEstimate(
             flops=4 * rows * TOPB * BLK * cols,
             bytes_accessed=4 * rows * cols + 4 * sum(sizes) * BLK * heads * HD,
             transcendentals=rows * TOPB * BLK * cols // HD,
         ),
-        compiler_params=pltpu.CompilerParams(vmem_limit_bytes=24 << 20),
+        compiler_params=pltpu.CompilerParams(vmem_limit_bytes=12 << 20),
         name="attend",
     )(slots, queries, *pools)
 
@@ -314,7 +349,6 @@
     devices = lax.axis_size("kv")
     plane = plane_size(devices)
     lines = devices // plane
-    tp = lax.axis_size("tp")
     streams = 2 if key_heads % 2 == 0 else 1
     heads = key_heads // streams
     cols = heads * HD
@@ -335,7 +369,7 @@
     for t in range(streams):
         if t > 0:
             section, _ = lax.optimization_barrier((section, own[-1]))
-        pair = project(section, key_weight, value_weight, t * cols, cols)
+        pair = project(section, [key_weight, value_weight], t * cols, cols)
         own.append(pair.reshape(own_blocks, BLK, 2 * cols))
         if lines > 1:
             line_parts[t].append(send(own[t], up))
@@ -370,20 +404,16 @@
             for t in range(streams):
                 line_parts[t].append(send(held[t], up))
         if queries is None:
-            queries = split_dot(section, query_weight)
-    total = None
-    me = lax.axis_index("tp")
+            queries = project(section, [query_weight], 0, query_weight.shape[1])
     share = group * cols
+    done = []
     for t in range(streams):
         pools = [own[t]] + line_parts[t] + side_parts[t]
         shifts = (0,) * (1 + len(line_parts[t])) + tuple(offsets[t])
-        done = attend(queries, slots, pools, shifts, heads, group, t * share)
-        for shift, piece in enumerate(spread(done)):
-            at = ((me + shift) % tp * streams + t) * share
-            rows = lax.dynamic_slice_in_dim(out_weight, at, share, 0)
-            term = jnp.dot(piece, rows, preferred_element_type=jnp.float32)
-            total = term if total is None else total + term
-    return total.astype(jnp.bfloat16)
+        done.append(attend(queries, slots, pools, shifts, heads, group, t * share))
+    done = lax.optimization_barrier(done)
+    pieces = [piece for part in done for piece in spread(part)]
+    return mix(pieces, out_weight, streams)
 
 
 def solution(mesh):

time: 118 us -> 102 us (0.86)
  the two profiles are of different devices: /device:TPU:23 before, /device:TPU:15 now
where the time goes in v1:
time: 102 us; the launch traced here: 100 us
  starting transfers between devices  36.1 us (35%)
  Pallas kernels  33.6 us (33%)
  waiting for transfers between devices  29.3 us (29%)
  local copies, waits for them, and re-layouts  1.14 us (1%)
    ppermute x27, starting transfers between devices, send(): return lax.ppermute(part, 'kv', pairs)  28.4 us
    ppermute x27, waiting for transfers between devices, send(): return lax.ppermute(part, 'kv', pairs)  25.3 us
    pallas_call x3, Pallas kernels, project(): pl.pallas_call(functools.partial(project_kernel, count, kinds, first, col...  10.7 us
    pallas_call x2, Pallas kernels, attend(): pl.pallas_call(functools.partial(attend_kernel, sizes, offsets, heads, gr...  9.09 us
    ppermute x3, starting transfers between devices, spread(): pieces.append(lax.ppermute(part, 'tp', pairs))  7.76 us
    pallas_call x6, Pallas kernels, pick(): pl.pallas_call(functools.partial(pick_kernel, targets, len(parts), step),...  6.22 us
    pallas_call x1, Pallas kernels, index(): pl.pallas_call(functools.partial(index_kernel, lines, plane, own_blocks),...  4.97 us
    ppermute x3, waiting for transfers between devices, spread(): pieces.append(lax.ppermute(part, 'tp', pairs))  3.96 us
  transfers between devices with their start and end apart: 30, of which 15 were waited for; matrix products, arithmetic and copies ran while one was open for 0% of the time, Pallas kernels for 23%

profile of v1, /device:TPU:15, one launch (start us, length us, event | category | flops | bytes accessed | tf_op | source)
XLA Modules:
  0.0 100.3 jit_solution(11798906492523667878)
XLA Ops:
  0.0 0.7 collective-permute-start
  0.7 2.1 %collective-permute-done.refs_1_ = bf16[384,1024]{1,0:T(8,128)(2,1)S(1)} collective-permute-done((bf16[384,1024]{1,0:T(8,128)(2,1)}, bf16[384,1024]{1,0:T(8,128)(2,1)S(1)}, u32[]{:S(2)}, u32[]{:S(2)}) %collective-permute-start) | collective-permute-done | bytes 786464 | tf_op jit(solution)/shard_map/ppermute | solution.py:49
  2.8 1.1 %copy-done = bf16[384,1024]{1,0:T(8,128)(2,1)S(1)} copy-done((bf16[384,1024]{1,0:T(8,128)(2,1)S(1)}, bf16[384,1024]{1,0:T(8,128)(2,1)}, u32[]{:S(2)}) %copy-start) | copy-done | bytes 786456
  3.9 3.3 %project.3 = bf16[384,512]{1,0:T(8,128)(2,1)S(1)} custom-call(bf16[384,1024]{1,0:T(8,128)(2,1)S(1)} %copy-done, bf16[384,1024]{1,0:T(8,128)(2,1)S(1)} %collective-permute-done.refs_1_, bf16[2048,512]{1,0:T(8,128)(2,1)} %refs_2_.4, bf16[2048,512]{1,0:T(8,128)(2,1)} %refs_3_.3), custom_call_target="tpu_custom_call" | custom-call | flops 805306368 | bytes 3670016 | tf_op jit(solution)/shard_map/project/pallas_call | solution.py:85
  7.3 1.3 %collective-permute-start.1 = (bf16[6,64,512]{2,1,0:T(8,128)(2,1)S(1)}, bf16[6,64,512]{2,1,0:T(8,128)(2,1)S(1)}, u32[]{:S(2)}, u32[]{:S(2)}) collective-permute-start(bf16[6,64,512]{2,1,0:T(8,128)(2,1)S(1)} %bitcast.5), channel_id=1, source_target_pairs={{0,8},{2,10},{4,12},{6,14},{8,16},{10,18},{12,20},{14,22},{16,24},... | collective-permute-start | bytes 1179656 | tf_op jit(solution)/shard_map/ppermute | solution.py:41
  8.6 3.3 %project.4 = bf16[384,512]{1,0:T(8,128)(2,1)S(1)} custom-call(bf16[384,1024]{1,0:T(8,128)(2,1)S(1)} %copy-done, bf16[384,1024]{1,0:T(8,128)(2,1)S(1)} %collective-permute-done.refs_1_, bf16[2048,512]{1,0:T(8,128)(2,1)} %refs_2_.4, bf16[2048,512]{1,0:T(8,128)(2,1)} %refs_3_.3), custom_call_target="tpu_custom_call" | custom-call | flops 805306368 | bytes 3670016 | tf_op jit(solution)/shard_map/project/pallas_call | solution.py:85
  11.9 1.3 %collective-permute-start.10 = (bf16[6,64,512]{2,1,0:T(8,128)(2,1)S(1)}, bf16[6,64,512]{2,1,0:T(8,128)(2,1)S(1)}, u32[]{:S(2)}, u32[]{:S(2)}) collective-permute-start(bf16[6,64,512]{2,1,0:T(8,128)(2,1)S(1)} %bitcast.2), channel_id=1, source_target_pairs={{0,8},{2,10},{4,12},{6,14},{8,16},{10,18},{12,20},{14,22},{16,24},... | collective-permute-start | bytes 1179656 | tf_op jit(solution)/shard_map/ppermute | solution.py:41
  13.3 4.3 %collective-permute-done.1.refs_3_ = bf16[6,64,512]{2,1,0:T(8,128)(2,1)S(1)} collective-permute-done((bf16[6,64,512]{2,1,0:T(8,128)(2,1)S(1)}, bf16[6,64,512]{2,1,0:T(8,128)(2,1)S(1)}, u32[]{:S(2)}, u32[]{:S(2)}) %collective-permute-start.1) | collective-permute-done | bytes 393248 | tf_op jit(solution)/shard_map/ppermute | solution.py:41
  17.6 1.3 %collective-permute-start.2 = (bf16[6,64,512]{2,1,0:T(8,128)(2,1)S(1)}, bf16[6,64,512]{2,1,0:T(8,128)(2,1)S(1)}, u32[]{:S(2)}, u32[]{:S(2)}) collective-permute-start(bf16[6,64,512]{2,1,0:T(8,128)(2,1)S(1)} %collective-permute-done.1.refs_3_), channel_id=1, source_target_pairs={{0,8},{2,10},{4,12},{6,14},{8,16},{10,18},{12,20},{14,22},{16,24},... | collective-permute-start | bytes 1179656 | tf_op jit(solution)/shard_map/ppermute | solution.py:41
  18.9 7.1 %collective-permute-done.10.refs_4_.refs_3_ = bf16[6,64,512]{2,1,0:T(8,128)(2,1)S(1)} collective-permute-done((bf16[6,64,512]{2,1,0:T(8,128)(2,1)S(1)}, bf16[6,64,512]{2,1,0:T(8,128)(2,1)S(1)}, u32[]{:S(2)}, u32[]{:S(2)}) %collective-permute-start.10) | collective-permute-done | bytes 393248 | tf_op jit(solution)/shard_map/ppermute | solution.py:41
  26.0 1.3 %collective-permute-start.20 = (bf16[6,64,512]{2,1,0:T(8,128)(2,1)S(1)}, bf16[6,64,512]{2,1,0:T(8,128)(2,1)S(1)}, u32[]{:S(2)}, u32[]{:S(2)}) collective-permute-start(bf16[6,64,512]{2,1,0:T(8,128)(2,1)S(1)} %collective-permute-done.10.refs_4_.refs_3_), channel_id=1, source_target_pairs={{0,8},{2,10},{4,12},{6,14},{8,16},{10,18},{12,20},{14,22},{16,24},... | collective-permute-start | bytes 1179656 | tf_op jit(solution)/shard_map/ppermute | solution.py:41
  27.3 5.0 %index.1 = (s32[192]{0:T(256)S(1)}, s32[8]{0:T(128)S(1)}, s32[8]{0:T(128)S(1)}, s32[8]{0:T(128)S(1)}) custom-call(s32[6,16]{1,0:T(8,128)S(1)} %copy-done.2), custom_call_target="tpu_custom_call" | custom-call | tf_op jit(solution)/shard_map/index/pallas_call | solution.py:197
  32.9 2.2 %collective-permute-start.6 = (s32[8]{0:T(128)S(1)}, s32[8]{0:T(128)S(1)}, u32[]{:S(2)}, u32[]{:S(2)}) collective-permute-start(s32[8]{0:T(128)S(1)} %get-tuple-element.41), channel_id=1, source_target_pairs={{0,6},{2,4},{4,2},{6,0},{8,14},{10,12},{12,10},{14,8},{16,22},{18,... | collective-permute-start | bytes 104 | tf_op jit(solution)/shard_map/ppermute | solution.py:41
  35.4 0.8 collective-permute-done.6.refs_2_
  36.2 0.8 pick.6
  37.0 1.3 %collective-permute-start.7 = (bf16[2,64,1024]{2,1,0:T(8,128)(2,1)S(1)}, bf16[2,64,1024]{2,1,0:T(8,128)(2,1)S(1)}, u32[]{:S(2)}, u32[]{:S(2)}) collective-permute-start(bf16[2,64,1024]{2,1,0:T(8,128)(2,1)S(1)} %get-tuple-element.42), channel_id=1, source_target_pairs={{0,2},{2,0},{4,6},{6,4},{8,10},{10,8},{12,14},{14,12},{16,18},{18,... | collective-permute-start | bytes 786440 | tf_op jit(solution)/shard_map/ppermute | solution.py:41
  38.3 1.3 %collective-permute-start.3 = (bf16[6,64,512]{2,1,0:T(8,128)(2,1)S(1)}, bf16[6,64,512]{2,1,0:T(8,128)(2,1)S(1)}, u32[]{:S(2)}, u32[]{:S(2)}) collective-permute-start(bf16[6,64,512]{2,1,0:T(8,128)(2,1)S(1)} %collective-permute-done.2.refs_3_.refs_4_), channel_id=1, source_target_pairs={{0,8},{2,10},{4,12},{6,14},{8,16},{10,18},{12,20},{14,22},{16,24},... | collective-permute-start | bytes 1179656 | tf_op jit(solution)/shard_map/ppermute | solution.py:41
  39.6 1.2 %collective-permute-start.8 = (bf16[2,64,1024]{2,1,0:T(8,128)(2,1)S(1)}, bf16[2,64,1024]{2,1,0:T(8,128)(2,1)S(1)}, u32[]{:S(2)}, u32[]{:S(2)}) collective-permute-start(bf16[2,64,1024]{2,1,0:T(8,128)(2,1)S(1)} %get-tuple-element.43), channel_id=1, source_target_pairs={{0,4},{2,6},{4,0},{6,2},{8,12},{10,14},{12,8},{14,10},{16,20},{18,... | collective-permute-start | bytes 786440 | tf_op jit(solution)/shard_map/ppermute | solution.py:41
  41.0 0.8 pick.7
  41.9 0.7 collective-permute-done.7.refs_6_
  42.6 1.2 %collective-permute-start.11 = (bf16[2,64,1024]{2,1,0:T(8,128)(2,1)S(1)}, bf16[2,64,1024]{2,1,0:T(8,128)(2,1)S(1)}, u32[]{:S(2)}, u32[]{:S(2)}) collective-permute-start(bf16[2,64,1024]{2,1,0:T(8,128)(2,1)S(1)} %get-tuple-element.45), channel_id=1, source_target_pairs={{0,2},{2,0},{4,6},{6,4},{8,10},{10,8},{12,14},{14,12},{16,18},{18,... | collective-permute-start | bytes 786440 | tf_op jit(solution)/shard_map/ppermute | solution.py:41
  43.8 1.3 %collective-permute-start.21 = (bf16[6,64,512]{2,1,0:T(8,128)(2,1)S(1)}, bf16[6,64,512]{2,1,0:T(8,128)(2,1)S(1)}, u32[]{:S(2)}, u32[]{:S(2)}) collective-permute-start(bf16[6,64,512]{2,1,0:T(8,128)(2,1)S(1)} %collective-permute-done.20.refs_3_.refs_4_), channel_id=1, source_target_pairs={{0,8},{2,10},{4,12},{6,14},{8,16},{10,18},{12,20},{14,22},{16,24},... | collective-permute-start | bytes 1179656 | tf_op jit(solution)/shard_map/ppermute | solution.py:41
  45.1 1.5 %collective-permute-done.8.refs_7_ = bf16[2,64,1024]{2,1,0:T(8,128)(2,1)S(1)} collective-permute-done((bf16[2,64,1024]{2,1,0:T(8,128)(2,1)S(1)}, bf16[2,64,1024]{2,1,0:T(8,128)(2,1)S(1)}, u32[]{:S(2)}, u32[]{:S(2)}) %collective-permute-start.8) | collective-permute-done | bytes 262176 | tf_op jit(solution)/shard_map/ppermute | solution.py:41
  46.6 2.4 %collective-permute-start.12 = (bf16[2,64,1024]{2,1,0:T(8,128)(2,1)S(1)}, bf16[2,64,1024]{2,1,0:T(8,128)(2,1)S(1)}, u32[]{:S(2)}, u32[]{:S(2)}) collective-permute-start(bf16[2,64,1024]{2,1,0:T(8,128)(2,1)S(1)} %get-tuple-element.46), channel_id=1, source_target_pairs={{0,4},{2,6},{4,0},{6,2},{8,12},{10,14},{12,8},{14,10},{16,20},{18,... | collective-permute-start | bytes 786440 | tf_op jit(solution)/shard_map/ppermute | solution.py:41
  49.1 0.6 collective-permute-start.13
  49.6 1.1 %pick.8 = (bf16[2,64,512]{2,1,0:T(8,128)(2,1)S(1)}, bf16[2,64,512]{2,1,0:T(8,128)(2,1)S(1)}, bf16[2,64,512]{2,1,0:T(8,128)(2,1)S(1)}) custom-call(s32[8]{0:T(128)S(1)} %collective-permute-done.4.refs_0_, s32[8]{0:T(128)S(1)} %collective-permute-done.5.refs_1_, s32[8]{0:T(128)S(1)} %collective-permute-done.6.refs_2_, ...), custom_call_target="tpu_custom_call" | custom-call | tf_op jit(solution)/shard_map/pick/pallas_call | solution.py:243
  50.8 3.1 %collective-permute-done.11.refs_9_ = bf16[2,64,1024]{2,1,0:T(8,128)(2,1)S(1)} collective-permute-done((bf16[2,64,1024]{2,1,0:T(8,128)(2,1)S(1)}, bf16[2,64,1024]{2,1,0:T(8,128)(2,1)S(1)}, u32[]{:S(2)}, u32[]{:S(2)}) %collective-permute-start.11) | collective-permute-done | bytes 262176 | tf_op jit(solution)/shard_map/ppermute | solution.py:41
  53.9 1.2 %collective-permute-start.15 = (bf16[2,64,512]{2,1,0:T(8,128)(2,1)S(1)}, bf16[2,64,512]{2,1,0:T(8,128)(2,1)S(1)}, u32[]{:S(2)}, u32[]{:S(2)}) collective-permute-start(bf16[2,64,512]{2,1,0:T(8,128)(2,1)S(1)} %get-tuple-element.49), channel_id=1, source_target_pairs={{0,4},{2,6},{4,0},{6,2},{8,12},{10,14},{12,8},{14,10},{16,20},{18,... | collective-permute-start | bytes 393224 | tf_op jit(solution)/shard_map/ppermute | solution.py:41
  55.2 4.0 %project.5.refs_1_ = bf16[384,1024]{1,0:T(8,128)(2,1)S(1)} custom-call(bf16[384,1024]{1,0:T(8,128)(2,1)S(1)} %copy-done, bf16[384,1024]{1,0:T(8,128)(2,1)S(1)} %collective-permute-done.refs_1_, bf16[2048,1024]{1,0:T(8,128)(2,1)} %refs_2_.5), custom_call_target="tpu_custom_call" | custom-call | flops 1610612736 | bytes 5767168 | tf_op jit(solution)/shard_map/project/pallas_call | solution.py:85
  59.2 1.1 %pick.10 = (bf16[2,64,512]{2,1,0:T(8,128)(2,1)S(1)}, bf16[2,64,512]{2,1,0:T(8,128)(2,1)S(1)}, bf16[2,64,512]{2,1,0:T(8,128)(2,1)S(1)}) custom-call(s32[8]{0:T(128)S(1)} %collective-permute-done.4.refs_0_, s32[8]{0:T(128)S(1)} %collective-permute-done.5.refs_1_, s32[8]{0:T(128)S(1)} %collective-permute-done.6.refs_2_, ...), custom_call_target="tpu_custom_call" | custom-call | tf_op jit(solution)/shard_map/pick/pallas_call | solution.py:243
  60.3 1.1 %pick.9 = (bf16[2,64,512]{2,1,0:T(8,128)(2,1)S(1)}, bf16[2,64,512]{2,1,0:T(8,128)(2,1)S(1)}, bf16[2,64,512]{2,1,0:T(8,128)(2,1)S(1)}) custom-call(s32[8]{0:T(128)S(1)} %collective-permute-done.4.refs_0_, s32[8]{0:T(128)S(1)} %collective-permute-done.5.refs_1_, s32[8]{0:T(128)S(1)} %collective-permute-done.6.refs_2_, ...), custom_call_target="tpu_custom_call" | custom-call | tf_op jit(solution)/shard_map/pick/pallas_call | solution.py:243
  61.5 1.5 %collective-permute-start.16 = (bf16[2,64,512]{2,1,0:T(8,128)(2,1)S(1)}, bf16[2,64,512]{2,1,0:T(8,128)(2,1)S(1)}, u32[]{:S(2)}, u32[]{:S(2)}) collective-permute-start(bf16[2,64,512]{2,1,0:T(8,128)(2,1)S(1)} %get-tuple-element.50), channel_id=1, source_target_pairs={{0,6},{2,4},{4,2},{6,0},{8,14},{10,12},{12,10},{14,8},{16,22},{18,... | collective-permute-start | bytes 393224 | tf_op jit(solution)/shard_map/ppermute | solution.py:41
  63.1 1.3 %collective-permute-start.17 = (bf16[2,64,512]{2,1,0:T(8,128)(2,1)S(1)}, bf16[2,64,512]{2,1,0:T(8,128)(2,1)S(1)}, u32[]{:S(2)}, u32[]{:S(2)}) collective-permute-start(bf16[2,64,512]{2,1,0:T(8,128)(2,1)S(1)} %get-tuple-element.52), channel_id=1, source_target_pairs={{0,2},{2,0},{4,6},{6,4},{8,10},{10,8},{12,14},{14,12},{16,18},{18,... | collective-permute-start | bytes 393224 | tf_op jit(solution)/shard_map/ppermute | solution.py:41
  64.5 2.6 %collective-permute-done.15.refs_13_ = bf16[2,64,512]{2,1,0:T(8,128)(2,1)S(1)} collective-permute-done((bf16[2,64,512]{2,1,0:T(8,128)(2,1)S(1)}, bf16[2,64,512]{2,1,0:T(8,128)(2,1)S(1)}, u32[]{:S(2)}, u32[]{:S(2)}) %collective-permute-start.15) | collective-permute-done | bytes 131104 | tf_op jit(solution)/shard_map/ppermute | solution.py:41
  67.1 1.5 %collective-permute-start.18 = (bf16[2,64,512]{2,1,0:T(8,128)(2,1)S(1)}, bf16[2,64,512]{2,1,0:T(8,128)(2,1)S(1)}, u32[]{:S(2)}, u32[]{:S(2)}) collective-permute-start(bf16[2,64,512]{2,1,0:T(8,128)(2,1)S(1)} %get-tuple-element.53), channel_id=1, source_target_pairs={{0,4},{2,6},{4,0},{6,2},{8,12},{10,14},{12,8},{14,10},{16,20},{18,... | collective-permute-start | bytes 393224 | tf_op jit(solution)/shard_map/ppermute | solution.py:41
  68.5 0.8 collective-permute-start.19
  69.3 1.1 %pick.11 = (bf16[2,64,512]{2,1,0:T(8,128)(2,1)S(1)}, bf16[2,64,512]{2,1,0:T(8,128)(2,1)S(1)}, bf16[2,64,512]{2,1,0:T(8,128)(2,1)S(1)}) custom-call(s32[8]{0:T(128)S(1)} %collective-permute-done.4.refs_0_, s32[8]{0:T(128)S(1)} %collective-permute-done.5.refs_1_, s32[8]{0:T(128)S(1)} %collective-permute-done.6.refs_2_, ...), custom_call_target="tpu_custom_call" | custom-call | tf_op jit(solution)/shard_map/pick/pallas_call | solution.py:243
  70.5 1.5 %collective-permute-start.23 = (bf16[2,64,512]{2,1,0:T(8,128)(2,1)S(1)}, bf16[2,64,512]{2,1,0:T(8,128)(2,1)S(1)}, u32[]{:S(2)}, u32[]{:S(2)}) collective-permute-start(bf16[2,64,512]{2,1,0:T(8,128)(2,1)S(1)} %get-tuple-element.56), channel_id=1, source_target_pairs={{0,4},{2,6},{4,0},{6,2},{8,12},{10,14},{12,8},{14,10},{16,20},{18,... | collective-permute-start | bytes 393224 | tf_op jit(solution)/shard_map/ppermute | solution.py:41
  72.2 1.1 %collective-permute-start.25 = (bf16[2,64,512]{2,1,0:T(8,128)(2,1)S(1)}, bf16[2,64,512]{2,1,0:T(8,128)(2,1)S(1)}, u32[]{:S(2)}, u32[]{:S(2)}) collective-permute-start(bf16[2,64,512]{2,1,0:T(8,128)(2,1)S(1)} %get-tuple-element.58), channel_id=1, source_target_pairs={{0,2},{2,0},{4,6},{6,4},{8,10},{10,8},{12,14},{14,12},{16,18},{18,... | collective-permute-start | bytes 393224 | tf_op jit(solution)/shard_map/ppermute | solution.py:41
  73.3 1.4 %collective-permute-start.26 = (bf16[2,64,512]{2,1,0:T(8,128)(2,1)S(1)}, bf16[2,64,512]{2,1,0:T(8,128)(2,1)S(1)}, u32[]{:S(2)}, u32[]{:S(2)}) collective-permute-start(bf16[2,64,512]{2,1,0:T(8,128)(2,1)S(1)} %get-tuple-element.59), channel_id=1, source_target_pairs={{0,4},{2,6},{4,0},{6,2},{8,12},{10,14},{12,8},{14,10},{16,20},{18,... | collective-permute-start | bytes 393224 | tf_op jit(solution)/shard_map/ppermute | solution.py:41
  74.9 4.5 %attend.2.refs_0_ = bf16[384,512]{1,0:T(8,128)(2,1)S(1)} custom-call(s32[192]{0:T(256)S(1)} %get-tuple-element.37.refs_0_, bf16[384,1024]{1,0:T(8,128)(2,1)S(1)} %project.5.refs_1_, bf16[6,64,512]{2,1,0:T(8,128)(2,1)S(1)} %bitcast.7, bf16[6,64,512]{2,1,0:T(8,128)(2,1)S(1)} %collective-permute-done.1.refs_3_, ...), custom_call_target="tpu_custom_call" | custom-call | flops 805306368 | bytes 3932160 | tf_op jit(solution)/shard_map/attend/pallas_call | solution.py:325
  79.5 0.7 collective-permute-done.25.refs_15_
  80.6 3.6 %collective-permute-done.27.refs_17_ = bf16[2,64,512]{2,1,0:T(8,128)(2,1)S(1)} collective-permute-done((bf16[2,64,512]{2,1,0:T(8,128)(2,1)S(1)}, bf16[2,64,512]{2,1,0:T(8,128)(2,1)S(1)}, u32[]{:S(2)}, u32[]{:S(2)}) %collective-permute-start.27) | collective-permute-done | bytes 131104 | tf_op jit(solution)/shard_map/ppermute | solution.py:41
  84.2 4.5 %attend.3.refs_2_ = bf16[384,512]{1,0:T(8,128)(2,1)S(1)} custom-call(s32[192]{0:T(256)S(1)} %get-tuple-element.37.refs_0_, bf16[384,1024]{1,0:T(8,128)(2,1)S(1)} %project.5.refs_1_, bf16[6,64,512]{2,1,0:T(8,128)(2,1)S(1)} %bitcast.4, bf16[6,64,512]{2,1,0:T(8,128)(2,1)S(1)} %collective-permute-done.10.refs_4_.refs_3_, ...), custom_call_target="tpu_custom_call" | custom-call | flops 805306368 | bytes 3932160 | tf_op jit(solution)/shard_map/attend/pallas_call | solution.py:325
  88.7 7.0 %collective-permute-start.28 = (bf16[384,512]{1,0:T(8,128)(2,1)S(1)}, bf16[384,512]{1,0:T(8,128)(2,1)S(1)}, u32[]{:S(2)}, u32[]{:S(2)}) collective-permute-start(bf16[384,512]{1,0:T(8,128)(2,1)S(1)} %attend.2.refs_0_), channel_id=1, source_target_pairs={{0,1},{1,0},{2,3},{3,2},{4,5},{5,4},{6,7},{7,6},{8,9},{9,8},{10,11... | collective-permute-start | bytes 1179656 | tf_op jit(solution)/shard_map/ppermute | solution.py:49
  95.8 1.3 %collective-permute-done.28.refs_1_ = bf16[384,512]{1,0:T(8,128)(2,1)S(1)} collective-permute-done((bf16[384,512]{1,0:T(8,128)(2,1)S(1)}, bf16[384,512]{1,0:T(8,128)(2,1)S(1)}, u32[]{:S(2)}, u32[]{:S(2)}) %collective-permute-start.28) | collective-permute-done | bytes 393248 | tf_op jit(solution)/shard_map/ppermute | solution.py:49
  97.1 0.6 collective-permute-done.29.refs_3_
  97.6 2.7 %mix.1 = bf16[384,1024]{1,0:T(8,128)(2,1)} custom-call(bf16[384,512]{1,0:T(8,128)(2,1)S(1)} %attend.2.refs_0_, bf16[384,512]{1,0:T(8,128)(2,1)S(1)} %collective-permute-done.28.refs_1_, bf16[384,512]{1,0:T(8,128)(2,1)S(1)} %attend.3.refs_2_, bf16[384,512]{1,0:T(8,128)(2,1)S(1)} %collective-permute-done.29.refs_3_, bf16[2048,1024]{1,0:T(8,128)(2,1)S(1)} %copy-done.1), custom_call_target="tpu_custom_call" | custom-call | flops 1610612736 | bytes 6553600 | tf_op jit(solution)/shard_map/mix/pallas_call | solution.py:128
  (31 shorter events, 2.1 us)
Async XLA Ops:
  0.0 2.8 %collective-permute-start = (bf16[384,1024]{1,0:T(8,128)(2,1)}, bf16[384,1024]{1,0:T(8,128)(2,1)S(1)}, u32[]{:S(2)}, u32[]{:S(2)}) collective-permute-start(bf16[384,1024]{1,0:T(8,128)(2,1)} %refs_0_.3), channel_id=1, source_target_pairs={{0,1},{1,0},{2,3},{3,2},{4,5},{5,4},{6,7},{7,6},{8,9},{9,8},{10,11... | collective-permute-start | bytes 2359304 | tf_op jit(solution)/shard_map/ppermute | solution.py:49
  2.8 1.1 %copy-start = (bf16[384,1024]{1,0:T(8,128)(2,1)S(1)}, bf16[384,1024]{1,0:T(8,128)(2,1)}, u32[]{:S(2)}) copy-start(bf16[384,1024]{1,0:T(8,128)(2,1)} %refs_0_.3) | copy-start | bytes 2359300
  7.3 20.1 %copy-start.2 = (s32[6,16]{1,0:T(8,128)S(1)}, s32[6,16]{1,0:T(8,128)}, u32[]{:S(2)}) copy-start(s32[6,16]{1,0:T(8,128)} %chosen_ref) | copy-start | bytes 1156
  7.3 10.3 %collective-permute-start.1 = (bf16[6,64,512]{2,1,0:T(8,128)(2,1)S(1)}, bf16[6,64,512]{2,1,0:T(8,128)(2,1)S(1)}, u32[]{:S(2)}, u32[]{:S(2)}) collective-permute-start(bf16[6,64,512]{2,1,0:T(8,128)(2,1)S(1)} %bitcast.5), channel_id=1, source_target_pairs={{0,8},{2,10},{4,12},{6,14},{8,16},{10,18},{12,20},{14,22},{16,24},... | collective-permute-start | bytes 1179656 | tf_op jit(solution)/shard_map/ppermute | solution.py:41
  11.9 14.1 %collective-permute-start.10 = (bf16[6,64,512]{2,1,0:T(8,128)(2,1)S(1)}, bf16[6,64,512]{2,1,0:T(8,128)(2,1)S(1)}, u32[]{:S(2)}, u32[]{:S(2)}) collective-permute-start(bf16[6,64,512]{2,1,0:T(8,128)(2,1)S(1)} %bitcast.2), channel_id=1, source_target_pairs={{0,8},{2,10},{4,12},{6,14},{8,16},{10,18},{12,20},{14,22},{16,24},... | collective-permute-start | bytes 1179656 | tf_op jit(solution)/shard_map/ppermute | solution.py:41
  17.6 20.7 %collective-permute-start.2 = (bf16[6,64,512]{2,1,0:T(8,128)(2,1)S(1)}, bf16[6,64,512]{2,1,0:T(8,128)(2,1)S(1)}, u32[]{:S(2)}, u32[]{:S(2)}) collective-permute-start(bf16[6,64,512]{2,1,0:T(8,128)(2,1)S(1)} %collective-permute-done.1.refs_3_), channel_id=1, source_target_pairs={{0,8},{2,10},{4,12},{6,14},{8,16},{10,18},{12,20},{14,22},{16,24},... | collective-permute-start | bytes 1179656 | tf_op jit(solution)/shard_map/ppermute | solution.py:41
  26.0 17.8 %collective-permute-start.20 = (bf16[6,64,512]{2,1,0:T(8,128)(2,1)S(1)}, bf16[6,64,512]{2,1,0:T(8,128)(2,1)S(1)}, u32[]{:S(2)}, u32[]{:S(2)}) collective-permute-start(bf16[6,64,512]{2,1,0:T(8,128)(2,1)S(1)} %collective-permute-done.10.refs_4_.refs_3_), channel_id=1, source_target_pairs={{0,8},{2,10},{4,12},{6,14},{8,16},{10,18},{12,20},{14,22},{16,24},... | collective-permute-start | bytes 1179656 | tf_op jit(solution)/shard_map/ppermute | solution.py:41
  32.3 2.8 %collective-permute-start.4 = (s32[8]{0:T(128)S(1)}, s32[8]{0:T(128)S(1)}, u32[]{:S(2)}, u32[]{:S(2)}) collective-permute-start(s32[8]{0:T(128)S(1)} %get-tuple-element.39), channel_id=1, source_target_pairs={{0,2},{2,0},{4,6},{6,4},{8,10},{10,8},{12,14},{14,12},{16,18},{18,... | collective-permute-start | bytes 104 | tf_op jit(solution)/shard_map/ppermute | solution.py:41
  32.7 2.7 %collective-permute-start.5 = (s32[8]{0:T(128)S(1)}, s32[8]{0:T(128)S(1)}, u32[]{:S(2)}, u32[]{:S(2)}) collective-permute-start(s32[8]{0:T(128)S(1)} %get-tuple-element.40), channel_id=1, source_target_pairs={{0,4},{2,6},{4,0},{6,2},{8,12},{10,14},{12,8},{14,10},{16,20},{18,... | collective-permute-start | bytes 104 | tf_op jit(solution)/shard_map/ppermute | solution.py:41
  32.9 3.3 %collective-permute-start.6 = (s32[8]{0:T(128)S(1)}, s32[8]{0:T(128)S(1)}, u32[]{:S(2)}, u32[]{:S(2)}) collective-permute-start(s32[8]{0:T(128)S(1)} %get-tuple-element.41), channel_id=1, source_target_pairs={{0,6},{2,4},{4,2},{6,0},{8,14},{10,12},{12,10},{14,8},{16,22},{18,... | collective-permute-start | bytes 104 | tf_op jit(solution)/shard_map/ppermute | solution.py:41
  37.0 5.6 %collective-permute-start.7 = (bf16[2,64,1024]{2,1,0:T(8,128)(2,1)S(1)}, bf16[2,64,1024]{2,1,0:T(8,128)(2,1)S(1)}, u32[]{:S(2)}, u32[]{:S(2)}) collective-permute-start(bf16[2,64,1024]{2,1,0:T(8,128)(2,1)S(1)} %get-tuple-element.42), channel_id=1, source_target_pairs={{0,2},{2,0},{4,6},{6,4},{8,10},{10,8},{12,14},{14,12},{16,18},{18,... | collective-permute-start | bytes 786440 | tf_op jit(solution)/shard_map/ppermute | solution.py:41
  38.3 15.6 %collective-permute-start.3 = (bf16[6,64,512]{2,1,0:T(8,128)(2,1)S(1)}, bf16[6,64,512]{2,1,0:T(8,128)(2,1)S(1)}, u32[]{:S(2)}, u32[]{:S(2)}) collective-permute-start(bf16[6,64,512]{2,1,0:T(8,128)(2,1)S(1)} %collective-permute-done.2.refs_3_.refs_4_), channel_id=1, source_target_pairs={{0,8},{2,10},{4,12},{6,14},{8,16},{10,18},{12,20},{14,22},{16,24},... | collective-permute-start | bytes 1179656 | tf_op jit(solution)/shard_map/ppermute | solution.py:41
  39.6 7.0 %collective-permute-start.8 = (bf16[2,64,1024]{2,1,0:T(8,128)(2,1)S(1)}, bf16[2,64,1024]{2,1,0:T(8,128)(2,1)S(1)}, u32[]{:S(2)}, u32[]{:S(2)}) collective-permute-start(bf16[2,64,1024]{2,1,0:T(8,128)(2,1)S(1)} %get-tuple-element.43), channel_id=1, source_target_pairs={{0,4},{2,6},{4,0},{6,2},{8,12},{10,14},{12,8},{14,10},{16,20},{18,... | collective-permute-start | bytes 786440 | tf_op jit(solution)/shard_map/ppermute | solution.py:41
  40.8 8.2 %collective-permute-start.9 = (bf16[2,64,1024]{2,1,0:T(8,128)(2,1)S(1)}, bf16[2,64,1024]{2,1,0:T(8,128)(2,1)S(1)}, u32[]{:S(2)}, u32[]{:S(2)}) collective-permute-start(bf16[2,64,1024]{2,1,0:T(8,128)(2,1)S(1)} %get-tuple-element.44), channel_id=1, source_target_pairs={{0,6},{2,4},{4,2},{6,0},{8,14},{10,12},{12,10},{14,8},{16,22},{18,... | collective-permute-start | bytes 786440 | tf_op jit(solution)/shard_map/ppermute | solution.py:41
  42.6 11.3 %collective-permute-start.11 = (bf16[2,64,1024]{2,1,0:T(8,128)(2,1)S(1)}, bf16[2,64,1024]{2,1,0:T(8,128)(2,1)S(1)}, u32[]{:S(2)}, u32[]{:S(2)}) collective-permute-start(bf16[2,64,1024]{2,1,0:T(8,128)(2,1)S(1)} %get-tuple-element.45), channel_id=1, source_target_pairs={{0,2},{2,0},{4,6},{6,4},{8,10},{10,8},{12,14},{14,12},{16,18},{18,... | collective-permute-start | bytes 786440 | tf_op jit(solution)/shard_map/ppermute | solution.py:41
  43.8 24.7 %collective-permute-start.21 = (bf16[6,64,512]{2,1,0:T(8,128)(2,1)S(1)}, bf16[6,64,512]{2,1,0:T(8,128)(2,1)S(1)}, u32[]{:S(2)}, u32[]{:S(2)}) collective-permute-start(bf16[6,64,512]{2,1,0:T(8,128)(2,1)S(1)} %collective-permute-done.20.refs_3_.refs_4_), channel_id=1, source_target_pairs={{0,8},{2,10},{4,12},{6,14},{8,16},{10,18},{12,20},{14,22},{16,24},... | collective-permute-start | bytes 1179656 | tf_op jit(solution)/shard_map/ppermute | solution.py:41
  46.6 14.9 %collective-permute-start.12 = (bf16[2,64,1024]{2,1,0:T(8,128)(2,1)S(1)}, bf16[2,64,1024]{2,1,0:T(8,128)(2,1)S(1)}, u32[]{:S(2)}, u32[]{:S(2)}) collective-permute-start(bf16[2,64,1024]{2,1,0:T(8,128)(2,1)S(1)} %get-tuple-element.46), channel_id=1, source_target_pairs={{0,4},{2,6},{4,0},{6,2},{8,12},{10,14},{12,8},{14,10},{16,20},{18,... | collective-permute-start | bytes 786440 | tf_op jit(solution)/shard_map/ppermute | solution.py:41
  49.1 13.9 %collective-permute-start.13 = (bf16[2,64,1024]{2,1,0:T(8,128)(2,1)S(1)}, bf16[2,64,1024]{2,1,0:T(8,128)(2,1)S(1)}, u32[]{:S(2)}, u32[]{:S(2)}) collective-permute-start(bf16[2,64,1024]{2,1,0:T(8,128)(2,1)S(1)} %get-tuple-element.47), channel_id=1, source_target_pairs={{0,6},{2,4},{4,2},{6,0},{8,14},{10,12},{12,10},{14,8},{16,22},{18,... | collective-permute-start | bytes 786440 | tf_op jit(solution)/shard_map/ppermute | solution.py:41
  53.9 9.2 %collective-permute-start.14 = (bf16[2,64,512]{2,1,0:T(8,128)(2,1)S(1)}, bf16[2,64,512]{2,1,0:T(8,128)(2,1)S(1)}, u32[]{:S(2)}, u32[]{:S(2)}) collective-permute-start(bf16[2,64,512]{2,1,0:T(8,128)(2,1)S(1)} %get-tuple-element.48), channel_id=1, source_target_pairs={{0,2},{2,0},{4,6},{6,4},{8,10},{10,8},{12,14},{14,12},{16,18},{18,... | collective-permute-start | bytes 393224 | tf_op jit(solution)/shard_map/ppermute | solution.py:41
  53.9 13.1 %collective-permute-start.15 = (bf16[2,64,512]{2,1,0:T(8,128)(2,1)S(1)}, bf16[2,64,512]{2,1,0:T(8,128)(2,1)S(1)}, u32[]{:S(2)}, u32[]{:S(2)}) collective-permute-start(bf16[2,64,512]{2,1,0:T(8,128)(2,1)S(1)} %get-tuple-element.49), channel_id=1, source_target_pairs={{0,4},{2,6},{4,0},{6,2},{8,12},{10,14},{12,8},{14,10},{16,20},{18,... | collective-permute-start | bytes 393224 | tf_op jit(solution)/shard_map/ppermute | solution.py:41
  61.5 9.0 %collective-permute-start.16 = (bf16[2,64,512]{2,1,0:T(8,128)(2,1)S(1)}, bf16[2,64,512]{2,1,0:T(8,128)(2,1)S(1)}, u32[]{:S(2)}, u32[]{:S(2)}) collective-permute-start(bf16[2,64,512]{2,1,0:T(8,128)(2,1)S(1)} %get-tuple-element.50), channel_id=1, source_target_pairs={{0,6},{2,4},{4,2},{6,0},{8,14},{10,12},{12,10},{14,8},{16,22},{18,... | collective-permute-start | bytes 393224 | tf_op jit(solution)/shard_map/ppermute | solution.py:41
  63.0 9.0 %collective-permute-start.22 = (bf16[2,64,512]{2,1,0:T(8,128)(2,1)S(1)}, bf16[2,64,512]{2,1,0:T(8,128)(2,1)S(1)}, u32[]{:S(2)}, u32[]{:S(2)}) collective-permute-start(bf16[2,64,512]{2,1,0:T(8,128)(2,1)S(1)} %get-tuple-element.55), channel_id=1, source_target_pairs={{0,2},{2,0},{4,6},{6,4},{8,10},{10,8},{12,14},{14,12},{16,18},{18,... | collective-permute-start | bytes 393224 | tf_op jit(solution)/shard_map/ppermute | solution.py:41
  63.1 9.1 %collective-permute-start.17 = (bf16[2,64,512]{2,1,0:T(8,128)(2,1)S(1)}, bf16[2,64,512]{2,1,0:T(8,128)(2,1)S(1)}, u32[]{:S(2)}, u32[]{:S(2)}) collective-permute-start(bf16[2,64,512]{2,1,0:T(8,128)(2,1)S(1)} %get-tuple-element.52), channel_id=1, source_target_pairs={{0,2},{2,0},{4,6},{6,4},{8,10},{10,8},{12,14},{14,12},{16,18},{18,... | collective-permute-start | bytes 393224 | tf_op jit(solution)/shard_map/ppermute | solution.py:41
  67.1 6.2 %collective-permute-start.18 = (bf16[2,64,512]{2,1,0:T(8,128)(2,1)S(1)}, bf16[2,64,512]{2,1,0:T(8,128)(2,1)S(1)}, u32[]{:S(2)}, u32[]{:S(2)}) collective-permute-start(bf16[2,64,512]{2,1,0:T(8,128)(2,1)S(1)} %get-tuple-element.53), channel_id=1, source_target_pairs={{0,4},{2,6},{4,0},{6,2},{8,12},{10,14},{12,8},{14,10},{16,20},{18,... | collective-permute-start | bytes 393224 | tf_op jit(solution)/shard_map/ppermute | solution.py:41
  68.5 6.1 %collective-permute-start.19 = (bf16[2,64,512]{2,1,0:T(8,128)(2,1)S(1)}, bf16[2,64,512]{2,1,0:T(8,128)(2,1)S(1)}, u32[]{:S(2)}, u32[]{:S(2)}) collective-permute-start(bf16[2,64,512]{2,1,0:T(8,128)(2,1)S(1)} %get-tuple-element.54), channel_id=1, source_target_pairs={{0,6},{2,4},{4,2},{6,0},{8,14},{10,12},{12,10},{14,8},{16,22},{18,... | collective-permute-start | bytes 393224 | tf_op jit(solution)/shard_map/ppermute | solution.py:41
  70.5 8.9 %collective-permute-start.23 = (bf16[2,64,512]{2,1,0:T(8,128)(2,1)S(1)}, bf16[2,64,512]{2,1,0:T(8,128)(2,1)S(1)}, u32[]{:S(2)}, u32[]{:S(2)}) collective-permute-start(bf16[2,64,512]{2,1,0:T(8,128)(2,1)S(1)} %get-tuple-element.56), channel_id=1, source_target_pairs={{0,4},{2,6},{4,0},{6,2},{8,12},{10,14},{12,8},{14,10},{16,20},{18,... | collective-permute-start | bytes 393224 | tf_op jit(solution)/shard_map/ppermute | solution.py:41
  72.0 7.4 %collective-permute-start.24 = (bf16[2,64,512]{2,1,0:T(8,128)(2,1)S(1)}, bf16[2,64,512]{2,1,0:T(8,128)(2,1)S(1)}, u32[]{:S(2)}, u32[]{:S(2)}) collective-permute-start(bf16[2,64,512]{2,1,0:T(8,128)(2,1)S(1)} %get-tuple-element.57), channel_id=1, source_target_pairs={{0,6},{2,4},{4,2},{6,0},{8,14},{10,12},{12,10},{14,8},{16,22},{18,... | collective-permute-start | bytes 393224 | tf_op jit(solution)/shard_map/ppermute | solution.py:41
  72.2 8.0 %collective-permute-start.25 = (bf16[2,64,512]{2,1,0:T(8,128)(2,1)S(1)}, bf16[2,64,512]{2,1,0:T(8,128)(2,1)S(1)}, u32[]{:S(2)}, u32[]{:S(2)}) collective-permute-start(bf16[2,64,512]{2,1,0:T(8,128)(2,1)S(1)} %get-tuple-element.58), channel_id=1, source_target_pairs={{0,2},{2,0},{4,6},{6,4},{8,10},{10,8},{12,14},{14,12},{16,18},{18,... | collective-permute-start | bytes 393224 | tf_op jit(solution)/shard_map/ppermute | solution.py:41
  73.3 7.3 %collective-permute-start.26 = (bf16[2,64,512]{2,1,0:T(8,128)(2,1)S(1)}, bf16[2,64,512]{2,1,0:T(8,128)(2,1)S(1)}, u32[]{:S(2)}, u32[]{:S(2)}) collective-permute-start(bf16[2,64,512]{2,1,0:T(8,128)(2,1)S(1)} %get-tuple-element.59), channel_id=1, source_target_pairs={{0,4},{2,6},{4,0},{6,2},{8,12},{10,14},{12,8},{14,10},{16,20},{18,... | collective-permute-start | bytes 393224 | tf_op jit(solution)/shard_map/ppermute | solution.py:41
  74.7 9.5 %collective-permute-start.27 = (bf16[2,64,512]{2,1,0:T(8,128)(2,1)S(1)}, bf16[2,64,512]{2,1,0:T(8,128)(2,1)S(1)}, u32[]{:S(2)}, u32[]{:S(2)}) collective-permute-start(bf16[2,64,512]{2,1,0:T(8,128)(2,1)S(1)} %get-tuple-element.60), channel_id=1, source_target_pairs={{0,6},{2,4},{4,2},{6,0},{8,14},{10,12},{12,10},{14,8},{16,22},{18,... | collective-permute-start | bytes 393224 | tf_op jit(solution)/shard_map/ppermute | solution.py:41
  74.9 22.7 %copy-start.1 = (bf16[2048,1024]{1,0:T(8,128)(2,1)S(1)}, bf16[2048,1024]{1,0:T(8,128)(2,1)}, u32[]{:S(2)}) copy-start(bf16[2048,1024]{1,0:T(8,128)(2,1)} %refs_4_.1) | copy-start | bytes 12582916
  88.7 8.4 %collective-permute-start.28 = (bf16[384,512]{1,0:T(8,128)(2,1)S(1)}, bf16[384,512]{1,0:T(8,128)(2,1)S(1)}, u32[]{:S(2)}, u32[]{:S(2)}) collective-permute-start(bf16[384,512]{1,0:T(8,128)(2,1)S(1)} %attend.2.refs_0_), channel_id=1, source_target_pairs={{0,1},{1,0},{2,3},{3,2},{4,5},{5,4},{6,7},{7,6},{8,9},{9,8},{10,11... | collective-permute-start | bytes 1179656 | tf_op jit(solution)/shard_map/ppermute | solution.py:49
  95.7 1.9 %collective-permute-start.29 = (bf16[384,512]{1,0:T(8,128)(2,1)S(1)}, bf16[384,512]{1,0:T(8,128)(2,1)S(1)}, u32[]{:S(2)}, u32[]{:S(2)}) collective-permute-start(bf16[384,512]{1,0:T(8,128)(2,1)S(1)} %attend.3.refs_2_), channel_id=1, source_target_pairs={{0,1},{1,0},{2,3},{3,2},{4,5},{5,4},{6,7},{7,6},{8,9},{9,8},{10,11... | collective-permute-start | bytes 1179656 | tf_op jit(solution)/shard_map/ppermute | solution.py:49

commit v2 on v1

--- a/solution.py
+++ b/solution.py
@@ -101,51 +101,130 @@
     )(*pieces, *[far(weight) for weight in weights])
 
 
-def mix_kernel(streams, *refs):
-    pieces = refs[:-2]
-    weight_ref, out_ref = refs[-2:]
-    count = len(pieces) // streams
+def front_kernel(others, cols, own_in, key_ref, value_ref, own_ref, part_ref, rest_ref, held, sems):
+    width = own_ref.shape[1]
+    me = lax.axis_index("tp")
+    own_copy = pltpu.make_async_copy(own_in, own_ref, sems.at[0, 0])
+    own_copy.start()
+    copies = []
+    for s in range(others + 1):
+        at = pl.multiple_of(lax.rem(me + s, others + 1) * width, width)
+        for i, ref in enumerate((key_ref, value_ref)):
+            target = held.at[i] if s == 0 else rest_ref.at[s - 1, i]
+            copy = pltpu.make_async_copy(
+                ref.at[pl.ds(at, width), pl.ds(0, cols)], target, sems.at[1 + s, i]
+            )
+            copy.start()
+            copies.append(copy)
+    own_copy.wait()
+    for i in range(2):
+        copies[i].wait()
+        part_ref[:, i * cols : (i + 1) * cols] = jnp.dot(
+            own_ref[...], held[i], preferred_element_type=jnp.float32
+        )
+    for copy in copies[2:]:
+        copy.wait()
+
+
+def front(own, key_weight, value_weight, cols):
+    rows, width = own.shape
+    others = lax.axis_size("tp") - 1
+    return pl.pallas_call(
+        functools.partial(front_kernel, others, cols),
+        out_shape=[
+            pltpu.VMEM((rows, width), jnp.bfloat16),
+            pltpu.VMEM((rows, 2 * cols), jnp.float32),
+            pltpu.VMEM((others, 2, width, cols), jnp.bfloat16),
+        ],
+        in_specs=[ANY] * 3,
+        out_specs=[VMEM] * 3,
+        scratch_shapes=[
+            pltpu.VMEM((2, width, cols), jnp.bfloat16),
+            pltpu.SemaphoreType.DMA((others + 2, 2)),
+        ],
+        compiler_params=pltpu.CompilerParams(vmem_limit_bytes=16 << 20),
+        name="front",
+    )(far(own), far(key_weight), far(value_weight))
+
+
+def join_kernel(*refs):
+    others = refs[:-3]
+    part_ref, rest_ref, out_ref = refs[-3:]
+    cols = rest_ref.shape[3]
+    for i in range(2):
+        span = slice(i * cols, (i + 1) * cols)
+        total = part_ref[:, span]
+        for s, other in enumerate(others):
+            total = total + jnp.dot(
+                other[...], rest_ref[s, i], preferred_element_type=jnp.float32
+            )
+        out_ref[:, span] = total.astype(jnp.bfloat16)
+
+
+def join(others, part, rest):
+    return pl.pallas_call(
+        join_kernel,
+        out_shape=jax.ShapeDtypeStruct(part.shape, jnp.bfloat16),
+        in_specs=[VMEM] * (len(others) + 2),
+        out_specs=VMEM,
+        compiler_params=pltpu.CompilerParams(vmem_limit_bytes=16 << 20),
+        name="join",
+    )(*others, near(part), near(rest))
+
+
+def mix_kernel(stream, streams, more, *refs):
+    pieces = refs[: -2 - more]
+    weight_ref, out_ref = refs[-2 - more], refs[-1]
+    count = len(pieces)
     width = pieces[0].shape[1]
     step = min(2 * HD, out_ref.shape[1])
     me = lax.axis_index("tp")
-    starts = [
-        pl.multiple_of((lax.rem(me + s, count) * streams + t) * width, width)
-        for t in range(streams)
-        for s in range(count)
-    ]
     for col in range(0, out_ref.shape[1], step):
-        total = None
-        for at, piece in zip(starts, pieces):
-            rows = weight_ref[pl.ds(at, width), col : col + step]
+        span = slice(col, col + step)
+        total = refs[-2][:, span] if more else None
+        for s, piece in enumerate(pieces):
+            at = pl.multiple_of((lax.rem(me + s, count) * streams + stream) * width, width)
+            rows = weight_ref[pl.ds(at, width), span]
             term = jnp.dot(piece[...], rows, preferred_element_type=jnp.float32)
             total = term if total is None else total + term
-        out_ref[:, col : col + step] = total.astype(jnp.bfloat16)
-
-
-def mix(pieces, weight, streams):
-    rows, _ = pieces[0].shape
-    depth, cols = weight.shape
+        out_ref[:, span] = total.astype(out_ref.dtype)
+
+
+def mix(pieces, weight, stream, streams, before):
+    rows, width = pieces[0].shape
+    cols = weight.shape[1]
+    more = [] if before is None else [before]
+    kind = jnp.bfloat16 if stream == streams - 1 else jnp.float32
     return pl.pallas_call(
-        functools.partial(mix_kernel, streams),
-        out_shape=jax.ShapeDtypeStruct((rows, cols), jnp.bfloat16),
-        in_specs=[VMEM] * (len(pieces) + 1),
+        functools.partial(mix_kernel, stream, streams, len(more)),
+        out_shape=jax.ShapeDtypeStruct((rows, cols), kind),
+        in_specs=[VMEM] * (len(pieces) + 1 + len(more)),
         out_specs=VMEM,
         cost_estimate=pl.CostEstimate(
-            flops=2 * rows * depth * cols,
-            bytes_accessed=2 * (rows * depth + depth * cols + rows * cols),
+            flops=2 * rows * width * len(pieces) * cols,
+            bytes_accessed=2 * width * len(pieces) * (rows + cols) + 4 * rows * cols,
             transcendentals=0,
         ),
         compiler_params=pltpu.CompilerParams(vmem_limit_bytes=16 << 20),
         name="mix",
-    )(*pieces, near(weight))
+    )(*pieces, near(weight), *more)
+
+
+def quotient(value, divisor, limit):
+    shift = 18
+    factor = (1 << shift) // divisor + 1
+    assert all(v * factor >> shift == v // divisor for v in range(limit))
+    assert limit * factor < 1 << 31
+    return lax.shift_right_logical(value * factor, shift)
 
 
 def index_kernel(lines, plane, own_blocks, chosen_ref, slots_ref, *refs):
     asks = refs[: plane - 1]
     count, seen, rows = refs[plane - 1 :]
     size = own_blocks * TOPB
+    devices = lines * plane
     device = lax.axis_index("kv")
-    line = lax.div(device, plane)
+    line = quotient(device, plane, devices)
     place = device - line * plane
     side_base = own_blocks * lines
 
@@ -154,38 +233,38 @@
             ref[i] = 0
             return carry
 
-        lax.fori_loop(0, ref.shape[0], one, 0)
+        lax.fori_loop(0, ref.shape[0], one, 0, unroll=8)
 
     clear(count)
     clear(seen)
     clear(rows)
 
-    def entry(e, carry):
-        at = lax.div(e, TOPB)
-        block = chosen_ref[at, e - at * TOPB]
-        holder = lax.div(block, own_blocks)
-        within = block - holder * own_blocks
-        remote = holder != device
-        spot = count[holder]
-        count[holder] = spot + jnp.where(remote, 1, 0)
-        spot = jnp.minimum(spot, CAP - 1)
-        from_line = lax.div(holder, plane)
-        from_place = holder - from_line * plane
-        if plane & (plane - 1) == 0:
-            shift = jnp.bitwise_xor(from_place, place)
-        else:
-            shift = lax.rem(from_place + place, plane)
-        gap = jnp.maximum(line - from_line, 0)
-        rows[(shift * lines + from_line) * CAP + spot] = within
-        straight = gap * own_blocks + within
-        across = side_base + (gap * (plane - 1) + shift - 1) * CAP + spot
-        slots_ref[e] = jnp.where(from_place == place, straight, across)
-        row = at + 1
-        slots_ref[size + e] = jnp.where(seen[block] == row, 1, 0)
-        seen[block] = row
+    def row(b, carry):
+        for s in range(TOPB):
+            e = b * TOPB + s
+            block = chosen_ref[b, s]
+            holder = quotient(block, own_blocks, devices * own_blocks)
+            within = block - holder * own_blocks
+            remote = holder != device
+            spot = count[holder]
+            count[holder] = spot + jnp.where(remote, 1, 0)
+            spot = jnp.minimum(spot, CAP - 1)
+            from_line = quotient(holder, plane, devices)
+            from_place = holder - from_line * plane
+            if plane & (plane - 1) == 0:
+                shift = jnp.bitwise_xor(from_place, place)
+            else:
+                shift = lax.rem(from_place + place, plane)
+            gap = jnp.maximum(line - from_line, 0)
+            rows[(shift * lines + from_line) * CAP + spot] = within
+            straight = gap * own_blocks + within
+            across = side_base + (gap * (plane - 1) + shift - 1) * CAP + spot
+            slots_ref[e] = jnp.where(from_place == place, straight, across)
+            slots_ref[size + e] = jnp.where(seen[block] == b + 1, 1, 0)
+            seen[block] = b + 1
         return carry
 
-    lax.fori_loop(0, size, entry, 0)
+    lax.fori_loop(0, own_blocks, row, 0)
     for shift, ask in enumerate(asks, 1):
         for i in range(lines * CAP):
             ask[i] = rows[shift * lines * CAP + i]
@@ -353,8 +432,16 @@
     heads = key_heads // streams
     cols = heads * HD
 
-    section = spread(tokens)
-    up = [(d, (d + plane) % devices) for d in range(devices)]
+    tokens_here, part, rest = front(tokens, key_weight, value_weight, cols)
+    section = [tokens_here] + spread(tokens)[1:]
+
+    def up(hop):
+        pairs = []
+        for l in range(lines):
+            to = l if l < hop else l + 1 if l < lines - 1 else hop
+            pairs += [(l * plane + c, to * plane + c) for c in range(plane)]
+        return pairs
+
     swaps = [
         [
             (l * plane + c, l * plane + partner(c, shift, plane))
@@ -367,14 +454,18 @@
     own = []
     line_parts = [[] for _ in range(streams)]
     for t in range(streams):
-        if t > 0:
-            section, _ = lax.optimization_barrier((section, own[-1]))
-        pair = project(section, [key_weight, value_weight], t * cols, cols)
+        if t == 1:
+            section, _ = lax.optimization_barrier((section, slots))
+        if t == 0:
+            pair = join(section[1:], part, rest)
+        else:
+            pair = project(section, [key_weight, value_weight], t * cols, cols)
         own.append(pair.reshape(own_blocks, BLK, 2 * cols))
         if lines > 1:
-            line_parts[t].append(send(own[t], up))
-    chosen, _ = lax.optimization_barrier((chosen, own[-1]))
-    slots, asks = index(chosen, lines, plane, own_blocks)
+            line_parts[t].append(send(own[t], up(0)))
+        if t == 0:
+            chosen, _ = lax.optimization_barrier((chosen, own[0]))
+            slots, asks = index(chosen, lines, plane, own_blocks)
     asked = []
     for shift in range(1, plane):
         asked.append(send(asks[shift - 1], swaps[shift - 1]))
@@ -402,18 +493,17 @@
             held = [line_parts[t][-1] for t in range(streams)]
         if step + 1 < lines - 1:
             for t in range(streams):
-                line_parts[t].append(send(held[t], up))
+                line_parts[t].append(send(held[t], up(step + 1)))
         if queries is None:
             queries = project(section, [query_weight], 0, query_weight.shape[1])
     share = group * cols
-    done = []
+    total = None
     for t in range(streams):
         pools = [own[t]] + line_parts[t] + side_parts[t]
         shifts = (0,) * (1 + len(line_parts[t])) + tuple(offsets[t])
-        done.append(attend(queries, slots, pools, shifts, heads, group, t * share))
-    done = lax.optimization_barrier(done)
-    pieces = [piece for part in done for piece in spread(part)]
-    return mix(pieces, out_weight, streams)
+        done = attend(queries, slots, pools, shifts, heads, group, t * share)
+        total = mix(spread(done), out_weight, t, streams, total)
+    return total
 
 
 def solution(mesh):

time: 102 us -> 93.7 us (0.919)
  the two profiles are of different devices: /device:TPU:15 before, /device:TPU:9 now
where the time goes in v2:
time: 93.7 us; the launch traced here: 93.4 us
  starting transfers between devices  43.1 us (46%)
  Pallas kernels  31.2 us (33%)
  waiting for transfers between devices  18.8 us (20%)
    ppermute x27, starting transfers between devices, send(): return lax.ppermute(part, 'kv', pairs)  30.1 us
    ppermute x27, waiting for transfers between devices, send(): return lax.ppermute(part, 'kv', pairs)  18.1 us
    ppermute x3, starting transfers between devices, spread(): pieces.append(lax.ppermute(part, 'tp', pairs))  12.9 us
    pallas_call x2, Pallas kernels, attend(): pl.pallas_call(functools.partial(attend_kernel, sizes, offsets, heads, gr...  9.1 us
    pallas_call x2, Pallas kernels, project(): pl.pallas_call(functools.partial(project_kernel, count, kinds, first, col...  7.36 us
    pallas_call x6, Pallas kernels, pick(): pl.pallas_call(functools.partial(pick_kernel, targets, len(parts), step),...  6.22 us
    pallas_call x2, Pallas kernels, mix(): pl.pallas_call(functools.partial(mix_kernel, stream, streams, len(more)),...  2.85 us
    pallas_call x1, Pallas kernels, index(): pl.pallas_call(functools.partial(index_kernel, lines, plane, own_blocks),...  2.7 us
  transfers between devices with their start and end apart: 30, of which 12 were waited for; matrix products, arithmetic and copies ran while one was open for 0% of the time, Pallas kernels for 31%

profile of v2, /device:TPU:9, one launch (start us, length us, event | category | flops | bytes accessed | tf_op | source)
XLA Modules:
  0.0 93.4 jit_solution(3997083608601548737)
XLA Ops:
  0.0 0.7 collective-permute-start
  0.7 2.4 %front.1 = (bf16[384,1024]{1,0:T(8,128)(2,1)S(1)}, f32[384,512]{1,0:T(8,128)S(1)}, bf16[1,2,1024,256]{3,2,1,0:T(8,128)(2,1)S(1)}) custom-call(bf16[384,1024]{1,0:T(8,128)(2,1)} %own_in.1, bf16[2048,512]{1,0:T(8,128)(2,1)} %refs_2_.5, bf16[2048,512]{1,0:T(8,128)(2,1)} %refs_3_.1), custom_call_target="tpu_custom_call" | custom-call | tf_op jit(solution)/shard_map/front/pallas_call | solution.py:132
  3.1 0.6 join.1
  3.7 1.4 %collective-permute-start.1 = (bf16[6,64,512]{2,1,0:T(8,128)(2,1)S(1)}, bf16[6,64,512]{2,1,0:T(8,128)(2,1)S(1)}, u32[]{:S(2)}, u32[]{:S(2)}) collective-permute-start(bf16[6,64,512]{2,1,0:T(8,128)(2,1)S(1)} %bitcast.5), channel_id=1, source_target_pairs={{0,8},{2,10},{4,12},{6,14},{8,16},{10,18},{12,20},{14,22},{16,24},... | collective-permute-start | bytes 1179656 | tf_op jit(solution)/shard_map/ppermute | solution.py:41
  5.1 2.7 %index.1 = (s32[192]{0:T(256)S(1)}, s32[8]{0:T(128)S(1)}, s32[8]{0:T(128)S(1)}, s32[8]{0:T(128)S(1)}) custom-call(s32[6,16]{1,0:T(8,128)S(1)} %copy-done.1), custom_call_target="tpu_custom_call" | custom-call | tf_op jit(solution)/shard_map/index/pallas_call | solution.py:276
  7.8 3.3 %project.3 = bf16[384,512]{1,0:T(8,128)(2,1)S(1)} custom-call(bf16[384,1024]{1,0:T(8,128)(2,1)S(1)} %get-tuple-element.40.refs_0_, bf16[384,1024]{1,0:T(8,128)(2,1)S(1)} %collective-permute-done.refs_0_.refs_1_, bf16[2048,512]{1,0:T(8,128)(2,1)} %refs_2_.5, bf16[2048,512]{1,0:T(8,128)(2,1)} %refs_3_.1), custom_call_target="tpu_custom_call" | custom-call | flops 805306368 | bytes 3670016 | tf_op jit(solution)/shard_map/project/pallas_call | solution.py:85
  11.1 1.3 %collective-permute-start.4 = (bf16[6,64,512]{2,1,0:T(8,128)(2,1)S(1)}, bf16[6,64,512]{2,1,0:T(8,128)(2,1)S(1)}, u32[]{:S(2)}, u32[]{:S(2)}) collective-permute-start(bf16[6,64,512]{2,1,0:T(8,128)(2,1)S(1)} %bitcast.2), channel_id=1, source_target_pairs={{0,8},{2,10},{4,12},{6,14},{8,16},{10,18},{12,20},{14,22},{16,24},... | collective-permute-start | bytes 1179656 | tf_op jit(solution)/shard_map/ppermute | solution.py:41
  12.5 1.9 %collective-permute-done.1.refs_3_ = bf16[6,64,512]{2,1,0:T(8,128)(2,1)S(1)} collective-permute-done((bf16[6,64,512]{2,1,0:T(8,128)(2,1)S(1)}, bf16[6,64,512]{2,1,0:T(8,128)(2,1)S(1)}, u32[]{:S(2)}, u32[]{:S(2)}) %collective-permute-start.1) | collective-permute-done | bytes 393248 | tf_op jit(solution)/shard_map/ppermute | solution.py:41
  14.4 3.2 %collective-permute-start.2 = (bf16[6,64,512]{2,1,0:T(8,128)(2,1)S(1)}, bf16[6,64,512]{2,1,0:T(8,128)(2,1)S(1)}, u32[]{:S(2)}, u32[]{:S(2)}) collective-permute-start(bf16[6,64,512]{2,1,0:T(8,128)(2,1)S(1)} %collective-permute-done.1.refs_3_), channel_id=1, source_target_pairs={{0,0},{2,2},{4,4},{6,6},{8,16},{10,18},{12,20},{14,22},{16,24},{18... | collective-permute-start | bytes 1179656 | tf_op jit(solution)/shard_map/ppermute | solution.py:41
  17.6 5.2 %collective-permute-done.4.refs_4_.refs_3_ = bf16[6,64,512]{2,1,0:T(8,128)(2,1)S(1)} collective-permute-done((bf16[6,64,512]{2,1,0:T(8,128)(2,1)S(1)}, bf16[6,64,512]{2,1,0:T(8,128)(2,1)S(1)}, u32[]{:S(2)}, u32[]{:S(2)}) %collective-permute-start.4) | collective-permute-done | bytes 393248 | tf_op jit(solution)/shard_map/ppermute | solution.py:41
  22.9 3.2 %collective-permute-start.5 = (bf16[6,64,512]{2,1,0:T(8,128)(2,1)S(1)}, bf16[6,64,512]{2,1,0:T(8,128)(2,1)S(1)}, u32[]{:S(2)}, u32[]{:S(2)}) collective-permute-start(bf16[6,64,512]{2,1,0:T(8,128)(2,1)S(1)} %collective-permute-done.4.refs_4_.refs_3_), channel_id=1, source_target_pairs={{0,0},{2,2},{4,4},{6,6},{8,16},{10,18},{12,20},{14,22},{16,24},{18... | collective-permute-start | bytes 1179656 | tf_op jit(solution)/shard_map/ppermute | solution.py:41
  26.1 1.3 %collective-permute-start.7 = (s32[8]{0:T(128)S(1)}, s32[8]{0:T(128)S(1)}, u32[]{:S(2)}, u32[]{:S(2)}) collective-permute-start(s32[8]{0:T(128)S(1)} %get-tuple-element.43), channel_id=1, source_target_pairs={{0,2},{2,0},{4,6},{6,4},{8,10},{10,8},{12,14},{14,12},{16,18},{18,... | collective-permute-start | bytes 104 | tf_op jit(solution)/shard_map/ppermute | solution.py:41
  27.3 1.2 %collective-permute-start.8 = (s32[8]{0:T(128)S(1)}, s32[8]{0:T(128)S(1)}, u32[]{:S(2)}, u32[]{:S(2)}) collective-permute-start(s32[8]{0:T(128)S(1)} %get-tuple-element.44), channel_id=1, source_target_pairs={{0,4},{2,6},{4,0},{6,2},{8,12},{10,14},{12,8},{14,10},{16,20},{18,... | collective-permute-start | bytes 104 | tf_op jit(solution)/shard_map/ppermute | solution.py:41
  28.8 1.2 %collective-permute-done.8.refs_1_ = s32[8]{0:T(128)S(1)} collective-permute-done((s32[8]{0:T(128)S(1)}, s32[8]{0:T(128)S(1)}, u32[]{:S(2)}, u32[]{:S(2)}) %collective-permute-start.8) | collective-permute-done | bytes 64 | tf_op jit(solution)/shard_map/ppermute | solution.py:41
  30.0 2.1 %collective-permute-done.9.refs_2_ = s32[8]{0:T(128)S(1)} collective-permute-done((s32[8]{0:T(128)S(1)}, s32[8]{0:T(128)S(1)}, u32[]{:S(2)}, u32[]{:S(2)}) %collective-permute-start.9) | collective-permute-done | bytes 64 | tf_op jit(solution)/shard_map/ppermute | solution.py:41
  32.2 0.8 pick.6
  33.0 0.3 collective-permute-start.10
  33.3 0.7 collective-permute-start.3
  34.3 2.2 %collective-permute-start.12 = (bf16[2,64,1024]{2,1,0:T(8,128)(2,1)S(1)}, bf16[2,64,1024]{2,1,0:T(8,128)(2,1)S(1)}, u32[]{:S(2)}, u32[]{:S(2)}) collective-permute-start(bf16[2,64,1024]{2,1,0:T(8,128)(2,1)S(1)} %get-tuple-element.48), channel_id=1, source_target_pairs={{0,6},{2,4},{4,2},{6,0},{8,14},{10,12},{12,10},{14,8},{16,22},{18,... | collective-permute-start | bytes 786440 | tf_op jit(solution)/shard_map/ppermute | solution.py:41
  36.5 0.8 pick.7
  37.3 1.3 %collective-permute-done.10.refs_6_ = bf16[2,64,1024]{2,1,0:T(8,128)(2,1)S(1)} collective-permute-done((bf16[2,64,1024]{2,1,0:T(8,128)(2,1)S(1)}, bf16[2,64,1024]{2,1,0:T(8,128)(2,1)S(1)}, u32[]{:S(2)}, u32[]{:S(2)}) %collective-permute-start.10) | collective-permute-done | bytes 262176 | tf_op jit(solution)/shard_map/ppermute | solution.py:41
  38.9 2.0 %collective-permute-done.5.refs_3_.refs_4_ = bf16[6,64,512]{2,1,0:T(8,128)(2,1)S(1)} collective-permute-done((bf16[6,64,512]{2,1,0:T(8,128)(2,1)S(1)}, bf16[6,64,512]{2,1,0:T(8,128)(2,1)S(1)}, u32[]{:S(2)}, u32[]{:S(2)}) %collective-permute-start.5) | collective-permute-done | bytes 393248 | tf_op jit(solution)/shard_map/ppermute | solution.py:41
  40.8 0.9 collective-permute-start.6
  41.7 0.5 collective-permute-done.11.refs_7_
  42.2 0.6 collective-permute-start.14
  42.8 0.4 collective-permute-done.12.refs_8_
  43.2 2.0 %collective-permute-start.15 = (bf16[2,64,1024]{2,1,0:T(8,128)(2,1)S(1)}, bf16[2,64,1024]{2,1,0:T(8,128)(2,1)S(1)}, u32[]{:S(2)}, u32[]{:S(2)}) collective-permute-start(bf16[2,64,1024]{2,1,0:T(8,128)(2,1)S(1)} %get-tuple-element.51), channel_id=1, source_target_pairs={{0,6},{2,4},{4,2},{6,0},{8,14},{10,12},{12,10},{14,8},{16,22},{18,... | collective-permute-start | bytes 786440 | tf_op jit(solution)/shard_map/ppermute | solution.py:41
  45.1 1.1 %pick.10 = (bf16[2,64,512]{2,1,0:T(8,128)(2,1)S(1)}, bf16[2,64,512]{2,1,0:T(8,128)(2,1)S(1)}, bf16[2,64,512]{2,1,0:T(8,128)(2,1)S(1)}) custom-call(s32[8]{0:T(128)S(1)} %collective-permute-done.7.refs_0_, s32[8]{0:T(128)S(1)} %collective-permute-done.8.refs_1_, s32[8]{0:T(128)S(1)} %collective-permute-done.9.refs_2_, ...), custom_call_target="tpu_custom_call" | custom-call | tf_op jit(solution)/shard_map/pick/pallas_call | solution.py:322
  46.3 2.9 %collective-permute-done.13.refs_9_ = bf16[2,64,1024]{2,1,0:T(8,128)(2,1)S(1)} collective-permute-done((bf16[2,64,1024]{2,1,0:T(8,128)(2,1)S(1)}, bf16[2,64,1024]{2,1,0:T(8,128)(2,1)S(1)}, u32[]{:S(2)}, u32[]{:S(2)}) %collective-permute-start.13) | collective-permute-done | bytes 262176 | tf_op jit(solution)/shard_map/ppermute | solution.py:41
  49.1 0.9 collective-permute-start.23
  50.3 4.0 %project.2.refs_1_ = bf16[384,1024]{1,0:T(8,128)(2,1)S(1)} custom-call(bf16[384,1024]{1,0:T(8,128)(2,1)S(1)} %get-tuple-element.40.refs_0_, bf16[384,1024]{1,0:T(8,128)(2,1)S(1)} %collective-permute-done.refs_0_.refs_1_, bf16[2048,1024]{1,0:T(8,128)(2,1)} %refs_2_.4), custom_call_target="tpu_custom_call" | custom-call | flops 1610612736 | bytes 5767168 | tf_op jit(solution)/shard_map/project/pallas_call | solution.py:85
  54.3 1.1 %pick.8 = (bf16[2,64,512]{2,1,0:T(8,128)(2,1)S(1)}, bf16[2,64,512]{2,1,0:T(8,128)(2,1)S(1)}, bf16[2,64,512]{2,1,0:T(8,128)(2,1)S(1)}) custom-call(s32[8]{0:T(128)S(1)} %collective-permute-done.7.refs_0_, s32[8]{0:T(128)S(1)} %collective-permute-done.8.refs_1_, s32[8]{0:T(128)S(1)} %collective-permute-done.9.refs_2_, ...), custom_call_target="tpu_custom_call" | custom-call | tf_op jit(solution)/shard_map/pick/pallas_call | solution.py:322
  55.5 1.1 %pick.11 = (bf16[2,64,512]{2,1,0:T(8,128)(2,1)S(1)}, bf16[2,64,512]{2,1,0:T(8,128)(2,1)S(1)}, bf16[2,64,512]{2,1,0:T(8,128)(2,1)S(1)}) custom-call(s32[8]{0:T(128)S(1)} %collective-permute-done.7.refs_0_, s32[8]{0:T(128)S(1)} %collective-permute-done.8.refs_1_, s32[8]{0:T(128)S(1)} %collective-permute-done.9.refs_2_, ...), custom_call_target="tpu_custom_call" | custom-call | tf_op jit(solution)/shard_map/pick/pallas_call | solution.py:322
  56.6 1.6 %collective-permute-start.25 = (bf16[2,64,512]{2,1,0:T(8,128)(2,1)S(1)}, bf16[2,64,512]{2,1,0:T(8,128)(2,1)S(1)}, u32[]{:S(2)}, u32[]{:S(2)}) collective-permute-start(bf16[2,64,512]{2,1,0:T(8,128)(2,1)S(1)} %get-tuple-element.60), channel_id=1, source_target_pairs={{0,6},{2,4},{4,2},{6,0},{8,14},{10,12},{12,10},{14,8},{16,22},{18,... | collective-permute-start | bytes 393224 | tf_op jit(solution)/shard_map/ppermute | solution.py:41
  58.2 0.9 collective-permute-start.16
  59.1 0.5 collective-permute-start.26
  59.7 0.6 collective-permute-done.24.refs_13_
  60.2 2.8 %collective-permute-start.28 = (bf16[2,64,512]{2,1,0:T(8,128)(2,1)S(1)}, bf16[2,64,512]{2,1,0:T(8,128)(2,1)S(1)}, u32[]{:S(2)}, u32[]{:S(2)}) collective-permute-start(bf16[2,64,512]{2,1,0:T(8,128)(2,1)S(1)} %get-tuple-element.64), channel_id=1, source_target_pairs={{0,6},{2,4},{4,2},{6,0},{8,14},{10,12},{12,10},{14,8},{16,22},{18,... | collective-permute-start | bytes 393224 | tf_op jit(solution)/shard_map/ppermute | solution.py:41
  63.0 1.1 %pick.9 = (bf16[2,64,512]{2,1,0:T(8,128)(2,1)S(1)}, bf16[2,64,512]{2,1,0:T(8,128)(2,1)S(1)}, bf16[2,64,512]{2,1,0:T(8,128)(2,1)S(1)}) custom-call(s32[8]{0:T(128)S(1)} %collective-permute-done.7.refs_0_, s32[8]{0:T(128)S(1)} %collective-permute-done.8.refs_1_, s32[8]{0:T(128)S(1)} %collective-permute-done.9.refs_2_, ...), custom_call_target="tpu_custom_call" | custom-call | tf_op jit(solution)/shard_map/pick/pallas_call | solution.py:322
  64.3 1.0 %collective-permute-start.18 = (bf16[2,64,512]{2,1,0:T(8,128)(2,1)S(1)}, bf16[2,64,512]{2,1,0:T(8,128)(2,1)S(1)}, u32[]{:S(2)}, u32[]{:S(2)}) collective-permute-start(bf16[2,64,512]{2,1,0:T(8,128)(2,1)S(1)} %get-tuple-element.54), channel_id=1, source_target_pairs={{0,6},{2,4},{4,2},{6,0},{8,14},{10,12},{12,10},{14,8},{16,22},{18,... | collective-permute-start | bytes 393224 | tf_op jit(solution)/shard_map/ppermute | solution.py:41
  65.3 1.6 %collective-permute-start.19 = (bf16[2,64,512]{2,1,0:T(8,128)(2,1)S(1)}, bf16[2,64,512]{2,1,0:T(8,128)(2,1)S(1)}, u32[]{:S(2)}, u32[]{:S(2)}) collective-permute-start(bf16[2,64,512]{2,1,0:T(8,128)(2,1)S(1)} %get-tuple-element.55), channel_id=1, source_target_pairs={{0,2},{2,0},{4,6},{6,4},{8,10},{10,8},{12,14},{14,12},{16,18},{18,... | collective-permute-start | bytes 393224 | tf_op jit(solution)/shard_map/ppermute | solution.py:41
  67.0 1.4 %collective-permute-start.21 = (bf16[2,64,512]{2,1,0:T(8,128)(2,1)S(1)}, bf16[2,64,512]{2,1,0:T(8,128)(2,1)S(1)}, u32[]{:S(2)}, u32[]{:S(2)}) collective-permute-start(bf16[2,64,512]{2,1,0:T(8,128)(2,1)S(1)} %get-tuple-element.57), channel_id=1, source_target_pairs={{0,6},{2,4},{4,2},{6,0},{8,14},{10,12},{12,10},{14,8},{16,22},{18,... | collective-permute-start | bytes 393224 | tf_op jit(solution)/shard_map/ppermute | solution.py:41
  68.4 4.5 %attend.3.refs_0_ = bf16[384,512]{1,0:T(8,128)(2,1)S(1)} custom-call(s32[192]{0:T(256)S(1)} %get-tuple-element.38.refs_0_, bf16[384,1024]{1,0:T(8,128)(2,1)S(1)} %project.2.refs_1_, bf16[6,64,512]{2,1,0:T(8,128)(2,1)S(1)} %bitcast.7, bf16[6,64,512]{2,1,0:T(8,128)(2,1)S(1)} %collective-permute-done.1.refs_3_, ...), custom_call_target="tpu_custom_call" | custom-call | flops 805306368 | bytes 3932160 | tf_op jit(solution)/shard_map/attend/pallas_call | solution.py:404
  73.0 12.2 %collective-permute-start.29 = (bf16[384,512]{1,0:T(8,128)(2,1)S(1)}, bf16[384,512]{1,0:T(8,128)(2,1)S(1)}, u32[]{:S(2)}, u32[]{:S(2)}) collective-permute-start(bf16[384,512]{1,0:T(8,128)(2,1)S(1)} %attend.3.refs_0_), channel_id=1, source_target_pairs={{0,1},{1,0},{2,3},{3,2},{4,5},{5,4},{6,7},{7,6},{8,9},{9,8},{10,11... | collective-permute-start | bytes 1179656 | tf_op jit(solution)/shard_map/ppermute | solution.py:49
  85.2 4.6 %attend.2.refs_0_ = bf16[384,512]{1,0:T(8,128)(2,1)S(1)} custom-call(s32[192]{0:T(256)S(1)} %get-tuple-element.38.refs_0_, bf16[384,1024]{1,0:T(8,128)(2,1)S(1)} %project.2.refs_1_, bf16[6,64,512]{2,1,0:T(8,128)(2,1)S(1)} %bitcast.4, bf16[6,64,512]{2,1,0:T(8,128)(2,1)S(1)} %collective-permute-done.4.refs_4_.refs_3_, ...), custom_call_target="tpu_custom_call" | custom-call | flops 805306368 | bytes 3932160 | tf_op jit(solution)/shard_map/attend/pallas_call | solution.py:404
  89.8 1.0 %mix.2.refs_3_ = f32[384,1024]{1,0:T(8,128)S(1)} custom-call(bf16[384,512]{1,0:T(8,128)(2,1)S(1)} %attend.3.refs_0_, bf16[384,512]{1,0:T(8,128)(2,1)S(1)} %collective-permute-done.29.refs_1_, bf16[2048,1024]{1,0:T(8,128)(2,1)S(1)} %copy-done), custom_call_target="tpu_custom_call" | custom-call | flops 805306368 | bytes 4456448 | tf_op jit(solution)/shard_map/mix/pallas_call | solution.py:198
  90.8 0.7 collective-permute-done.22.refs_1_
  91.5 1.9 %mix.3 = bf16[384,1024]{1,0:T(8,128)(2,1)} custom-call(bf16[384,512]{1,0:T(8,128)(2,1)S(1)} %attend.2.refs_0_, bf16[384,512]{1,0:T(8,128)(2,1)S(1)} %collective-permute-done.22.refs_1_, bf16[2048,1024]{1,0:T(8,128)(2,1)S(1)} %copy-done, f32[384,1024]{1,0:T(8,128)S(1)} %mix.2.refs_3_), custom_call_target="tpu_custom_call" | custom-call | flops 805306368 | bytes 4456448 | tf_op jit(solution)/shard_map/mix/pallas_call | solution.py:198
  (31 shorter events, 1.4 us)
Async XLA Ops:
  0.0 3.1 %collective-permute-start = (bf16[384,1024]{1,0:T(8,128)(2,1)}, bf16[384,1024]{1,0:T(8,128)(2,1)S(1)}, u32[]{:S(2)}, u32[]{:S(2)}) collective-permute-start(bf16[384,1024]{1,0:T(8,128)(2,1)} %own_in.1), channel_id=1, source_target_pairs={{0,1},{1,0},{2,3},{3,2},{4,5},{5,4},{6,7},{7,6},{8,9},{9,8},{10,11... | collective-permute-start | bytes 2359304 | tf_op jit(solution)/shard_map/ppermute | solution.py:49
  3.1 2.0 %copy-start.1 = (s32[6,16]{1,0:T(8,128)S(1)}, s32[6,16]{1,0:T(8,128)}, u32[]{:S(2)}) copy-start(s32[6,16]{1,0:T(8,128)} %chosen_ref) | copy-start | bytes 1156
  3.7 10.7 %collective-permute-start.1 = (bf16[6,64,512]{2,1,0:T(8,128)(2,1)S(1)}, bf16[6,64,512]{2,1,0:T(8,128)(2,1)S(1)}, u32[]{:S(2)}, u32[]{:S(2)}) collective-permute-start(bf16[6,64,512]{2,1,0:T(8,128)(2,1)S(1)} %bitcast.5), channel_id=1, source_target_pairs={{0,8},{2,10},{4,12},{6,14},{8,16},{10,18},{12,20},{14,22},{16,24},... | collective-permute-start | bytes 1179656 | tf_op jit(solution)/shard_map/ppermute | solution.py:41
  11.1 11.7 %collective-permute-start.4 = (bf16[6,64,512]{2,1,0:T(8,128)(2,1)S(1)}, bf16[6,64,512]{2,1,0:T(8,128)(2,1)S(1)}, u32[]{:S(2)}, u32[]{:S(2)}) collective-permute-start(bf16[6,64,512]{2,1,0:T(8,128)(2,1)S(1)} %bitcast.2), channel_id=1, source_target_pairs={{0,8},{2,10},{4,12},{6,14},{8,16},{10,18},{12,20},{14,22},{16,24},... | collective-permute-start | bytes 1179656 | tf_op jit(solution)/shard_map/ppermute | solution.py:41
  14.4 18.9 %collective-permute-start.2 = (bf16[6,64,512]{2,1,0:T(8,128)(2,1)S(1)}, bf16[6,64,512]{2,1,0:T(8,128)(2,1)S(1)}, u32[]{:S(2)}, u32[]{:S(2)}) collective-permute-start(bf16[6,64,512]{2,1,0:T(8,128)(2,1)S(1)} %collective-permute-done.1.refs_3_), channel_id=1, source_target_pairs={{0,0},{2,2},{4,4},{6,6},{8,16},{10,18},{12,20},{14,22},{16,24},{18... | collective-permute-start | bytes 1179656 | tf_op jit(solution)/shard_map/ppermute | solution.py:41
  22.9 18.0 %collective-permute-start.5 = (bf16[6,64,512]{2,1,0:T(8,128)(2,1)S(1)}, bf16[6,64,512]{2,1,0:T(8,128)(2,1)S(1)}, u32[]{:S(2)}, u32[]{:S(2)}) collective-permute-start(bf16[6,64,512]{2,1,0:T(8,128)(2,1)S(1)} %collective-permute-done.4.refs_4_.refs_3_), channel_id=1, source_target_pairs={{0,0},{2,2},{4,4},{6,6},{8,16},{10,18},{12,20},{14,22},{16,24},{18... | collective-permute-start | bytes 1179656 | tf_op jit(solution)/shard_map/ppermute | solution.py:41
  26.1 2.8 %collective-permute-start.7 = (s32[8]{0:T(128)S(1)}, s32[8]{0:T(128)S(1)}, u32[]{:S(2)}, u32[]{:S(2)}) collective-permute-start(s32[8]{0:T(128)S(1)} %get-tuple-element.43), channel_id=1, source_target_pairs={{0,2},{2,0},{4,6},{6,4},{8,10},{10,8},{12,14},{14,12},{16,18},{18,... | collective-permute-start | bytes 104 | tf_op jit(solution)/shard_map/ppermute | solution.py:41
  27.3 2.7 %collective-permute-start.8 = (s32[8]{0:T(128)S(1)}, s32[8]{0:T(128)S(1)}, u32[]{:S(2)}, u32[]{:S(2)}) collective-permute-start(s32[8]{0:T(128)S(1)} %get-tuple-element.44), channel_id=1, source_target_pairs={{0,4},{2,6},{4,0},{6,2},{8,12},{10,14},{12,8},{14,10},{16,20},{18,... | collective-permute-start | bytes 104 | tf_op jit(solution)/shard_map/ppermute | solution.py:41
  28.6 3.6 %collective-permute-start.9 = (s32[8]{0:T(128)S(1)}, s32[8]{0:T(128)S(1)}, u32[]{:S(2)}, u32[]{:S(2)}) collective-permute-start(s32[8]{0:T(128)S(1)} %get-tuple-element.45), channel_id=1, source_target_pairs={{0,6},{2,4},{4,2},{6,0},{8,14},{10,12},{12,10},{14,8},{16,22},{18,... | collective-permute-start | bytes 104 | tf_op jit(solution)/shard_map/ppermute | solution.py:41
  33.0 5.6 %collective-permute-start.10 = (bf16[2,64,1024]{2,1,0:T(8,128)(2,1)S(1)}, bf16[2,64,1024]{2,1,0:T(8,128)(2,1)S(1)}, u32[]{:S(2)}, u32[]{:S(2)}) collective-permute-start(bf16[2,64,1024]{2,1,0:T(8,128)(2,1)S(1)} %get-tuple-element.46), channel_id=1, source_target_pairs={{0,2},{2,0},{4,6},{6,4},{8,10},{10,8},{12,14},{14,12},{16,18},{18,... | collective-permute-start | bytes 786440 | tf_op jit(solution)/shard_map/ppermute | solution.py:41
  33.3 16.7 %collective-permute-start.3 = (bf16[6,64,512]{2,1,0:T(8,128)(2,1)S(1)}, bf16[6,64,512]{2,1,0:T(8,128)(2,1)S(1)}, u32[]{:S(2)}, u32[]{:S(2)}) collective-permute-start(bf16[6,64,512]{2,1,0:T(8,128)(2,1)S(1)} %collective-permute-done.2.refs_3_.refs_4_), channel_id=1, source_target_pairs={{0,0},{2,2},{4,4},{6,6},{8,8},{10,10},{12,12},{14,14},{16,24},{18,... | collective-permute-start | bytes 1179656 | tf_op jit(solution)/shard_map/ppermute | solution.py:41
  34.0 8.1 %collective-permute-start.11 = (bf16[2,64,1024]{2,1,0:T(8,128)(2,1)S(1)}, bf16[2,64,1024]{2,1,0:T(8,128)(2,1)S(1)}, u32[]{:S(2)}, u32[]{:S(2)}) collective-permute-start(bf16[2,64,1024]{2,1,0:T(8,128)(2,1)S(1)} %get-tuple-element.47), channel_id=1, source_target_pairs={{0,4},{2,6},{4,0},{6,2},{8,12},{10,14},{12,8},{14,10},{16,20},{18,... | collective-permute-start | bytes 786440 | tf_op jit(solution)/shard_map/ppermute | solution.py:41
  34.3 8.8 %collective-permute-start.12 = (bf16[2,64,1024]{2,1,0:T(8,128)(2,1)S(1)}, bf16[2,64,1024]{2,1,0:T(8,128)(2,1)S(1)}, u32[]{:S(2)}, u32[]{:S(2)}) collective-permute-start(bf16[2,64,1024]{2,1,0:T(8,128)(2,1)S(1)} %get-tuple-element.48), channel_id=1, source_target_pairs={{0,6},{2,4},{4,2},{6,0},{8,14},{10,12},{12,10},{14,8},{16,22},{18,... | collective-permute-start | bytes 786440 | tf_op jit(solution)/shard_map/ppermute | solution.py:41
  38.6 10.5 %collective-permute-start.13 = (bf16[2,64,1024]{2,1,0:T(8,128)(2,1)S(1)}, bf16[2,64,1024]{2,1,0:T(8,128)(2,1)S(1)}, u32[]{:S(2)}, u32[]{:S(2)}) collective-permute-start(bf16[2,64,1024]{2,1,0:T(8,128)(2,1)S(1)} %get-tuple-element.49), channel_id=1, source_target_pairs={{0,2},{2,0},{4,6},{6,4},{8,10},{10,8},{12,14},{14,12},{16,18},{18,... | collective-permute-start | bytes 786440 | tf_op jit(solution)/shard_map/ppermute | solution.py:41
  40.8 19.4 %collective-permute-start.6 = (bf16[6,64,512]{2,1,0:T(8,128)(2,1)S(1)}, bf16[6,64,512]{2,1,0:T(8,128)(2,1)S(1)}, u32[]{:S(2)}, u32[]{:S(2)}) collective-permute-start(bf16[6,64,512]{2,1,0:T(8,128)(2,1)S(1)} %collective-permute-done.5.refs_3_.refs_4_), channel_id=1, source_target_pairs={{0,0},{2,2},{4,4},{6,6},{8,8},{10,10},{12,12},{14,14},{16,24},{18,... | collective-permute-start | bytes 1179656 | tf_op jit(solution)/shard_map/ppermute | solution.py:41
  42.2 14.5 %collective-permute-start.14 = (bf16[2,64,1024]{2,1,0:T(8,128)(2,1)S(1)}, bf16[2,64,1024]{2,1,0:T(8,128)(2,1)S(1)}, u32[]{:S(2)}, u32[]{:S(2)}) collective-permute-start(bf16[2,64,1024]{2,1,0:T(8,128)(2,1)S(1)} %get-tuple-element.50), channel_id=1, source_target_pairs={{0,4},{2,6},{4,0},{6,2},{8,12},{10,14},{12,8},{14,10},{16,20},{18,... | collective-permute-start | bytes 786440 | tf_op jit(solution)/shard_map/ppermute | solution.py:41
  43.2 15.0 %collective-permute-start.15 = (bf16[2,64,1024]{2,1,0:T(8,128)(2,1)S(1)}, bf16[2,64,1024]{2,1,0:T(8,128)(2,1)S(1)}, u32[]{:S(2)}, u32[]{:S(2)}) collective-permute-start(bf16[2,64,1024]{2,1,0:T(8,128)(2,1)S(1)} %get-tuple-element.51), channel_id=1, source_target_pairs={{0,6},{2,4},{4,2},{6,0},{8,14},{10,12},{12,10},{14,8},{16,22},{18,... | collective-permute-start | bytes 786440 | tf_op jit(solution)/shard_map/ppermute | solution.py:41
  49.1 10.0 %collective-permute-start.23 = (bf16[2,64,512]{2,1,0:T(8,128)(2,1)S(1)}, bf16[2,64,512]{2,1,0:T(8,128)(2,1)S(1)}, u32[]{:S(2)}, u32[]{:S(2)}) collective-permute-start(bf16[2,64,512]{2,1,0:T(8,128)(2,1)S(1)} %get-tuple-element.58), channel_id=1, source_target_pairs={{0,2},{2,0},{4,6},{6,4},{8,10},{10,8},{12,14},{14,12},{16,18},{18,... | collective-permute-start | bytes 393224 | tf_op jit(solution)/shard_map/ppermute | solution.py:41
  50.1 10.2 %collective-permute-start.24 = (bf16[2,64,512]{2,1,0:T(8,128)(2,1)S(1)}, bf16[2,64,512]{2,1,0:T(8,128)(2,1)S(1)}, u32[]{:S(2)}, u32[]{:S(2)}) collective-permute-start(bf16[2,64,512]{2,1,0:T(8,128)(2,1)S(1)} %get-tuple-element.59), channel_id=1, source_target_pairs={{0,4},{2,6},{4,0},{6,2},{8,12},{10,14},{12,8},{14,10},{16,20},{18,... | collective-permute-start | bytes 393224 | tf_op jit(solution)/shard_map/ppermute | solution.py:41
  56.6 7.5 %collective-permute-start.25 = (bf16[2,64,512]{2,1,0:T(8,128)(2,1)S(1)}, bf16[2,64,512]{2,1,0:T(8,128)(2,1)S(1)}, u32[]{:S(2)}, u32[]{:S(2)}) collective-permute-start(bf16[2,64,512]{2,1,0:T(8,128)(2,1)S(1)} %get-tuple-element.60), channel_id=1, source_target_pairs={{0,6},{2,4},{4,2},{6,0},{8,14},{10,12},{12,10},{14,8},{16,22},{18,... | collective-permute-start | bytes 393224 | tf_op jit(solution)/shard_map/ppermute | solution.py:41
  58.2 6.1 %collective-permute-start.16 = (bf16[2,64,512]{2,1,0:T(8,128)(2,1)S(1)}, bf16[2,64,512]{2,1,0:T(8,128)(2,1)S(1)}, u32[]{:S(2)}, u32[]{:S(2)}) collective-permute-start(bf16[2,64,512]{2,1,0:T(8,128)(2,1)S(1)} %get-tuple-element.52), channel_id=1, source_target_pairs={{0,2},{2,0},{4,6},{6,4},{8,10},{10,8},{12,14},{14,12},{16,18},{18,... | collective-permute-start | bytes 393224 | tf_op jit(solution)/shard_map/ppermute | solution.py:41
  59.1 6.2 %collective-permute-start.26 = (bf16[2,64,512]{2,1,0:T(8,128)(2,1)S(1)}, bf16[2,64,512]{2,1,0:T(8,128)(2,1)S(1)}, u32[]{:S(2)}, u32[]{:S(2)}) collective-permute-start(bf16[2,64,512]{2,1,0:T(8,128)(2,1)S(1)} %get-tuple-element.62), channel_id=1, source_target_pairs={{0,2},{2,0},{4,6},{6,4},{8,10},{10,8},{12,14},{14,12},{16,18},{18,... | collective-permute-start | bytes 393224 | tf_op jit(solution)/shard_map/ppermute | solution.py:41
  60.2 6.7 %collective-permute-start.27 = (bf16[2,64,512]{2,1,0:T(8,128)(2,1)S(1)}, bf16[2,64,512]{2,1,0:T(8,128)(2,1)S(1)}, u32[]{:S(2)}, u32[]{:S(2)}) collective-permute-start(bf16[2,64,512]{2,1,0:T(8,128)(2,1)S(1)} %get-tuple-element.63), channel_id=1, source_target_pairs={{0,4},{2,6},{4,0},{6,2},{8,12},{10,14},{12,8},{14,10},{16,20},{18,... | collective-permute-start | bytes 393224 | tf_op jit(solution)/shard_map/ppermute | solution.py:41
  60.2 6.8 %collective-permute-start.28 = (bf16[2,64,512]{2,1,0:T(8,128)(2,1)S(1)}, bf16[2,64,512]{2,1,0:T(8,128)(2,1)S(1)}, u32[]{:S(2)}, u32[]{:S(2)}) collective-permute-start(bf16[2,64,512]{2,1,0:T(8,128)(2,1)S(1)} %get-tuple-element.64), channel_id=1, source_target_pairs={{0,6},{2,4},{4,2},{6,0},{8,14},{10,12},{12,10},{14,8},{16,22},{18,... | collective-permute-start | bytes 393224 | tf_op jit(solution)/shard_map/ppermute | solution.py:41
  64.2 8.8 %collective-permute-start.17 = (bf16[2,64,512]{2,1,0:T(8,128)(2,1)S(1)}, bf16[2,64,512]{2,1,0:T(8,128)(2,1)S(1)}, u32[]{:S(2)}, u32[]{:S(2)}) collective-permute-start(bf16[2,64,512]{2,1,0:T(8,128)(2,1)S(1)} %get-tuple-element.53), channel_id=1, source_target_pairs={{0,4},{2,6},{4,0},{6,2},{8,12},{10,14},{12,8},{14,10},{16,20},{18,... | collective-permute-start | bytes 393224 | tf_op jit(solution)/shard_map/ppermute | solution.py:41
  64.3 20.9 %collective-permute-start.18 = (bf16[2,64,512]{2,1,0:T(8,128)(2,1)S(1)}, bf16[2,64,512]{2,1,0:T(8,128)(2,1)S(1)}, u32[]{:S(2)}, u32[]{:S(2)}) collective-permute-start(bf16[2,64,512]{2,1,0:T(8,128)(2,1)S(1)} %get-tuple-element.54), channel_id=1, source_target_pairs={{0,6},{2,4},{4,2},{6,0},{8,14},{10,12},{12,10},{14,8},{16,22},{18,... | collective-permute-start | bytes 393224 | tf_op jit(solution)/shard_map/ppermute | solution.py:41
  65.3 19.9 %collective-permute-start.19 = (bf16[2,64,512]{2,1,0:T(8,128)(2,1)S(1)}, bf16[2,64,512]{2,1,0:T(8,128)(2,1)S(1)}, u32[]{:S(2)}, u32[]{:S(2)}) collective-permute-start(bf16[2,64,512]{2,1,0:T(8,128)(2,1)S(1)} %get-tuple-element.55), channel_id=1, source_target_pairs={{0,2},{2,0},{4,6},{6,4},{8,10},{10,8},{12,14},{14,12},{16,18},{18,... | collective-permute-start | bytes 393224 | tf_op jit(solution)/shard_map/ppermute | solution.py:41
  66.9 18.3 %collective-permute-start.20 = (bf16[2,64,512]{2,1,0:T(8,128)(2,1)S(1)}, bf16[2,64,512]{2,1,0:T(8,128)(2,1)S(1)}, u32[]{:S(2)}, u32[]{:S(2)}) collective-permute-start(bf16[2,64,512]{2,1,0:T(8,128)(2,1)S(1)} %get-tuple-element.56), channel_id=1, source_target_pairs={{0,4},{2,6},{4,0},{6,2},{8,12},{10,14},{12,8},{14,10},{16,20},{18,... | collective-permute-start | bytes 393224 | tf_op jit(solution)/shard_map/ppermute | solution.py:41
  67.0 18.2 %collective-permute-start.21 = (bf16[2,64,512]{2,1,0:T(8,128)(2,1)S(1)}, bf16[2,64,512]{2,1,0:T(8,128)(2,1)S(1)}, u32[]{:S(2)}, u32[]{:S(2)}) collective-permute-start(bf16[2,64,512]{2,1,0:T(8,128)(2,1)S(1)} %get-tuple-element.57), channel_id=1, source_target_pairs={{0,6},{2,4},{4,2},{6,0},{8,14},{10,12},{12,10},{14,8},{16,22},{18,... | collective-permute-start | bytes 393224 | tf_op jit(solution)/shard_map/ppermute | solution.py:41
  72.9 16.9 %copy-start = (bf16[2048,1024]{1,0:T(8,128)(2,1)S(1)}, bf16[2048,1024]{1,0:T(8,128)(2,1)}, u32[]{:S(2)}) copy-start(bf16[2048,1024]{1,0:T(8,128)(2,1)} %refs_2_.7) | copy-start | bytes 12582916
  73.0 16.9 %collective-permute-start.29 = (bf16[384,512]{1,0:T(8,128)(2,1)S(1)}, bf16[384,512]{1,0:T(8,128)(2,1)S(1)}, u32[]{:S(2)}, u32[]{:S(2)}) collective-permute-start(bf16[384,512]{1,0:T(8,128)(2,1)S(1)} %attend.3.refs_0_), channel_id=1, source_target_pairs={{0,1},{1,0},{2,3},{3,2},{4,5},{5,4},{6,7},{7,6},{8,9},{9,8},{10,11... | collective-permute-start | bytes 1179656 | tf_op jit(solution)/shard_map/ppermute | solution.py:49
  89.7 1.8 %collective-permute-start.22 = (bf16[384,512]{1,0:T(8,128)(2,1)S(1)}, bf16[384,512]{1,0:T(8,128)(2,1)S(1)}, u32[]{:S(2)}, u32[]{:S(2)}) collective-permute-start(bf16[384,512]{1,0:T(8,128)(2,1)S(1)} %attend.2.refs_0_), channel_id=1, source_target_pairs={{0,1},{1,0},{2,3},{3,2},{4,5},{5,4},{6,7},{7,6},{8,9},{9,8},{10,11... | collective-permute-start | bytes 1179656 | tf_op jit(solution)/shard_map/ppermute | solution.py:49

commit v3 on v2

--- a/solution.py
+++ b/solution.py
@@ -172,32 +172,34 @@
     )(*others, near(part), near(rest))
 
 
-def mix_kernel(stream, streams, more, *refs):
+def mix_kernel(part, streams, more, *refs):
     pieces = refs[: -2 - more]
     weight_ref, out_ref = refs[-2 - more], refs[-1]
-    count = len(pieces)
+    count = lax.axis_size("tp")
     width = pieces[0].shape[1]
     step = min(2 * HD, out_ref.shape[1])
     me = lax.axis_index("tp")
+    starts = [
+        pl.multiple_of((lax.rem(me + s, count) * streams + t) * width, width)
+        for t, s in part
+    ]
     for col in range(0, out_ref.shape[1], step):
         span = slice(col, col + step)
         total = refs[-2][:, span] if more else None
-        for s, piece in enumerate(pieces):
-            at = pl.multiple_of((lax.rem(me + s, count) * streams + stream) * width, width)
+        for at, piece in zip(starts, pieces):
             rows = weight_ref[pl.ds(at, width), span]
             term = jnp.dot(piece[...], rows, preferred_element_type=jnp.float32)
             total = term if total is None else total + term
         out_ref[:, span] = total.astype(out_ref.dtype)
 
 
-def mix(pieces, weight, stream, streams, before):
+def mix(pieces, part, weight, streams, before, last):
     rows, width = pieces[0].shape
     cols = weight.shape[1]
     more = [] if before is None else [before]
-    kind = jnp.bfloat16 if stream == streams - 1 else jnp.float32
     return pl.pallas_call(
-        functools.partial(mix_kernel, stream, streams, len(more)),
-        out_shape=jax.ShapeDtypeStruct((rows, cols), kind),
+        functools.partial(mix_kernel, part, streams, len(more)),
+        out_shape=jax.ShapeDtypeStruct((rows, cols), jnp.bfloat16 if last else jnp.float32),
         in_specs=[VMEM] * (len(pieces) + 1 + len(more)),
         out_specs=VMEM,
         cost_estimate=pl.CostEstimate(
@@ -292,66 +294,42 @@
 def pick_kernel(targets, count, step, *refs):
     tables = refs[:targets]
     parts = refs[targets : targets + count]
-    outs = refs[targets + count : -1]
-    sems = refs[-1]
+    outs = refs[targets + count :]
     line = lax.div(lax.axis_index("kv"), targets + 1)
     row = jnp.maximum(line - step, 0)
-    copies = []
-    for r, out in enumerate(outs):
+    for table, out in zip(tables, outs):
         for i in range(CAP):
-            block = tables[r][row * CAP + i]
+            block = table[row * CAP + i]
             for t, part in enumerate(parts):
                 cols = part.shape[2]
-                copies.append(
-                    pltpu.make_async_copy(
-                        part.at[block],
-                        out.at[i, :, pl.ds(t * cols, cols)],
-                        sems.at[r, i, t],
-                    )
-                )
-    for copy in copies:
-        copy.start()
-    for copy in copies:
-        copy.wait()
+                out[i, :, t * cols : (t + 1) * cols] = part[block]
 
 
 def pick(tables, parts, step):
     targets = len(tables)
     _, rows, cols = parts[0].shape
-    shape = jax.ShapeDtypeStruct((CAP, rows, cols * len(parts)), jnp.bfloat16)
+    shape = pltpu.VMEM((CAP, rows, cols * len(parts)), jnp.bfloat16)
     return pl.pallas_call(
         functools.partial(pick_kernel, targets, len(parts), step),
         out_shape=[shape] * targets,
-        in_specs=[SMEM] * targets + [ANY] * len(parts),
+        in_specs=[SMEM] * targets + [VMEM] * len(parts),
         out_specs=[VMEM] * targets,
-        scratch_shapes=[pltpu.SemaphoreType.DMA((targets, CAP, len(parts)))],
         compiler_params=pltpu.CompilerParams(vmem_limit_bytes=8 << 20),
         name="pick",
-    )(*tables, *parts)
-
-
-def attend_kernel(sizes, offsets, heads, group, first, *refs):
-    n = len(sizes)
+    )(*tables, *[near(part) for part in parts])
+
+
+def attend_kernel(offsets, heads, group, first, *refs):
     slots_ref, q_ref = refs[:2]
-    pool_refs = refs[2 : 2 + n]
-    out_ref, pool, sems = refs[2 + n :]
-    width = heads * HD
-    copies = []
-    for j in range(heads):
-        at = 0
-        for i, size in enumerate(sizes):
+    parts = refs[2:-2]
+    out_ref, pool = refs[-2:]
+    at = 0
+    for part, offset in zip(parts, offsets):
+        for j in range(heads):
             for kind in range(2):
-                col = offsets[i] + kind * width + j * HD
-                copies.append(
-                    pltpu.make_async_copy(
-                        pool_refs[i].at[:, :, pl.ds(col, HD)],
-                        pool.at[j, kind, pl.ds(at, size)],
-                        sems.at[j, kind, i],
-                    )
-                )
-            at += size
-    for copy in copies:
-        copy.start()
+                col = offset + (kind * heads + j) * HD
+                pool[j, kind, at : at + part.shape[0]] = part[:, :, col : col + HD]
+        at += part.shape[0]
     blocks = q_ref.shape[0] // BLK
     low = lax.broadcasted_iota(jnp.int32, (1, 2 * BLK), 1) < BLK
     tri_row = lax.broadcasted_iota(jnp.int32, (BLK, HD), 0)
@@ -390,34 +368,28 @@
             out_ref[pl.ds(at_row, BLK), c : c + HD] = o[g * BLK : (g + 1) * BLK]
         return carry
 
-    each = 2 * n
     for j in range(heads):
-        for copy in copies[j * each : (j + 1) * each]:
-            copy.wait()
         lax.fori_loop(0, blocks, functools.partial(block, j), 0, unroll=blocks)
 
 
-def attend(queries, slots, pools, offsets, heads, group, first):
+def attend(queries, slots, parts, offsets, heads, group, first):
     rows = queries.shape[0]
     cols = heads * group * HD
-    sizes = tuple(p.shape[0] for p in pools)
+    size = sum(part.shape[0] for part in parts)
     return pl.pallas_call(
-        functools.partial(attend_kernel, sizes, offsets, heads, group, first),
+        functools.partial(attend_kernel, offsets, heads, group, first),
         out_shape=jax.ShapeDtypeStruct((rows, cols), jnp.bfloat16),
-        in_specs=[SMEM, VMEM] + [ANY] * len(pools),
+        in_specs=[SMEM, VMEM] + [VMEM] * len(parts),
         out_specs=VMEM,
-        scratch_shapes=[
-            pltpu.VMEM((heads, 2, sum(sizes), BLK, HD), jnp.bfloat16),
-            pltpu.SemaphoreType.DMA((heads, 2, len(sizes))),
-        ],
+        scratch_shapes=[pltpu.VMEM((heads, 2, size, BLK, HD), jnp.bfloat16)],
         cost_estimate=pl.CostEstimate(
             flops=4 * rows * TOPB * BLK * cols,
-            bytes_accessed=4 * rows * cols + 4 * sum(sizes) * BLK * heads * HD,
+            bytes_accessed=4 * rows * cols + 4 * size * BLK * heads * HD,
             transcendentals=rows * TOPB * BLK * cols // HD,
         ),
         compiler_params=pltpu.CompilerParams(vmem_limit_bytes=12 << 20),
         name="attend",
-    )(slots, queries, *pools)
+    )(slots, queries, *[near(part) for part in parts])
 
 
 def local(tokens, query_weight, key_weight, value_weight, out_weight, chosen):
@@ -428,6 +400,7 @@
     devices = lax.axis_size("kv")
     plane = plane_size(devices)
     lines = devices // plane
+    tp = lax.axis_size("tp")
     streams = 2 if key_heads % 2 == 0 else 1
     heads = key_heads // streams
     cols = heads * HD
@@ -497,12 +470,20 @@
         if queries is None:
             queries = project(section, [query_weight], 0, query_weight.shape[1])
     share = group * cols
+    pieces = []
+    for t in range(streams):
+        parts = [own[t]] + line_parts[t] + side_parts[t]
+        shifts = [0] * (1 + len(line_parts[t])) + offsets[t]
+        done = attend(queries, slots, parts, shifts, heads, group, t * share)
+        pieces.append(spread(done))
+    early = [(t, s) for t in range(streams) for s in range(tp)][: streams * tp - tp + 1]
+    rest = [(streams - 1, s) for s in range(1, tp)]
     total = None
-    for t in range(streams):
-        pools = [own[t]] + line_parts[t] + side_parts[t]
-        shifts = (0,) * (1 + len(line_parts[t])) + tuple(offsets[t])
-        done = attend(queries, slots, pools, shifts, heads, group, t * share)
-        total = mix(spread(done), out_weight, t, streams, total)
+    for part in (early, rest):
+        if part:
+            total = mix(
+                [pieces[t][s] for t, s in part], part, out_weight, streams, total, part == rest
+            )
     return total
 
 

time: 93.7 us -> 95.4 us (1.018)
  the two profiles are of different devices: /device:TPU:9 before, /device:TPU:17 now
where the time goes in v3:
time: 95.4 us; the launch traced here: 95.1 us
  starting transfers between devices  49.3 us (52%)
  Pallas kernels  26.2 us (27%)
  waiting for transfers between devices  19.4 us (20%)
    ppermute x27, starting transfers between devices, send(): return lax.ppermute(part, 'kv', pairs)  33.6 us
    ppermute x27, waiting for transfers between devices, send(): return lax.ppermute(part, 'kv', pairs)  19.4 us
    ppermute x3, starting transfers between devices, spread(): pieces.append(lax.ppermute(part, 'tp', pairs))  15.6 us
    pallas_call x2, Pallas kernels, project(): pl.pallas_call(functools.partial(project_kernel, count, kinds, first, col...  7.36 us
    pallas_call x2, Pallas kernels, attend(): pl.pallas_call(functools.partial(attend_kernel, offsets, heads, group, fi...  6.62 us
    pallas_call x6, Pallas kernels, pick(): pl.pallas_call(functools.partial(pick_kernel, targets, len(parts), step),...  3.63 us
    pallas_call x2, Pallas kernels, mix(): pl.pallas_call(functools.partial(mix_kernel, part, streams, len(more)), o...  2.85 us
    pallas_call x1, Pallas kernels, index(): pl.pallas_call(functools.partial(index_kernel, lines, plane, own_blocks),...  2.7 us
  transfers between devices with their start and end apart: 30, of which 11 were waited for; matrix products, arithmetic and copies ran while one was open for 0% of the time, Pallas kernels for 25%

profile of v3, /device:TPU:17, one launch (start us, length us, event | category | flops | bytes accessed | tf_op | source)
XLA Modules:
  0.0 95.1 jit_solution(15600996401628517145)
XLA Ops:
  0.0 0.7 collective-permute-start
  0.7 2.4 %front.1 = (bf16[384,1024]{1,0:T(8,128)(2,1)S(1)}, f32[384,512]{1,0:T(8,128)S(1)}, bf16[1,2,1024,256]{3,2,1,0:T(8,128)(2,1)S(1)}) custom-call(bf16[384,1024]{1,0:T(8,128)(2,1)} %own_in.1, bf16[2048,512]{1,0:T(8,128)(2,1)} %refs_2_.3, bf16[2048,512]{1,0:T(8,128)(2,1)} %refs_3_.2), custom_call_target="tpu_custom_call" | custom-call | tf_op jit(solution)/shard_map/front/pallas_call | solution.py:132
  3.1 0.6 join.1
  3.7 1.3 %collective-permute-start.1 = (bf16[6,64,512]{2,1,0:T(8,128)(2,1)S(1)}, bf16[6,64,512]{2,1,0:T(8,128)(2,1)S(1)}, u32[]{:S(2)}, u32[]{:S(2)}) collective-permute-start(bf16[6,64,512]{2,1,0:T(8,128)(2,1)S(1)} %bitcast.5), channel_id=1, source_target_pairs={{0,8},{2,10},{4,12},{6,14},{8,16},{10,18},{12,20},{14,22},{16,24},... | collective-permute-start | bytes 1179656 | tf_op jit(solution)/shard_map/ppermute | solution.py:41
  5.1 2.7 %index.1 = (s32[192]{0:T(256)S(1)}, s32[8]{0:T(128)S(1)}, s32[8]{0:T(128)S(1)}, s32[8]{0:T(128)S(1)}) custom-call(s32[6,16]{1,0:T(8,128)S(1)} %copy-done.1), custom_call_target="tpu_custom_call" | custom-call | tf_op jit(solution)/shard_map/index/pallas_call | solution.py:278
  7.8 3.3 %project.3 = bf16[384,512]{1,0:T(8,128)(2,1)S(1)} custom-call(bf16[384,1024]{1,0:T(8,128)(2,1)S(1)} %get-tuple-element.40.refs_0_, bf16[384,1024]{1,0:T(8,128)(2,1)S(1)} %collective-permute-done.refs_0_.refs_1_, bf16[2048,512]{1,0:T(8,128)(2,1)} %refs_2_.3, bf16[2048,512]{1,0:T(8,128)(2,1)} %refs_3_.2), custom_call_target="tpu_custom_call" | custom-call | flops 805306368 | bytes 3670016 | tf_op jit(solution)/shard_map/project/pallas_call | solution.py:85
  11.2 3.2 %collective-permute-done.1.refs_3_ = bf16[6,64,512]{2,1,0:T(8,128)(2,1)S(1)} collective-permute-done((bf16[6,64,512]{2,1,0:T(8,128)(2,1)S(1)}, bf16[6,64,512]{2,1,0:T(8,128)(2,1)S(1)}, u32[]{:S(2)}, u32[]{:S(2)}) %collective-permute-start.1) | collective-permute-done | bytes 393248 | tf_op jit(solution)/shard_map/ppermute | solution.py:41
  14.4 3.2 %collective-permute-start.2 = (bf16[6,64,512]{2,1,0:T(8,128)(2,1)S(1)}, bf16[6,64,512]{2,1,0:T(8,128)(2,1)S(1)}, u32[]{:S(2)}, u32[]{:S(2)}) collective-permute-start(bf16[6,64,512]{2,1,0:T(8,128)(2,1)S(1)} %collective-permute-done.1.refs_3_), channel_id=1, source_target_pairs={{0,0},{2,2},{4,4},{6,6},{8,16},{10,18},{12,20},{14,22},{16,24},{18... | collective-permute-start | bytes 1179656 | tf_op jit(solution)/shard_map/ppermute | solution.py:41
  17.6 5.2 %collective-permute-done.4.refs_4_.refs_3_ = bf16[6,64,512]{2,1,0:T(8,128)(2,1)S(1)} collective-permute-done((bf16[6,64,512]{2,1,0:T(8,128)(2,1)S(1)}, bf16[6,64,512]{2,1,0:T(8,128)(2,1)S(1)}, u32[]{:S(2)}, u32[]{:S(2)}) %collective-permute-start.4) | collective-permute-done | bytes 393248 | tf_op jit(solution)/shard_map/ppermute | solution.py:41
  22.9 3.2 %collective-permute-start.5 = (bf16[6,64,512]{2,1,0:T(8,128)(2,1)S(1)}, bf16[6,64,512]{2,1,0:T(8,128)(2,1)S(1)}, u32[]{:S(2)}, u32[]{:S(2)}) collective-permute-start(bf16[6,64,512]{2,1,0:T(8,128)(2,1)S(1)} %collective-permute-done.4.refs_4_.refs_3_), channel_id=1, source_target_pairs={{0,0},{2,2},{4,4},{6,6},{8,16},{10,18},{12,20},{14,22},{16,24},{18... | collective-permute-start | bytes 1179656 | tf_op jit(solution)/shard_map/ppermute | solution.py:41
  26.1 1.3 %collective-permute-start.7 = (s32[8]{0:T(128)S(1)}, s32[8]{0:T(128)S(1)}, u32[]{:S(2)}, u32[]{:S(2)}) collective-permute-start(s32[8]{0:T(128)S(1)} %get-tuple-element.43), channel_id=1, source_target_pairs={{0,2},{2,0},{4,6},{6,4},{8,10},{10,8},{12,14},{14,12},{16,18},{18,... | collective-permute-start | bytes 104 | tf_op jit(solution)/shard_map/ppermute | solution.py:41
  27.3 1.2 %collective-permute-start.8 = (s32[8]{0:T(128)S(1)}, s32[8]{0:T(128)S(1)}, u32[]{:S(2)}, u32[]{:S(2)}) collective-permute-start(s32[8]{0:T(128)S(1)} %get-tuple-element.44), channel_id=1, source_target_pairs={{0,4},{2,6},{4,0},{6,2},{8,12},{10,14},{12,8},{14,10},{16,20},{18,... | collective-permute-start | bytes 104 | tf_op jit(solution)/shard_map/ppermute | solution.py:41
  28.8 1.2 %collective-permute-done.8.refs_1_ = s32[8]{0:T(128)S(1)} collective-permute-done((s32[8]{0:T(128)S(1)}, s32[8]{0:T(128)S(1)}, u32[]{:S(2)}, u32[]{:S(2)}) %collective-permute-start.8) | collective-permute-done | bytes 64 | tf_op jit(solution)/shard_map/ppermute | solution.py:41
  30.0 1.8 %collective-permute-done.9.refs_2_ = s32[8]{0:T(128)S(1)} collective-permute-done((s32[8]{0:T(128)S(1)}, s32[8]{0:T(128)S(1)}, u32[]{:S(2)}, u32[]{:S(2)}) %collective-permute-start.9) | collective-permute-done | bytes 64 | tf_op jit(solution)/shard_map/ppermute | solution.py:41
  31.9 0.6 pick.6
  32.5 0.3 collective-permute-start.10
  33.1 2.0 %collective-permute-start.3 = (bf16[6,64,512]{2,1,0:T(8,128)(2,1)S(1)}, bf16[6,64,512]{2,1,0:T(8,128)(2,1)S(1)}, u32[]{:S(2)}, u32[]{:S(2)}) collective-permute-start(bf16[6,64,512]{2,1,0:T(8,128)(2,1)S(1)} %collective-permute-done.2.refs_3_.refs_4_), channel_id=1, source_target_pairs={{0,0},{2,2},{4,4},{6,6},{8,8},{10,10},{12,12},{14,14},{16,24},{18,... | collective-permute-start | bytes 1179656 | tf_op jit(solution)/shard_map/ppermute | solution.py:41
  35.0 2.2 %collective-permute-start.12 = (bf16[2,64,1024]{2,1,0:T(8,128)(2,1)S(1)}, bf16[2,64,1024]{2,1,0:T(8,128)(2,1)S(1)}, u32[]{:S(2)}, u32[]{:S(2)}) collective-permute-start(bf16[2,64,1024]{2,1,0:T(8,128)(2,1)S(1)} %get-tuple-element.48), channel_id=1, source_target_pairs={{0,6},{2,4},{4,2},{6,0},{8,14},{10,12},{12,10},{14,8},{16,22},{18,... | collective-permute-start | bytes 786440 | tf_op jit(solution)/shard_map/ppermute | solution.py:41
  37.3 0.6 pick.7
  38.1 0.3 collective-permute-start.13
  38.6 1.1 %collective-permute-done.5.refs_3_.refs_4_ = bf16[6,64,512]{2,1,0:T(8,128)(2,1)S(1)} collective-permute-done((bf16[6,64,512]{2,1,0:T(8,128)(2,1)S(1)}, bf16[6,64,512]{2,1,0:T(8,128)(2,1)S(1)}, u32[]{:S(2)}, u32[]{:S(2)}) %collective-permute-start.5) | collective-permute-done | bytes 393248 | tf_op jit(solution)/shard_map/ppermute | solution.py:41
  39.7 3.4 %collective-permute-start.6 = (bf16[6,64,512]{2,1,0:T(8,128)(2,1)S(1)}, bf16[6,64,512]{2,1,0:T(8,128)(2,1)S(1)}, u32[]{:S(2)}, u32[]{:S(2)}) collective-permute-start(bf16[6,64,512]{2,1,0:T(8,128)(2,1)S(1)} %collective-permute-done.5.refs_3_.refs_4_), channel_id=1, source_target_pairs={{0,0},{2,2},{4,4},{6,6},{8,8},{10,10},{12,12},{14,14},{16,24},{18,... | collective-permute-start | bytes 1179656 | tf_op jit(solution)/shard_map/ppermute | solution.py:41
  43.1 0.6 collective-permute-done.12.refs_8_
  43.7 2.9 %collective-permute-start.15 = (bf16[2,64,1024]{2,1,0:T(8,128)(2,1)S(1)}, bf16[2,64,1024]{2,1,0:T(8,128)(2,1)S(1)}, u32[]{:S(2)}, u32[]{:S(2)}) collective-permute-start(bf16[2,64,1024]{2,1,0:T(8,128)(2,1)S(1)} %get-tuple-element.51), channel_id=1, source_target_pairs={{0,6},{2,4},{4,2},{6,0},{8,14},{10,12},{12,10},{14,8},{16,22},{18,... | collective-permute-start | bytes 786440 | tf_op jit(solution)/shard_map/ppermute | solution.py:41
  46.5 0.6 pick.10
  47.1 2.5 %collective-permute-done.13.refs_9_ = bf16[2,64,1024]{2,1,0:T(8,128)(2,1)S(1)} collective-permute-done((bf16[2,64,1024]{2,1,0:T(8,128)(2,1)S(1)}, bf16[2,64,1024]{2,1,0:T(8,128)(2,1)S(1)}, u32[]{:S(2)}, u32[]{:S(2)}) %collective-permute-start.13) | collective-permute-done | bytes 262176 | tf_op jit(solution)/shard_map/ppermute | solution.py:41
  49.6 1.6 %collective-permute-start.23 = (bf16[2,64,512]{2,1,0:T(8,128)(2,1)S(1)}, bf16[2,64,512]{2,1,0:T(8,128)(2,1)S(1)}, u32[]{:S(2)}, u32[]{:S(2)}) collective-permute-start(bf16[2,64,512]{2,1,0:T(8,128)(2,1)S(1)} %get-tuple-element.58), channel_id=1, source_target_pairs={{0,2},{2,0},{4,6},{6,4},{8,10},{10,8},{12,14},{14,12},{16,18},{18,... | collective-permute-start | bytes 393224 | tf_op jit(solution)/shard_map/ppermute | solution.py:41
  51.5 1.7 %collective-permute-start.25 = (bf16[2,64,512]{2,1,0:T(8,128)(2,1)S(1)}, bf16[2,64,512]{2,1,0:T(8,128)(2,1)S(1)}, u32[]{:S(2)}, u32[]{:S(2)}) collective-permute-start(bf16[2,64,512]{2,1,0:T(8,128)(2,1)S(1)} %get-tuple-element.60), channel_id=1, source_target_pairs={{0,6},{2,4},{4,2},{6,0},{8,14},{10,12},{12,10},{14,8},{16,22},{18,... | collective-permute-start | bytes 393224 | tf_op jit(solution)/shard_map/ppermute | solution.py:41
  53.2 4.0 %project.2.refs_1_ = bf16[384,1024]{1,0:T(8,128)(2,1)S(1)} custom-call(bf16[384,1024]{1,0:T(8,128)(2,1)S(1)} %get-tuple-element.40.refs_0_, bf16[384,1024]{1,0:T(8,128)(2,1)S(1)} %collective-permute-done.refs_0_.refs_1_, bf16[2048,1024]{1,0:T(8,128)(2,1)} %refs_2_.2), custom_call_target="tpu_custom_call" | custom-call | flops 1610612736 | bytes 5767168 | tf_op jit(solution)/shard_map/project/pallas_call | solution.py:85
  57.3 0.6 pick.8
  57.9 0.6 pick.11
  58.5 0.7 collective-permute-start.16
  59.2 0.8 collective-permute-start.26
  60.0 1.6 %collective-permute-done.24.refs_13_ = bf16[2,64,512]{2,1,0:T(8,128)(2,1)S(1)} collective-permute-done((bf16[2,64,512]{2,1,0:T(8,128)(2,1)S(1)}, bf16[2,64,512]{2,1,0:T(8,128)(2,1)S(1)}, u32[]{:S(2)}, u32[]{:S(2)}) %collective-permute-start.24) | collective-permute-done | bytes 131104 | tf_op jit(solution)/shard_map/ppermute | solution.py:41
  61.6 2.4 %collective-permute-start.28 = (bf16[2,64,512]{2,1,0:T(8,128)(2,1)S(1)}, bf16[2,64,512]{2,1,0:T(8,128)(2,1)S(1)}, u32[]{:S(2)}, u32[]{:S(2)}) collective-permute-start(bf16[2,64,512]{2,1,0:T(8,128)(2,1)S(1)} %get-tuple-element.64), channel_id=1, source_target_pairs={{0,6},{2,4},{4,2},{6,0},{8,14},{10,12},{12,10},{14,8},{16,22},{18,... | collective-permute-start | bytes 393224 | tf_op jit(solution)/shard_map/ppermute | solution.py:41
  64.0 0.7 collective-permute-start.17
  64.7 0.6 pick.9
  65.3 0.8 collective-permute-start.18
  66.1 1.2 %collective-permute-start.19 = (bf16[2,64,512]{2,1,0:T(8,128)(2,1)S(1)}, bf16[2,64,512]{2,1,0:T(8,128)(2,1)S(1)}, u32[]{:S(2)}, u32[]{:S(2)}) collective-permute-start(bf16[2,64,512]{2,1,0:T(8,128)(2,1)S(1)} %get-tuple-element.55), channel_id=1, source_target_pairs={{0,2},{2,0},{4,6},{6,4},{8,10},{10,8},{12,14},{14,12},{16,18},{18,... | collective-permute-start | bytes 393224 | tf_op jit(solution)/shard_map/ppermute | solution.py:41
  67.3 0.7 collective-permute-start.20
  68.0 0.8 collective-permute-start.21
  68.8 3.3 %attend.3.refs_0_ = bf16[384,512]{1,0:T(8,128)(2,1)S(1)} custom-call(s32[192]{0:T(256)S(1)} %get-tuple-element.38.refs_0_, bf16[384,1024]{1,0:T(8,128)(2,1)S(1)} %project.2.refs_1_, bf16[6,64,512]{2,1,0:T(8,128)(2,1)S(1)} %bitcast.7, bf16[6,64,512]{2,1,0:T(8,128)(2,1)S(1)} %collective-permute-done.1.refs_3_, ...), custom_call_target="tpu_custom_call" | custom-call | flops 805306368 | bytes 3932160 | tf_op jit(solution)/shard_map/attend/pallas_call | solution.py:379
  72.1 1.8 %collective-permute-done.17.refs_13_ = bf16[2,64,512]{2,1,0:T(8,128)(2,1)S(1)} collective-permute-done((bf16[2,64,512]{2,1,0:T(8,128)(2,1)S(1)}, bf16[2,64,512]{2,1,0:T(8,128)(2,1)S(1)}, u32[]{:S(2)}, u32[]{:S(2)}) %collective-permute-start.17) | collective-permute-done | bytes 131104 | tf_op jit(solution)/shard_map/ppermute | solution.py:41
  74.0 13.2 %collective-permute-start.29 = (bf16[384,512]{1,0:T(8,128)(2,1)S(1)}, bf16[384,512]{1,0:T(8,128)(2,1)S(1)}, u32[]{:S(2)}, u32[]{:S(2)}) collective-permute-start(bf16[384,512]{1,0:T(8,128)(2,1)S(1)} %attend.3.refs_0_), channel_id=1, source_target_pairs={{0,1},{1,0},{2,3},{3,2},{4,5},{5,4},{6,7},{7,6},{8,9},{9,8},{10,11... | collective-permute-start | bytes 1179656 | tf_op jit(solution)/shard_map/ppermute | solution.py:49
  87.2 3.3 %attend.2.refs_2_ = bf16[384,512]{1,0:T(8,128)(2,1)S(1)} custom-call(s32[192]{0:T(256)S(1)} %get-tuple-element.38.refs_0_, bf16[384,1024]{1,0:T(8,128)(2,1)S(1)} %project.2.refs_1_, bf16[6,64,512]{2,1,0:T(8,128)(2,1)S(1)} %bitcast.4, bf16[6,64,512]{2,1,0:T(8,128)(2,1)S(1)} %collective-permute-done.4.refs_4_.refs_3_, ...), custom_call_target="tpu_custom_call" | custom-call | flops 805306368 | bytes 3932160 | tf_op jit(solution)/shard_map/attend/pallas_call | solution.py:379
  90.5 1.8 %collective-permute-start.22 = (bf16[384,512]{1,0:T(8,128)(2,1)S(1)}, bf16[384,512]{1,0:T(8,128)(2,1)S(1)}, u32[]{:S(2)}, u32[]{:S(2)}) collective-permute-start(bf16[384,512]{1,0:T(8,128)(2,1)S(1)} %attend.2.refs_2_), channel_id=1, source_target_pairs={{0,1},{1,0},{2,3},{3,2},{4,5},{5,4},{6,7},{7,6},{8,9},{9,8},{10,11... | collective-permute-start | bytes 1179656 | tf_op jit(solution)/shard_map/ppermute | solution.py:49
  92.3 1.4 %mix.2.refs_2_ = f32[384,1024]{1,0:T(8,128)S(1)} custom-call(bf16[384,512]{1,0:T(8,128)(2,1)S(1)} %attend.3.refs_0_, bf16[384,512]{1,0:T(8,128)(2,1)S(1)} %collective-permute-done.29.refs_1_, bf16[384,512]{1,0:T(8,128)(2,1)S(1)} %attend.2.refs_2_, bf16[2048,1024]{1,0:T(8,128)(2,1)S(1)} %copy-done), custom_call_target="tpu_custom_call" | custom-call | flops 1207959552 | bytes 5898240 | tf_op jit(solution)/shard_map/mix/pallas_call | solution.py:200
  93.6 1.5 %mix.3 = bf16[384,1024]{1,0:T(8,128)(2,1)} custom-call(bf16[384,512]{1,0:T(8,128)(2,1)S(1)} %collective-permute-done.22.refs_0_, bf16[2048,1024]{1,0:T(8,128)(2,1)S(1)} %copy-done, f32[384,1024]{1,0:T(8,128)S(1)} %mix.2.refs_2_), custom_call_target="tpu_custom_call" | custom-call | flops 402653184 | bytes 3014656 | tf_op jit(solution)/shard_map/mix/pallas_call | solution.py:200
  (31 shorter events, 1.3 us)
Async XLA Ops:
  0.0 3.1 %collective-permute-start = (bf16[384,1024]{1,0:T(8,128)(2,1)}, bf16[384,1024]{1,0:T(8,128)(2,1)S(1)}, u32[]{:S(2)}, u32[]{:S(2)}) collective-permute-start(bf16[384,1024]{1,0:T(8,128)(2,1)} %own_in.1), channel_id=1, source_target_pairs={{0,1},{1,0},{2,3},{3,2},{4,5},{5,4},{6,7},{7,6},{8,9},{9,8},{10,11... | collective-permute-start | bytes 2359304 | tf_op jit(solution)/shard_map/ppermute | solution.py:49
  3.1 2.0 %copy-start.1 = (s32[6,16]{1,0:T(8,128)S(1)}, s32[6,16]{1,0:T(8,128)}, u32[]{:S(2)}) copy-start(s32[6,16]{1,0:T(8,128)} %chosen_ref) | copy-start | bytes 1156
  3.7 10.7 %collective-permute-start.1 = (bf16[6,64,512]{2,1,0:T(8,128)(2,1)S(1)}, bf16[6,64,512]{2,1,0:T(8,128)(2,1)S(1)}, u32[]{:S(2)}, u32[]{:S(2)}) collective-permute-start(bf16[6,64,512]{2,1,0:T(8,128)(2,1)S(1)} %bitcast.5), channel_id=1, source_target_pairs={{0,8},{2,10},{4,12},{6,14},{8,16},{10,18},{12,20},{14,22},{16,24},... | collective-permute-start | bytes 1179656 | tf_op jit(solution)/shard_map/ppermute | solution.py:41
  11.1 11.7 %collective-permute-start.4 = (bf16[6,64,512]{2,1,0:T(8,128)(2,1)S(1)}, bf16[6,64,512]{2,1,0:T(8,128)(2,1)S(1)}, u32[]{:S(2)}, u32[]{:S(2)}) collective-permute-start(bf16[6,64,512]{2,1,0:T(8,128)(2,1)S(1)} %bitcast.2), channel_id=1, source_target_pairs={{0,8},{2,10},{4,12},{6,14},{8,16},{10,18},{12,20},{14,22},{16,24},... | collective-permute-start | bytes 1179656 | tf_op jit(solution)/shard_map/ppermute | solution.py:41
  14.4 18.6 %collective-permute-start.2 = (bf16[6,64,512]{2,1,0:T(8,128)(2,1)S(1)}, bf16[6,64,512]{2,1,0:T(8,128)(2,1)S(1)}, u32[]{:S(2)}, u32[]{:S(2)}) collective-permute-start(bf16[6,64,512]{2,1,0:T(8,128)(2,1)S(1)} %collective-permute-done.1.refs_3_), channel_id=1, source_target_pairs={{0,0},{2,2},{4,4},{6,6},{8,16},{10,18},{12,20},{14,22},{16,24},{18... | collective-permute-start | bytes 1179656 | tf_op jit(solution)/shard_map/ppermute | solution.py:41
  22.9 16.9 %collective-permute-start.5 = (bf16[6,64,512]{2,1,0:T(8,128)(2,1)S(1)}, bf16[6,64,512]{2,1,0:T(8,128)(2,1)S(1)}, u32[]{:S(2)}, u32[]{:S(2)}) collective-permute-start(bf16[6,64,512]{2,1,0:T(8,128)(2,1)S(1)} %collective-permute-done.4.refs_4_.refs_3_), channel_id=1, source_target_pairs={{0,0},{2,2},{4,4},{6,6},{8,16},{10,18},{12,20},{14,22},{16,24},{18... | collective-permute-start | bytes 1179656 | tf_op jit(solution)/shard_map/ppermute | solution.py:41
  26.1 2.8 %collective-permute-start.7 = (s32[8]{0:T(128)S(1)}, s32[8]{0:T(128)S(1)}, u32[]{:S(2)}, u32[]{:S(2)}) collective-permute-start(s32[8]{0:T(128)S(1)} %get-tuple-element.43), channel_id=1, source_target_pairs={{0,2},{2,0},{4,6},{6,4},{8,10},{10,8},{12,14},{14,12},{16,18},{18,... | collective-permute-start | bytes 104 | tf_op jit(solution)/shard_map/ppermute | solution.py:41
  27.3 2.7 %collective-permute-start.8 = (s32[8]{0:T(128)S(1)}, s32[8]{0:T(128)S(1)}, u32[]{:S(2)}, u32[]{:S(2)}) collective-permute-start(s32[8]{0:T(128)S(1)} %get-tuple-element.44), channel_id=1, source_target_pairs={{0,4},{2,6},{4,0},{6,2},{8,12},{10,14},{12,8},{14,10},{16,20},{18,... | collective-permute-start | bytes 104 | tf_op jit(solution)/shard_map/ppermute | solution.py:41
  28.6 3.3 %collective-permute-start.9 = (s32[8]{0:T(128)S(1)}, s32[8]{0:T(128)S(1)}, u32[]{:S(2)}, u32[]{:S(2)}) collective-permute-start(s32[8]{0:T(128)S(1)} %get-tuple-element.45), channel_id=1, source_target_pairs={{0,6},{2,4},{4,2},{6,0},{8,14},{10,12},{12,10},{14,8},{16,22},{18,... | collective-permute-start | bytes 104 | tf_op jit(solution)/shard_map/ppermute | solution.py:41
  32.5 5.6 %collective-permute-start.10 = (bf16[2,64,1024]{2,1,0:T(8,128)(2,1)S(1)}, bf16[2,64,1024]{2,1,0:T(8,128)(2,1)S(1)}, u32[]{:S(2)}, u32[]{:S(2)}) collective-permute-start(bf16[2,64,1024]{2,1,0:T(8,128)(2,1)S(1)} %get-tuple-element.46), channel_id=1, source_target_pairs={{0,2},{2,0},{4,6},{6,4},{8,10},{10,8},{12,14},{14,12},{16,18},{18,... | collective-permute-start | bytes 786440 | tf_op jit(solution)/shard_map/ppermute | solution.py:41
  32.8 5.5 %collective-permute-start.11 = (bf16[2,64,1024]{2,1,0:T(8,128)(2,1)S(1)}, bf16[2,64,1024]{2,1,0:T(8,128)(2,1)S(1)}, u32[]{:S(2)}, u32[]{:S(2)}) collective-permute-start(bf16[2,64,1024]{2,1,0:T(8,128)(2,1)S(1)} %get-tuple-element.47), channel_id=1, source_target_pairs={{0,4},{2,6},{4,0},{6,2},{8,12},{10,14},{12,8},{14,10},{16,20},{18,... | collective-permute-start | bytes 786440 | tf_op jit(solution)/shard_map/ppermute | solution.py:41
  33.1 18.4 %collective-permute-start.3 = (bf16[6,64,512]{2,1,0:T(8,128)(2,1)S(1)}, bf16[6,64,512]{2,1,0:T(8,128)(2,1)S(1)}, u32[]{:S(2)}, u32[]{:S(2)}) collective-permute-start(bf16[6,64,512]{2,1,0:T(8,128)(2,1)S(1)} %collective-permute-done.2.refs_3_.refs_4_), channel_id=1, source_target_pairs={{0,0},{2,2},{4,4},{6,6},{8,8},{10,10},{12,12},{14,14},{16,24},{18,... | collective-permute-start | bytes 1179656 | tf_op jit(solution)/shard_map/ppermute | solution.py:41
  35.0 8.6 %collective-permute-start.12 = (bf16[2,64,1024]{2,1,0:T(8,128)(2,1)S(1)}, bf16[2,64,1024]{2,1,0:T(8,128)(2,1)S(1)}, u32[]{:S(2)}, u32[]{:S(2)}) collective-permute-start(bf16[2,64,1024]{2,1,0:T(8,128)(2,1)S(1)} %get-tuple-element.48), channel_id=1, source_target_pairs={{0,6},{2,4},{4,2},{6,0},{8,14},{10,12},{12,10},{14,8},{16,22},{18,... | collective-permute-start | bytes 786440 | tf_op jit(solution)/shard_map/ppermute | solution.py:41
  38.1 11.5 %collective-permute-start.13 = (bf16[2,64,1024]{2,1,0:T(8,128)(2,1)S(1)}, bf16[2,64,1024]{2,1,0:T(8,128)(2,1)S(1)}, u32[]{:S(2)}, u32[]{:S(2)}) collective-permute-start(bf16[2,64,1024]{2,1,0:T(8,128)(2,1)S(1)} %get-tuple-element.49), channel_id=1, source_target_pairs={{0,2},{2,0},{4,6},{6,4},{8,10},{10,8},{12,14},{14,12},{16,18},{18,... | collective-permute-start | bytes 786440 | tf_op jit(solution)/shard_map/ppermute | solution.py:41
  38.4 12.9 %collective-permute-start.14 = (bf16[2,64,1024]{2,1,0:T(8,128)(2,1)S(1)}, bf16[2,64,1024]{2,1,0:T(8,128)(2,1)S(1)}, u32[]{:S(2)}, u32[]{:S(2)}) collective-permute-start(bf16[2,64,1024]{2,1,0:T(8,128)(2,1)S(1)} %get-tuple-element.50), channel_id=1, source_target_pairs={{0,4},{2,6},{4,0},{6,2},{8,12},{10,14},{12,8},{14,10},{16,20},{18,... | collective-permute-start | bytes 786440 | tf_op jit(solution)/shard_map/ppermute | solution.py:41
  39.7 24.3 %collective-permute-start.6 = (bf16[6,64,512]{2,1,0:T(8,128)(2,1)S(1)}, bf16[6,64,512]{2,1,0:T(8,128)(2,1)S(1)}, u32[]{:S(2)}, u32[]{:S(2)}) collective-permute-start(bf16[6,64,512]{2,1,0:T(8,128)(2,1)S(1)} %collective-permute-done.5.refs_3_.refs_4_), channel_id=1, source_target_pairs={{0,0},{2,2},{4,4},{6,6},{8,8},{10,10},{12,12},{14,14},{16,24},{18,... | collective-permute-start | bytes 1179656 | tf_op jit(solution)/shard_map/ppermute | solution.py:41
  43.7 14.8 %collective-permute-start.15 = (bf16[2,64,1024]{2,1,0:T(8,128)(2,1)S(1)}, bf16[2,64,1024]{2,1,0:T(8,128)(2,1)S(1)}, u32[]{:S(2)}, u32[]{:S(2)}) collective-permute-start(bf16[2,64,1024]{2,1,0:T(8,128)(2,1)S(1)} %get-tuple-element.51), channel_id=1, source_target_pairs={{0,6},{2,4},{4,2},{6,0},{8,14},{10,12},{12,10},{14,8},{16,22},{18,... | collective-permute-start | bytes 786440 | tf_op jit(solution)/shard_map/ppermute | solution.py:41
  49.6 9.6 %collective-permute-start.23 = (bf16[2,64,512]{2,1,0:T(8,128)(2,1)S(1)}, bf16[2,64,512]{2,1,0:T(8,128)(2,1)S(1)}, u32[]{:S(2)}, u32[]{:S(2)}) collective-permute-start(bf16[2,64,512]{2,1,0:T(8,128)(2,1)S(1)} %get-tuple-element.58), channel_id=1, source_target_pairs={{0,2},{2,0},{4,6},{6,4},{8,10},{10,8},{12,14},{14,12},{16,18},{18,... | collective-permute-start | bytes 393224 | tf_op jit(solution)/shard_map/ppermute | solution.py:41
  51.3 10.3 %collective-permute-start.24 = (bf16[2,64,512]{2,1,0:T(8,128)(2,1)S(1)}, bf16[2,64,512]{2,1,0:T(8,128)(2,1)S(1)}, u32[]{:S(2)}, u32[]{:S(2)}) collective-permute-start(bf16[2,64,512]{2,1,0:T(8,128)(2,1)S(1)} %get-tuple-element.59), channel_id=1, source_target_pairs={{0,4},{2,6},{4,0},{6,2},{8,12},{10,14},{12,8},{14,10},{16,20},{18,... | collective-permute-start | bytes 393224 | tf_op jit(solution)/shard_map/ppermute | solution.py:41
  51.5 10.1 %collective-permute-start.25 = (bf16[2,64,512]{2,1,0:T(8,128)(2,1)S(1)}, bf16[2,64,512]{2,1,0:T(8,128)(2,1)S(1)}, u32[]{:S(2)}, u32[]{:S(2)}) collective-permute-start(bf16[2,64,512]{2,1,0:T(8,128)(2,1)S(1)} %get-tuple-element.60), channel_id=1, source_target_pairs={{0,6},{2,4},{4,2},{6,0},{8,14},{10,12},{12,10},{14,8},{16,22},{18,... | collective-permute-start | bytes 393224 | tf_op jit(solution)/shard_map/ppermute | solution.py:41
  58.5 6.8 %collective-permute-start.16 = (bf16[2,64,512]{2,1,0:T(8,128)(2,1)S(1)}, bf16[2,64,512]{2,1,0:T(8,128)(2,1)S(1)}, u32[]{:S(2)}, u32[]{:S(2)}) collective-permute-start(bf16[2,64,512]{2,1,0:T(8,128)(2,1)S(1)} %get-tuple-element.52), channel_id=1, source_target_pairs={{0,2},{2,0},{4,6},{6,4},{8,10},{10,8},{12,14},{14,12},{16,18},{18,... | collective-permute-start | bytes 393224 | tf_op jit(solution)/shard_map/ppermute | solution.py:41
  59.2 6.9 %collective-permute-start.26 = (bf16[2,64,512]{2,1,0:T(8,128)(2,1)S(1)}, bf16[2,64,512]{2,1,0:T(8,128)(2,1)S(1)}, u32[]{:S(2)}, u32[]{:S(2)}) collective-permute-start(bf16[2,64,512]{2,1,0:T(8,128)(2,1)S(1)} %get-tuple-element.62), channel_id=1, source_target_pairs={{0,2},{2,0},{4,6},{6,4},{8,10},{10,8},{12,14},{14,12},{16,18},{18,... | collective-permute-start | bytes 393224 | tf_op jit(solution)/shard_map/ppermute | solution.py:41
  61.6 5.7 %collective-permute-start.27 = (bf16[2,64,512]{2,1,0:T(8,128)(2,1)S(1)}, bf16[2,64,512]{2,1,0:T(8,128)(2,1)S(1)}, u32[]{:S(2)}, u32[]{:S(2)}) collective-permute-start(bf16[2,64,512]{2,1,0:T(8,128)(2,1)S(1)} %get-tuple-element.63), channel_id=1, source_target_pairs={{0,4},{2,6},{4,0},{6,2},{8,12},{10,14},{12,8},{14,10},{16,20},{18,... | collective-permute-start | bytes 393224 | tf_op jit(solution)/shard_map/ppermute | solution.py:41
  61.6 6.4 %collective-permute-start.28 = (bf16[2,64,512]{2,1,0:T(8,128)(2,1)S(1)}, bf16[2,64,512]{2,1,0:T(8,128)(2,1)S(1)}, u32[]{:S(2)}, u32[]{:S(2)}) collective-permute-start(bf16[2,64,512]{2,1,0:T(8,128)(2,1)S(1)} %get-tuple-element.64), channel_id=1, source_target_pairs={{0,6},{2,4},{4,2},{6,0},{8,14},{10,12},{12,10},{14,8},{16,22},{18,... | collective-permute-start | bytes 393224 | tf_op jit(solution)/shard_map/ppermute | solution.py:41
  64.0 10.0 %collective-permute-start.17 = (bf16[2,64,512]{2,1,0:T(8,128)(2,1)S(1)}, bf16[2,64,512]{2,1,0:T(8,128)(2,1)S(1)}, u32[]{:S(2)}, u32[]{:S(2)}) collective-permute-start(bf16[2,64,512]{2,1,0:T(8,128)(2,1)S(1)} %get-tuple-element.53), channel_id=1, source_target_pairs={{0,4},{2,6},{4,0},{6,2},{8,12},{10,14},{12,8},{14,10},{16,20},{18,... | collective-permute-start | bytes 393224 | tf_op jit(solution)/shard_map/ppermute | solution.py:41
  65.3 21.8 %collective-permute-start.18 = (bf16[2,64,512]{2,1,0:T(8,128)(2,1)S(1)}, bf16[2,64,512]{2,1,0:T(8,128)(2,1)S(1)}, u32[]{:S(2)}, u32[]{:S(2)}) collective-permute-start(bf16[2,64,512]{2,1,0:T(8,128)(2,1)S(1)} %get-tuple-element.54), channel_id=1, source_target_pairs={{0,6},{2,4},{4,2},{6,0},{8,14},{10,12},{12,10},{14,8},{16,22},{18,... | collective-permute-start | bytes 393224 | tf_op jit(solution)/shard_map/ppermute | solution.py:41
  66.1 21.0 %collective-permute-start.19 = (bf16[2,64,512]{2,1,0:T(8,128)(2,1)S(1)}, bf16[2,64,512]{2,1,0:T(8,128)(2,1)S(1)}, u32[]{:S(2)}, u32[]{:S(2)}) collective-permute-start(bf16[2,64,512]{2,1,0:T(8,128)(2,1)S(1)} %get-tuple-element.55), channel_id=1, source_target_pairs={{0,2},{2,0},{4,6},{6,4},{8,10},{10,8},{12,14},{14,12},{16,18},{18,... | collective-permute-start | bytes 393224 | tf_op jit(solution)/shard_map/ppermute | solution.py:41
  67.3 19.8 %collective-permute-start.20 = (bf16[2,64,512]{2,1,0:T(8,128)(2,1)S(1)}, bf16[2,64,512]{2,1,0:T(8,128)(2,1)S(1)}, u32[]{:S(2)}, u32[]{:S(2)}) collective-permute-start(bf16[2,64,512]{2,1,0:T(8,128)(2,1)S(1)} %get-tuple-element.56), channel_id=1, source_target_pairs={{0,4},{2,6},{4,0},{6,2},{8,12},{10,14},{12,8},{14,10},{16,20},{18,... | collective-permute-start | bytes 393224 | tf_op jit(solution)/shard_map/ppermute | solution.py:41
  68.0 19.1 %collective-permute-start.21 = (bf16[2,64,512]{2,1,0:T(8,128)(2,1)S(1)}, bf16[2,64,512]{2,1,0:T(8,128)(2,1)S(1)}, u32[]{:S(2)}, u32[]{:S(2)}) collective-permute-start(bf16[2,64,512]{2,1,0:T(8,128)(2,1)S(1)} %get-tuple-element.57), channel_id=1, source_target_pairs={{0,6},{2,4},{4,2},{6,0},{8,14},{10,12},{12,10},{14,8},{16,22},{18,... | collective-permute-start | bytes 393224 | tf_op jit(solution)/shard_map/ppermute | solution.py:41
  72.1 20.1 %copy-start = (bf16[2048,1024]{1,0:T(8,128)(2,1)S(1)}, bf16[2048,1024]{1,0:T(8,128)(2,1)}, u32[]{:S(2)}) copy-start(bf16[2048,1024]{1,0:T(8,128)(2,1)} %refs_1_.1) | copy-start | bytes 12582916
  74.0 18.3 %collective-permute-start.29 = (bf16[384,512]{1,0:T(8,128)(2,1)S(1)}, bf16[384,512]{1,0:T(8,128)(2,1)S(1)}, u32[]{:S(2)}, u32[]{:S(2)}) collective-permute-start(bf16[384,512]{1,0:T(8,128)(2,1)S(1)} %attend.3.refs_0_), channel_id=1, source_target_pairs={{0,1},{1,0},{2,3},{3,2},{4,5},{5,4},{6,7},{7,6},{8,9},{9,8},{10,11... | collective-permute-start | bytes 1179656 | tf_op jit(solution)/shard_map/ppermute | solution.py:49
  90.5 3.1 %collective-permute-start.22 = (bf16[384,512]{1,0:T(8,128)(2,1)S(1)}, bf16[384,512]{1,0:T(8,128)(2,1)S(1)}, u32[]{:S(2)}, u32[]{:S(2)}) collective-permute-start(bf16[384,512]{1,0:T(8,128)(2,1)S(1)} %attend.2.refs_2_), channel_id=1, source_target_pairs={{0,1},{1,0},{2,3},{3,2},{4,5},{5,4},{6,7},{7,6},{8,9},{9,8},{10,11... | collective-permute-start | bytes 1179656 | tf_op jit(solution)/shard_map/ppermute | solution.py:49

commit v4 on v3

--- a/solution.py
+++ b/solution.py
@@ -172,9 +172,12 @@
     )(*others, near(part), near(rest))
 
 
-def mix_kernel(part, streams, more, *refs):
-    pieces = refs[: -2 - more]
-    weight_ref, out_ref = refs[-2 - more], refs[-1]
+def mix_kernel(part, streams, more, last, *refs):
+    home = refs[-3] if last else None
+    out_ref, sems = refs[-2:] if last else (refs[-1], None)
+    refs = refs[:-3] if last else refs[:-1]
+    pieces = refs[: -1 - more]
+    weight_ref = refs[-1 - more]
     count = lax.axis_size("tp")
     width = pieces[0].shape[1]
     step = min(2 * HD, out_ref.shape[1])
@@ -183,14 +186,21 @@
         pl.multiple_of((lax.rem(me + s, count) * streams + t) * width, width)
         for t, s in part
     ]
-    for col in range(0, out_ref.shape[1], step):
+    copies = []
+    for i, col in enumerate(range(0, out_ref.shape[1], step)):
         span = slice(col, col + step)
-        total = refs[-2][:, span] if more else None
+        total = refs[-1][:, span] if more else None
         for at, piece in zip(starts, pieces):
             rows = weight_ref[pl.ds(at, width), span]
             term = jnp.dot(piece[...], rows, preferred_element_type=jnp.float32)
             total = term if total is None else total + term
         out_ref[:, span] = total.astype(out_ref.dtype)
+        if last:
+            copy = pltpu.make_async_copy(out_ref.at[:, span], home.at[:, span], sems.at[i])
+            copy.start()
+            copies.append(copy)
+    for copy in copies:
+        copy.wait()
 
 
 def mix(pieces, part, weight, streams, before, last):
@@ -198,10 +208,16 @@
     cols = weight.shape[1]
     more = [] if before is None else [before]
     return pl.pallas_call(
-        functools.partial(mix_kernel, part, streams, len(more)),
+        functools.partial(mix_kernel, part, streams, len(more), last),
         out_shape=jax.ShapeDtypeStruct((rows, cols), jnp.bfloat16 if last else jnp.float32),
         in_specs=[VMEM] * (len(pieces) + 1 + len(more)),
-        out_specs=VMEM,
+        out_specs=ANY if last else VMEM,
+        scratch_shapes=[
+            pltpu.VMEM((rows, cols), jnp.bfloat16),
+            pltpu.SemaphoreType.DMA((pl.cdiv(cols, 2 * HD),)),
+        ]
+        if last
+        else [],
         cost_estimate=pl.CostEstimate(
             flops=2 * rows * width * len(pieces) * cols,
             bytes_accessed=2 * width * len(pieces) * (rows + cols) + 4 * rows * cols,
@@ -449,7 +465,7 @@
     held = own
     for step in range(lines):
         last = step == lines - 1
-        split = step >= lines - 2
+        split = step >= 1
         batches = [[t] for t in range(streams)] if split else [list(range(streams))]
         if last and queries is not None:
             held[0], queries = lax.optimization_barrier((held[0], queries))

time: 95.4 us -> 96 us (level)
  the two profiles are of different devices: /device:TPU:17 before, /device:TPU:0 now
where the time goes in v4:
time: 96 us; the launch traced here: 95.7 us
  starting transfers between devices  38.4 us (40%)
  waiting for transfers between devices  30.2 us (31%)
  Pallas kernels  26.6 us (28%)
    ppermute x30, starting transfers between devices, send(): return lax.ppermute(part, 'kv', pairs)  37.8 us
    ppermute x30, waiting for transfers between devices, send(): return lax.ppermute(part, 'kv', pairs)  29.9 us
    pallas_call x2, Pallas kernels, project(): pl.pallas_call(functools.partial(project_kernel, count, kinds, first, col...  7.36 us
    pallas_call x2, Pallas kernels, attend(): pl.pallas_call(functools.partial(attend_kernel, offsets, heads, group, fi...  6.57 us
    pallas_call x7, Pallas kernels, pick(): pl.pallas_call(functools.partial(pick_kernel, targets, len(parts), step),...  4.2 us
    pallas_call x2, Pallas kernels, mix(): pl.pallas_call(functools.partial(mix_kernel, part, streams, len(more), la...  2.76 us
    pallas_call x1, Pallas kernels, index(): pl.pallas_call(functools.partial(index_kernel, lines, plane, own_blocks),...  2.7 us
    pallas_call x1, Pallas kernels, front(): pl.pallas_call(functools.partial(front_kernel, others, cols), out_shape=[...  2.44 us
  transfers between devices with their start and end apart: 33, of which 13 were waited for; matrix products, arithmetic and copies ran while one was open for 0% of the time, Pallas kernels for 26%

profile of v4, /device:TPU:0, one launch (start us, length us, event | category | flops | bytes accessed | tf_op | source)
XLA Modules:
  0.0 95.7 jit_solution(12155555853446350870)
XLA Ops:
  0.0 0.5 collective-permute-start
  0.5 2.4 %front.1 = (bf16[384,1024]{1,0:T(8,128)(2,1)S(1)}, f32[384,512]{1,0:T(8,128)S(1)}, bf16[1,2,1024,256]{3,2,1,0:T(8,128)(2,1)S(1)}) custom-call(bf16[384,1024]{1,0:T(8,128)(2,1)} %own_in.1, bf16[2048,512]{1,0:T(8,128)(2,1)} %refs_2_.3, bf16[2048,512]{1,0:T(8,128)(2,1)} %refs_3_.2), custom_call_target="tpu_custom_call" | custom-call | tf_op jit(solution)/shard_map/front/pallas_call | solution.py:132
  3.0 0.6 join.1
  3.5 2.6 %collective-permute-start.1 = (bf16[6,64,512]{2,1,0:T(8,128)(2,1)S(1)}, bf16[6,64,512]{2,1,0:T(8,128)(2,1)S(1)}, u32[]{:S(2)}, u32[]{:S(2)}) collective-permute-start(bf16[6,64,512]{2,1,0:T(8,128)(2,1)S(1)} %bitcast.5), channel_id=1, source_target_pairs={{0,8},{2,10},{4,12},{6,14},{8,16},{10,18},{12,20},{14,22},{16,24},... | collective-permute-start | bytes 1179656 | tf_op jit(solution)/shard_map/ppermute | solution.py:41
  6.2 2.7 %index.1 = (s32[192]{0:T(256)S(1)}, s32[8]{0:T(128)S(1)}, s32[8]{0:T(128)S(1)}, s32[8]{0:T(128)S(1)}) custom-call(s32[6,16]{1,0:T(8,128)S(1)} %copy-done.1), custom_call_target="tpu_custom_call" | custom-call | tf_op jit(solution)/shard_map/index/pallas_call | solution.py:294
  8.9 3.3 %project.3 = bf16[384,512]{1,0:T(8,128)(2,1)S(1)} custom-call(bf16[384,1024]{1,0:T(8,128)(2,1)S(1)} %get-tuple-element.43.refs_0_, bf16[384,1024]{1,0:T(8,128)(2,1)S(1)} %collective-permute-done.refs_0_.refs_1_, bf16[2048,512]{1,0:T(8,128)(2,1)} %refs_2_.3, bf16[2048,512]{1,0:T(8,128)(2,1)} %refs_3_.2), custom_call_target="tpu_custom_call" | custom-call | flops 805306368 | bytes 3670016 | tf_op jit(solution)/shard_map/project/pallas_call | solution.py:85
  12.2 1.6 %collective-permute-start.4 = (bf16[6,64,512]{2,1,0:T(8,128)(2,1)S(1)}, bf16[6,64,512]{2,1,0:T(8,128)(2,1)S(1)}, u32[]{:S(2)}, u32[]{:S(2)}) collective-permute-start(bf16[6,64,512]{2,1,0:T(8,128)(2,1)S(1)} %bitcast.2), channel_id=1, source_target_pairs={{0,8},{2,10},{4,12},{6,14},{8,16},{10,18},{12,20},{14,22},{16,24},... | collective-permute-start | bytes 1179656 | tf_op jit(solution)/shard_map/ppermute | solution.py:41
  13.9 4.3 %collective-permute-done.1.refs_3_ = bf16[6,64,512]{2,1,0:T(8,128)(2,1)S(1)} collective-permute-done((bf16[6,64,512]{2,1,0:T(8,128)(2,1)S(1)}, bf16[6,64,512]{2,1,0:T(8,128)(2,1)S(1)}, u32[]{:S(2)}, u32[]{:S(2)}) %collective-permute-start.1) | collective-permute-done | bytes 393248 | tf_op jit(solution)/shard_map/ppermute | solution.py:41
  18.2 0.7 collective-permute-start.2
  18.9 7.7 %collective-permute-done.4.refs_3_ = bf16[6,64,512]{2,1,0:T(8,128)(2,1)S(1)} collective-permute-done((bf16[6,64,512]{2,1,0:T(8,128)(2,1)S(1)}, bf16[6,64,512]{2,1,0:T(8,128)(2,1)S(1)}, u32[]{:S(2)}, u32[]{:S(2)}) %collective-permute-start.4) | collective-permute-done | bytes 393248 | tf_op jit(solution)/shard_map/ppermute | solution.py:41
  26.6 0.7 collective-permute-start.5
  27.3 1.8 %collective-permute-start.7 = (s32[8]{0:T(128)S(1)}, s32[8]{0:T(128)S(1)}, u32[]{:S(2)}, u32[]{:S(2)}) collective-permute-start(s32[8]{0:T(128)S(1)} %get-tuple-element.46), channel_id=1, source_target_pairs={{0,2},{2,0},{4,6},{6,4},{8,10},{10,8},{12,14},{14,12},{16,18},{18,... | collective-permute-start | bytes 104 | tf_op jit(solution)/shard_map/ppermute | solution.py:41
  29.1 1.5 %collective-permute-start.8 = (s32[8]{0:T(128)S(1)}, s32[8]{0:T(128)S(1)}, u32[]{:S(2)}, u32[]{:S(2)}) collective-permute-start(s32[8]{0:T(128)S(1)} %get-tuple-element.47), channel_id=1, source_target_pairs={{0,4},{2,6},{4,0},{6,2},{8,12},{10,14},{12,8},{14,10},{16,20},{18,... | collective-permute-start | bytes 104 | tf_op jit(solution)/shard_map/ppermute | solution.py:41
  30.9 1.7 %collective-permute-done.8.refs_1_ = s32[8]{0:T(128)S(1)} collective-permute-done((s32[8]{0:T(128)S(1)}, s32[8]{0:T(128)S(1)}, u32[]{:S(2)}, u32[]{:S(2)}) %collective-permute-start.8) | collective-permute-done | bytes 64 | tf_op jit(solution)/shard_map/ppermute | solution.py:41
  32.6 2.4 %collective-permute-done.9.refs_2_ = s32[8]{0:T(128)S(1)} collective-permute-done((s32[8]{0:T(128)S(1)}, s32[8]{0:T(128)S(1)}, u32[]{:S(2)}, u32[]{:S(2)}) %collective-permute-start.9) | collective-permute-done | bytes 64 | tf_op jit(solution)/shard_map/ppermute | solution.py:41
  35.0 0.6 pick.7
  35.7 0.6 collective-permute-start.10
  36.6 2.7 %collective-permute-start.12 = (bf16[2,64,1024]{2,1,0:T(8,128)(2,1)S(1)}, bf16[2,64,1024]{2,1,0:T(8,128)(2,1)S(1)}, u32[]{:S(2)}, u32[]{:S(2)}) collective-permute-start(bf16[2,64,1024]{2,1,0:T(8,128)(2,1)S(1)} %get-tuple-element.51), channel_id=1, source_target_pairs={{0,6},{2,4},{4,2},{6,0},{8,14},{10,12},{12,10},{14,8},{16,22},{18,... | collective-permute-start | bytes 786440 | tf_op jit(solution)/shard_map/ppermute | solution.py:41
  39.2 0.7 collective-permute-start.3
  39.9 0.6 pick.11
  40.5 4.4 %collective-permute-done.10.refs_6_ = bf16[2,64,1024]{2,1,0:T(8,128)(2,1)S(1)} collective-permute-done((bf16[2,64,1024]{2,1,0:T(8,128)(2,1)S(1)}, bf16[2,64,1024]{2,1,0:T(8,128)(2,1)S(1)}, u32[]{:S(2)}, u32[]{:S(2)}) %collective-permute-start.10) | collective-permute-done | bytes 262176 | tf_op jit(solution)/shard_map/ppermute | solution.py:41
  44.9 0.5 collective-permute-start.23
  45.5 4.7 %collective-permute-done.11.refs_7_ = bf16[2,64,1024]{2,1,0:T(8,128)(2,1)S(1)} collective-permute-done((bf16[2,64,1024]{2,1,0:T(8,128)(2,1)S(1)}, bf16[2,64,1024]{2,1,0:T(8,128)(2,1)S(1)}, u32[]{:S(2)}, u32[]{:S(2)}) %collective-permute-start.11) | collective-permute-done | bytes 262176 | tf_op jit(solution)/shard_map/ppermute | solution.py:41
  50.2 0.9 collective-permute-start.6
  51.1 0.6 pick.8
  51.7 2.9 %collective-permute-start.25 = (bf16[2,64,512]{2,1,0:T(8,128)(2,1)S(1)}, bf16[2,64,512]{2,1,0:T(8,128)(2,1)S(1)}, u32[]{:S(2)}, u32[]{:S(2)}) collective-permute-start(bf16[2,64,512]{2,1,0:T(8,128)(2,1)S(1)} %get-tuple-element.63), channel_id=1, source_target_pairs={{0,6},{2,4},{4,2},{6,0},{8,14},{10,12},{12,10},{14,8},{16,22},{18,... | collective-permute-start | bytes 393224 | tf_op jit(solution)/shard_map/ppermute | solution.py:41
  54.6 0.7 collective-permute-start.13
  55.2 2.7 %collective-permute-done.24.refs_10_ = bf16[2,64,512]{2,1,0:T(8,128)(2,1)S(1)} collective-permute-done((bf16[2,64,512]{2,1,0:T(8,128)(2,1)S(1)}, bf16[2,64,512]{2,1,0:T(8,128)(2,1)S(1)}, u32[]{:S(2)}, u32[]{:S(2)}) %collective-permute-start.24) | collective-permute-done | bytes 131104 | tf_op jit(solution)/shard_map/ppermute | solution.py:41
  58.0 0.6 pick.12
  58.8 3.0 %collective-permute-start.15 = (bf16[2,64,512]{2,1,0:T(8,128)(2,1)S(1)}, bf16[2,64,512]{2,1,0:T(8,128)(2,1)S(1)}, u32[]{:S(2)}, u32[]{:S(2)}) collective-permute-start(bf16[2,64,512]{2,1,0:T(8,128)(2,1)S(1)} %get-tuple-element.54), channel_id=1, source_target_pairs={{0,6},{2,4},{4,2},{6,0},{8,14},{10,12},{12,10},{14,8},{16,22},{18,... | collective-permute-start | bytes 393224 | tf_op jit(solution)/shard_map/ppermute | solution.py:41
  61.8 0.3 collective-permute-start.26
  62.1 1.0 %collective-permute-done.14.refs_10_ = bf16[2,64,512]{2,1,0:T(8,128)(2,1)S(1)} collective-permute-done((bf16[2,64,512]{2,1,0:T(8,128)(2,1)S(1)}, bf16[2,64,512]{2,1,0:T(8,128)(2,1)S(1)}, u32[]{:S(2)}, u32[]{:S(2)}) %collective-permute-start.14) | collective-permute-done | bytes 131104 | tf_op jit(solution)/shard_map/ppermute | solution.py:41
  63.1 1.2 %collective-permute-start.27 = (bf16[2,64,512]{2,1,0:T(8,128)(2,1)S(1)}, bf16[2,64,512]{2,1,0:T(8,128)(2,1)S(1)}, u32[]{:S(2)}, u32[]{:S(2)}) collective-permute-start(bf16[2,64,512]{2,1,0:T(8,128)(2,1)S(1)} %get-tuple-element.65), channel_id=1, source_target_pairs={{0,4},{2,6},{4,0},{6,2},{8,12},{10,14},{12,8},{14,10},{16,20},{18,... | collective-permute-start | bytes 393224 | tf_op jit(solution)/shard_map/ppermute | solution.py:41
  64.3 3.6 %collective-permute-start.28 = (bf16[2,64,512]{2,1,0:T(8,128)(2,1)S(1)}, bf16[2,64,512]{2,1,0:T(8,128)(2,1)S(1)}, u32[]{:S(2)}, u32[]{:S(2)}) collective-permute-start(bf16[2,64,512]{2,1,0:T(8,128)(2,1)S(1)} %get-tuple-element.66), channel_id=1, source_target_pairs={{0,6},{2,4},{4,2},{6,0},{8,14},{10,12},{12,10},{14,8},{16,22},{18,... | collective-permute-start | bytes 393224 | tf_op jit(solution)/shard_map/ppermute | solution.py:41
  68.0 4.0 %project.2.refs_1_ = bf16[384,1024]{1,0:T(8,128)(2,1)S(1)} custom-call(bf16[384,1024]{1,0:T(8,128)(2,1)S(1)} %get-tuple-element.43.refs_0_, bf16[384,1024]{1,0:T(8,128)(2,1)S(1)} %collective-permute-done.refs_0_.refs_1_, bf16[2048,1024]{1,0:T(8,128)(2,1)} %refs_2_.2), custom_call_target="tpu_custom_call" | custom-call | flops 1610612736 | bytes 5767168 | tf_op jit(solution)/shard_map/project/pallas_call | solution.py:85
  72.0 0.6 pick.9
  72.6 0.6 pick.13
  73.3 2.0 %collective-permute-start.29 = (bf16[2,64,512]{2,1,0:T(8,128)(2,1)S(1)}, bf16[2,64,512]{2,1,0:T(8,128)(2,1)S(1)}, u32[]{:S(2)}, u32[]{:S(2)}) collective-permute-start(bf16[2,64,512]{2,1,0:T(8,128)(2,1)S(1)} %get-tuple-element.68), channel_id=1, source_target_pairs={{0,2},{2,0},{4,6},{6,4},{8,10},{10,8},{12,14},{14,12},{16,18},{18,... | collective-permute-start | bytes 393224 | tf_op jit(solution)/shard_map/ppermute | solution.py:41
  75.3 3.2 %collective-permute-start.31 = (bf16[2,64,512]{2,1,0:T(8,128)(2,1)S(1)}, bf16[2,64,512]{2,1,0:T(8,128)(2,1)S(1)}, u32[]{:S(2)}, u32[]{:S(2)}) collective-permute-start(bf16[2,64,512]{2,1,0:T(8,128)(2,1)S(1)} %get-tuple-element.70), channel_id=1, source_target_pairs={{0,6},{2,4},{4,2},{6,0},{8,14},{10,12},{12,10},{14,8},{16,22},{18,... | collective-permute-start | bytes 393224 | tf_op jit(solution)/shard_map/ppermute | solution.py:41
  78.6 0.6 pick.10
  79.2 1.8 %collective-permute-start.18 = (bf16[2,64,512]{2,1,0:T(8,128)(2,1)S(1)}, bf16[2,64,512]{2,1,0:T(8,128)(2,1)S(1)}, u32[]{:S(2)}, u32[]{:S(2)}) collective-permute-start(bf16[2,64,512]{2,1,0:T(8,128)(2,1)S(1)} %get-tuple-element.57), channel_id=1, source_target_pairs={{0,6},{2,4},{4,2},{6,0},{8,14},{10,12},{12,10},{14,8},{16,22},{18,... | collective-permute-start | bytes 393224 | tf_op jit(solution)/shard_map/ppermute | solution.py:41
  81.1 1.7 %collective-permute-start.19 = (bf16[2,64,512]{2,1,0:T(8,128)(2,1)S(1)}, bf16[2,64,512]{2,1,0:T(8,128)(2,1)S(1)}, u32[]{:S(2)}, u32[]{:S(2)}) collective-permute-start(bf16[2,64,512]{2,1,0:T(8,128)(2,1)S(1)} %get-tuple-element.58), channel_id=1, source_target_pairs={{0,2},{2,0},{4,6},{6,4},{8,10},{10,8},{12,14},{14,12},{16,18},{18,... | collective-permute-start | bytes 393224 | tf_op jit(solution)/shard_map/ppermute | solution.py:41
  82.7 2.5 %collective-permute-start.21 = (bf16[2,64,512]{2,1,0:T(8,128)(2,1)S(1)}, bf16[2,64,512]{2,1,0:T(8,128)(2,1)S(1)}, u32[]{:S(2)}, u32[]{:S(2)}) collective-permute-start(bf16[2,64,512]{2,1,0:T(8,128)(2,1)S(1)} %get-tuple-element.60), channel_id=1, source_target_pairs={{0,6},{2,4},{4,2},{6,0},{8,14},{10,12},{12,10},{14,8},{16,22},{18,... | collective-permute-start | bytes 393224 | tf_op jit(solution)/shard_map/ppermute | solution.py:41
  85.2 3.3 %attend.3.refs_0_ = bf16[384,512]{1,0:T(8,128)(2,1)S(1)} custom-call(s32[192]{0:T(256)S(1)} %get-tuple-element.41.refs_0_, bf16[384,1024]{1,0:T(8,128)(2,1)S(1)} %project.2.refs_1_, bf16[6,64,512]{2,1,0:T(8,128)(2,1)S(1)} %bitcast.7, bf16[6,64,512]{2,1,0:T(8,128)(2,1)S(1)} %collective-permute-done.1.refs_3_, ...), custom_call_target="tpu_custom_call" | custom-call | flops 805306368 | bytes 3932160 | tf_op jit(solution)/shard_map/attend/pallas_call | solution.py:395
  88.6 0.5 collective-permute-done.20.refs_16_
  89.1 3.3 %attend.2.refs_2_ = bf16[384,512]{1,0:T(8,128)(2,1)S(1)} custom-call(s32[192]{0:T(256)S(1)} %get-tuple-element.41.refs_0_, bf16[384,1024]{1,0:T(8,128)(2,1)S(1)} %project.2.refs_1_, bf16[6,64,512]{2,1,0:T(8,128)(2,1)S(1)} %bitcast.4, bf16[6,64,512]{2,1,0:T(8,128)(2,1)S(1)} %collective-permute-done.4.refs_3_, ...), custom_call_target="tpu_custom_call" | custom-call | flops 805306368 | bytes 3932160 | tf_op jit(solution)/shard_map/attend/pallas_call | solution.py:395
  92.5 1.4 %mix.2.refs_2_ = f32[384,1024]{1,0:T(8,128)S(1)} custom-call(bf16[384,512]{1,0:T(8,128)(2,1)S(1)} %attend.3.refs_0_, bf16[384,512]{1,0:T(8,128)(2,1)S(1)} %collective-permute-done.32.refs_1_, bf16[384,512]{1,0:T(8,128)(2,1)S(1)} %attend.2.refs_2_, bf16[2048,1024]{1,0:T(8,128)(2,1)S(1)} %copy-done), custom_call_target="tpu_custom_call" | custom-call | flops 1207959552 | bytes 5898240 | tf_op jit(solution)/shard_map/mix/pallas_call | solution.py:210
  94.2 1.4 %mix.3 = bf16[384,1024]{1,0:T(8,128)(2,1)} custom-call(bf16[384,512]{1,0:T(8,128)(2,1)S(1)} %collective-permute-done.22.refs_0_, bf16[2048,1024]{1,0:T(8,128)(2,1)S(1)} %copy-done, f32[384,1024]{1,0:T(8,128)S(1)} %mix.2.refs_2_), custom_call_target="tpu_custom_call" | custom-call | flops 402653184 | bytes 3014656 | tf_op jit(solution)/shard_map/mix/pallas_call | solution.py:210
  (38 shorter events, 1.6 us)
Async XLA Ops:
  0.0 3.0 %collective-permute-start = (bf16[384,1024]{1,0:T(8,128)(2,1)}, bf16[384,1024]{1,0:T(8,128)(2,1)S(1)}, u32[]{:S(2)}, u32[]{:S(2)}) collective-permute-start(bf16[384,1024]{1,0:T(8,128)(2,1)} %own_in.1), channel_id=1, source_target_pairs={{0,1},{1,0},{2,3},{3,2},{4,5},{5,4},{6,7},{7,6},{8,9},{9,8},{10,11... | collective-permute-start | bytes 2359304 | tf_op jit(solution)/shard_map/ppermute | solution.py:49
  2.9 3.2 %copy-start.1 = (s32[6,16]{1,0:T(8,128)S(1)}, s32[6,16]{1,0:T(8,128)}, u32[]{:S(2)}) copy-start(s32[6,16]{1,0:T(8,128)} %chosen_ref) | copy-start | bytes 1156
  3.5 14.6 %collective-permute-start.1 = (bf16[6,64,512]{2,1,0:T(8,128)(2,1)S(1)}, bf16[6,64,512]{2,1,0:T(8,128)(2,1)S(1)}, u32[]{:S(2)}, u32[]{:S(2)}) collective-permute-start(bf16[6,64,512]{2,1,0:T(8,128)(2,1)S(1)} %bitcast.5), channel_id=1, source_target_pairs={{0,8},{2,10},{4,12},{6,14},{8,16},{10,18},{12,20},{14,22},{16,24},... | collective-permute-start | bytes 1179656 | tf_op jit(solution)/shard_map/ppermute | solution.py:41
  12.2 14.4 %collective-permute-start.4 = (bf16[6,64,512]{2,1,0:T(8,128)(2,1)S(1)}, bf16[6,64,512]{2,1,0:T(8,128)(2,1)S(1)}, u32[]{:S(2)}, u32[]{:S(2)}) collective-permute-start(bf16[6,64,512]{2,1,0:T(8,128)(2,1)S(1)} %bitcast.2), channel_id=1, source_target_pairs={{0,8},{2,10},{4,12},{6,14},{8,16},{10,18},{12,20},{14,22},{16,24},... | collective-permute-start | bytes 1179656 | tf_op jit(solution)/shard_map/ppermute | solution.py:41
  18.2 21.1 %collective-permute-start.2 = (bf16[6,64,512]{2,1,0:T(8,128)(2,1)S(1)}, bf16[6,64,512]{2,1,0:T(8,128)(2,1)S(1)}, u32[]{:S(2)}, u32[]{:S(2)}) collective-permute-start(bf16[6,64,512]{2,1,0:T(8,128)(2,1)S(1)} %collective-permute-done.1.refs_3_), channel_id=1, source_target_pairs={{0,0},{2,2},{4,4},{6,6},{8,16},{10,18},{12,20},{14,22},{16,24},{18... | collective-permute-start | bytes 1179656 | tf_op jit(solution)/shard_map/ppermute | solution.py:41
  26.6 23.6 %collective-permute-start.5 = (bf16[6,64,512]{2,1,0:T(8,128)(2,1)S(1)}, bf16[6,64,512]{2,1,0:T(8,128)(2,1)S(1)}, u32[]{:S(2)}, u32[]{:S(2)}) collective-permute-start(bf16[6,64,512]{2,1,0:T(8,128)(2,1)S(1)} %collective-permute-done.4.refs_3_), channel_id=1, source_target_pairs={{0,0},{2,2},{4,4},{6,6},{8,16},{10,18},{12,20},{14,22},{16,24},{18... | collective-permute-start | bytes 1179656 | tf_op jit(solution)/shard_map/ppermute | solution.py:41
  27.3 3.6 %collective-permute-start.7 = (s32[8]{0:T(128)S(1)}, s32[8]{0:T(128)S(1)}, u32[]{:S(2)}, u32[]{:S(2)}) collective-permute-start(s32[8]{0:T(128)S(1)} %get-tuple-element.46), channel_id=1, source_target_pairs={{0,2},{2,0},{4,6},{6,4},{8,10},{10,8},{12,14},{14,12},{16,18},{18,... | collective-permute-start | bytes 104 | tf_op jit(solution)/shard_map/ppermute | solution.py:41
  29.1 3.6 %collective-permute-start.8 = (s32[8]{0:T(128)S(1)}, s32[8]{0:T(128)S(1)}, u32[]{:S(2)}, u32[]{:S(2)}) collective-permute-start(s32[8]{0:T(128)S(1)} %get-tuple-element.47), channel_id=1, source_target_pairs={{0,4},{2,6},{4,0},{6,2},{8,12},{10,14},{12,8},{14,10},{16,20},{18,... | collective-permute-start | bytes 104 | tf_op jit(solution)/shard_map/ppermute | solution.py:41
  30.6 4.5 %collective-permute-start.9 = (s32[8]{0:T(128)S(1)}, s32[8]{0:T(128)S(1)}, u32[]{:S(2)}, u32[]{:S(2)}) collective-permute-start(s32[8]{0:T(128)S(1)} %get-tuple-element.48), channel_id=1, source_target_pairs={{0,6},{2,4},{4,2},{6,0},{8,14},{10,12},{12,10},{14,8},{16,22},{18,... | collective-permute-start | bytes 104 | tf_op jit(solution)/shard_map/ppermute | solution.py:41
  35.7 9.2 %collective-permute-start.10 = (bf16[2,64,1024]{2,1,0:T(8,128)(2,1)S(1)}, bf16[2,64,1024]{2,1,0:T(8,128)(2,1)S(1)}, u32[]{:S(2)}, u32[]{:S(2)}) collective-permute-start(bf16[2,64,1024]{2,1,0:T(8,128)(2,1)S(1)} %get-tuple-element.49), channel_id=1, source_target_pairs={{0,2},{2,0},{4,6},{6,4},{8,10},{10,8},{12,14},{14,12},{16,18},{18,... | collective-permute-start | bytes 786440 | tf_op jit(solution)/shard_map/ppermute | solution.py:41
  36.3 13.9 %collective-permute-start.11 = (bf16[2,64,1024]{2,1,0:T(8,128)(2,1)S(1)}, bf16[2,64,1024]{2,1,0:T(8,128)(2,1)S(1)}, u32[]{:S(2)}, u32[]{:S(2)}) collective-permute-start(bf16[2,64,1024]{2,1,0:T(8,128)(2,1)S(1)} %get-tuple-element.50), channel_id=1, source_target_pairs={{0,4},{2,6},{4,0},{6,2},{8,12},{10,14},{12,8},{14,10},{16,20},{18,... | collective-permute-start | bytes 786440 | tf_op jit(solution)/shard_map/ppermute | solution.py:41
  36.6 15.1 %collective-permute-start.12 = (bf16[2,64,1024]{2,1,0:T(8,128)(2,1)S(1)}, bf16[2,64,1024]{2,1,0:T(8,128)(2,1)S(1)}, u32[]{:S(2)}, u32[]{:S(2)}) collective-permute-start(bf16[2,64,1024]{2,1,0:T(8,128)(2,1)S(1)} %get-tuple-element.51), channel_id=1, source_target_pairs={{0,6},{2,4},{4,2},{6,0},{8,14},{10,12},{12,10},{14,8},{16,22},{18,... | collective-permute-start | bytes 786440 | tf_op jit(solution)/shard_map/ppermute | solution.py:41
  39.2 25.1 %collective-permute-start.3 = (bf16[6,64,512]{2,1,0:T(8,128)(2,1)S(1)}, bf16[6,64,512]{2,1,0:T(8,128)(2,1)S(1)}, u32[]{:S(2)}, u32[]{:S(2)}) collective-permute-start(bf16[6,64,512]{2,1,0:T(8,128)(2,1)S(1)} %collective-permute-done.2.refs_3_.refs_4_), channel_id=1, source_target_pairs={{0,0},{2,2},{4,4},{6,6},{8,8},{10,10},{12,12},{14,14},{16,24},{18,... | collective-permute-start | bytes 1179656 | tf_op jit(solution)/shard_map/ppermute | solution.py:41
  44.9 9.7 %collective-permute-start.23 = (bf16[2,64,512]{2,1,0:T(8,128)(2,1)S(1)}, bf16[2,64,512]{2,1,0:T(8,128)(2,1)S(1)}, u32[]{:S(2)}, u32[]{:S(2)}) collective-permute-start(bf16[2,64,512]{2,1,0:T(8,128)(2,1)S(1)} %get-tuple-element.61), channel_id=1, source_target_pairs={{0,2},{2,0},{4,6},{6,4},{8,10},{10,8},{12,14},{14,12},{16,18},{18,... | collective-permute-start | bytes 393224 | tf_op jit(solution)/shard_map/ppermute | solution.py:41
  50.2 7.8 %collective-permute-start.24 = (bf16[2,64,512]{2,1,0:T(8,128)(2,1)S(1)}, bf16[2,64,512]{2,1,0:T(8,128)(2,1)S(1)}, u32[]{:S(2)}, u32[]{:S(2)}) collective-permute-start(bf16[2,64,512]{2,1,0:T(8,128)(2,1)S(1)} %get-tuple-element.62), channel_id=1, source_target_pairs={{0,4},{2,6},{4,0},{6,2},{8,12},{10,14},{12,8},{14,10},{16,20},{18,... | collective-permute-start | bytes 393224 | tf_op jit(solution)/shard_map/ppermute | solution.py:41
  50.2 28.3 %collective-permute-start.6 = (bf16[6,64,512]{2,1,0:T(8,128)(2,1)S(1)}, bf16[6,64,512]{2,1,0:T(8,128)(2,1)S(1)}, u32[]{:S(2)}, u32[]{:S(2)}) collective-permute-start(bf16[6,64,512]{2,1,0:T(8,128)(2,1)S(1)} %collective-permute-done.5.refs_3_.refs_4_), channel_id=1, source_target_pairs={{0,0},{2,2},{4,4},{6,6},{8,8},{10,10},{12,12},{14,14},{16,24},{18,... | collective-permute-start | bytes 1179656 | tf_op jit(solution)/shard_map/ppermute | solution.py:41
  51.7 7.1 %collective-permute-start.25 = (bf16[2,64,512]{2,1,0:T(8,128)(2,1)S(1)}, bf16[2,64,512]{2,1,0:T(8,128)(2,1)S(1)}, u32[]{:S(2)}, u32[]{:S(2)}) collective-permute-start(bf16[2,64,512]{2,1,0:T(8,128)(2,1)S(1)} %get-tuple-element.63), channel_id=1, source_target_pairs={{0,6},{2,4},{4,2},{6,0},{8,14},{10,12},{12,10},{14,8},{16,22},{18,... | collective-permute-start | bytes 393224 | tf_op jit(solution)/shard_map/ppermute | solution.py:41
  54.6 7.2 %collective-permute-start.13 = (bf16[2,64,512]{2,1,0:T(8,128)(2,1)S(1)}, bf16[2,64,512]{2,1,0:T(8,128)(2,1)S(1)}, u32[]{:S(2)}, u32[]{:S(2)}) collective-permute-start(bf16[2,64,512]{2,1,0:T(8,128)(2,1)S(1)} %get-tuple-element.52), channel_id=1, source_target_pairs={{0,2},{2,0},{4,6},{6,4},{8,10},{10,8},{12,14},{14,12},{16,18},{18,... | collective-permute-start | bytes 393224 | tf_op jit(solution)/shard_map/ppermute | solution.py:41
  57.9 5.2 %collective-permute-start.14 = (bf16[2,64,512]{2,1,0:T(8,128)(2,1)S(1)}, bf16[2,64,512]{2,1,0:T(8,128)(2,1)S(1)}, u32[]{:S(2)}, u32[]{:S(2)}) collective-permute-start(bf16[2,64,512]{2,1,0:T(8,128)(2,1)S(1)} %get-tuple-element.53), channel_id=1, source_target_pairs={{0,4},{2,6},{4,0},{6,2},{8,12},{10,14},{12,8},{14,10},{16,20},{18,... | collective-permute-start | bytes 393224 | tf_op jit(solution)/shard_map/ppermute | solution.py:41
  58.8 14.4 %collective-permute-start.15 = (bf16[2,64,512]{2,1,0:T(8,128)(2,1)S(1)}, bf16[2,64,512]{2,1,0:T(8,128)(2,1)S(1)}, u32[]{:S(2)}, u32[]{:S(2)}) collective-permute-start(bf16[2,64,512]{2,1,0:T(8,128)(2,1)S(1)} %get-tuple-element.54), channel_id=1, source_target_pairs={{0,6},{2,4},{4,2},{6,0},{8,14},{10,12},{12,10},{14,8},{16,22},{18,... | collective-permute-start | bytes 393224 | tf_op jit(solution)/shard_map/ppermute | solution.py:41
  61.8 11.5 %collective-permute-start.26 = (bf16[2,64,512]{2,1,0:T(8,128)(2,1)S(1)}, bf16[2,64,512]{2,1,0:T(8,128)(2,1)S(1)}, u32[]{:S(2)}, u32[]{:S(2)}) collective-permute-start(bf16[2,64,512]{2,1,0:T(8,128)(2,1)S(1)} %get-tuple-element.64), channel_id=1, source_target_pairs={{0,2},{2,0},{4,6},{6,4},{8,10},{10,8},{12,14},{14,12},{16,18},{18,... | collective-permute-start | bytes 393224 | tf_op jit(solution)/shard_map/ppermute | solution.py:41
  63.1 12.2 %collective-permute-start.27 = (bf16[2,64,512]{2,1,0:T(8,128)(2,1)S(1)}, bf16[2,64,512]{2,1,0:T(8,128)(2,1)S(1)}, u32[]{:S(2)}, u32[]{:S(2)}) collective-permute-start(bf16[2,64,512]{2,1,0:T(8,128)(2,1)S(1)} %get-tuple-element.65), channel_id=1, source_target_pairs={{0,4},{2,6},{4,0},{6,2},{8,12},{10,14},{12,8},{14,10},{16,20},{18,... | collective-permute-start | bytes 393224 | tf_op jit(solution)/shard_map/ppermute | solution.py:41
  64.3 11.0 %collective-permute-start.28 = (bf16[2,64,512]{2,1,0:T(8,128)(2,1)S(1)}, bf16[2,64,512]{2,1,0:T(8,128)(2,1)S(1)}, u32[]{:S(2)}, u32[]{:S(2)}) collective-permute-start(bf16[2,64,512]{2,1,0:T(8,128)(2,1)S(1)} %get-tuple-element.66), channel_id=1, source_target_pairs={{0,6},{2,4},{4,2},{6,0},{8,14},{10,12},{12,10},{14,8},{16,22},{18,... | collective-permute-start | bytes 393224 | tf_op jit(solution)/shard_map/ppermute | solution.py:41
  73.2 5.9 %collective-permute-start.16 = (bf16[2,64,512]{2,1,0:T(8,128)(2,1)S(1)}, bf16[2,64,512]{2,1,0:T(8,128)(2,1)S(1)}, u32[]{:S(2)}, u32[]{:S(2)}) collective-permute-start(bf16[2,64,512]{2,1,0:T(8,128)(2,1)S(1)} %get-tuple-element.55), channel_id=1, source_target_pairs={{0,2},{2,0},{4,6},{6,4},{8,10},{10,8},{12,14},{14,12},{16,18},{18,... | collective-permute-start | bytes 393224 | tf_op jit(solution)/shard_map/ppermute | solution.py:41
  73.3 7.8 %collective-permute-start.29 = (bf16[2,64,512]{2,1,0:T(8,128)(2,1)S(1)}, bf16[2,64,512]{2,1,0:T(8,128)(2,1)S(1)}, u32[]{:S(2)}, u32[]{:S(2)}) collective-permute-start(bf16[2,64,512]{2,1,0:T(8,128)(2,1)S(1)} %get-tuple-element.68), channel_id=1, source_target_pairs={{0,2},{2,0},{4,6},{6,4},{8,10},{10,8},{12,14},{14,12},{16,18},{18,... | collective-permute-start | bytes 393224 | tf_op jit(solution)/shard_map/ppermute | solution.py:41
  75.3 7.4 %collective-permute-start.30 = (bf16[2,64,512]{2,1,0:T(8,128)(2,1)S(1)}, bf16[2,64,512]{2,1,0:T(8,128)(2,1)S(1)}, u32[]{:S(2)}, u32[]{:S(2)}) collective-permute-start(bf16[2,64,512]{2,1,0:T(8,128)(2,1)S(1)} %get-tuple-element.69), channel_id=1, source_target_pairs={{0,4},{2,6},{4,0},{6,2},{8,12},{10,14},{12,8},{14,10},{16,20},{18,... | collective-permute-start | bytes 393224 | tf_op jit(solution)/shard_map/ppermute | solution.py:41
  75.3 7.4 %collective-permute-start.31 = (bf16[2,64,512]{2,1,0:T(8,128)(2,1)S(1)}, bf16[2,64,512]{2,1,0:T(8,128)(2,1)S(1)}, u32[]{:S(2)}, u32[]{:S(2)}) collective-permute-start(bf16[2,64,512]{2,1,0:T(8,128)(2,1)S(1)} %get-tuple-element.70), channel_id=1, source_target_pairs={{0,6},{2,4},{4,2},{6,0},{8,14},{10,12},{12,10},{14,8},{16,22},{18,... | collective-permute-start | bytes 393224 | tf_op jit(solution)/shard_map/ppermute | solution.py:41
  78.5 10.0 %collective-permute-start.17 = (bf16[2,64,512]{2,1,0:T(8,128)(2,1)S(1)}, bf16[2,64,512]{2,1,0:T(8,128)(2,1)S(1)}, u32[]{:S(2)}, u32[]{:S(2)}) collective-permute-start(bf16[2,64,512]{2,1,0:T(8,128)(2,1)S(1)} %get-tuple-element.56), channel_id=1, source_target_pairs={{0,4},{2,6},{4,0},{6,2},{8,12},{10,14},{12,8},{14,10},{16,20},{18,... | collective-permute-start | bytes 393224 | tf_op jit(solution)/shard_map/ppermute | solution.py:41
  79.2 9.5 %collective-permute-start.18 = (bf16[2,64,512]{2,1,0:T(8,128)(2,1)S(1)}, bf16[2,64,512]{2,1,0:T(8,128)(2,1)S(1)}, u32[]{:S(2)}, u32[]{:S(2)}) collective-permute-start(bf16[2,64,512]{2,1,0:T(8,128)(2,1)S(1)} %get-tuple-element.57), channel_id=1, source_target_pairs={{0,6},{2,4},{4,2},{6,0},{8,14},{10,12},{12,10},{14,8},{16,22},{18,... | collective-permute-start | bytes 393224 | tf_op jit(solution)/shard_map/ppermute | solution.py:41
  81.1 7.6 %collective-permute-start.19 = (bf16[2,64,512]{2,1,0:T(8,128)(2,1)S(1)}, bf16[2,64,512]{2,1,0:T(8,128)(2,1)S(1)}, u32[]{:S(2)}, u32[]{:S(2)}) collective-permute-start(bf16[2,64,512]{2,1,0:T(8,128)(2,1)S(1)} %get-tuple-element.58), channel_id=1, source_target_pairs={{0,2},{2,0},{4,6},{6,4},{8,10},{10,8},{12,14},{14,12},{16,18},{18,... | collective-permute-start | bytes 393224 | tf_op jit(solution)/shard_map/ppermute | solution.py:41
  82.7 6.4 %collective-permute-start.20 = (bf16[2,64,512]{2,1,0:T(8,128)(2,1)S(1)}, bf16[2,64,512]{2,1,0:T(8,128)(2,1)S(1)}, u32[]{:S(2)}, u32[]{:S(2)}) collective-permute-start(bf16[2,64,512]{2,1,0:T(8,128)(2,1)S(1)} %get-tuple-element.59), channel_id=1, source_target_pairs={{0,4},{2,6},{4,0},{6,2},{8,12},{10,14},{12,8},{14,10},{16,20},{18,... | collective-permute-start | bytes 393224 | tf_op jit(solution)/shard_map/ppermute | solution.py:41
  82.7 6.4 %collective-permute-start.21 = (bf16[2,64,512]{2,1,0:T(8,128)(2,1)S(1)}, bf16[2,64,512]{2,1,0:T(8,128)(2,1)S(1)}, u32[]{:S(2)}, u32[]{:S(2)}) collective-permute-start(bf16[2,64,512]{2,1,0:T(8,128)(2,1)S(1)} %get-tuple-element.60), channel_id=1, source_target_pairs={{0,6},{2,4},{4,2},{6,0},{8,14},{10,12},{12,10},{14,8},{16,22},{18,... | collective-permute-start | bytes 393224 | tf_op jit(solution)/shard_map/ppermute | solution.py:41
  88.5 4.0 %copy-start = (bf16[2048,1024]{1,0:T(8,128)(2,1)S(1)}, bf16[2048,1024]{1,0:T(8,128)(2,1)}, u32[]{:S(2)}) copy-start(bf16[2048,1024]{1,0:T(8,128)(2,1)} %refs_1_.1) | copy-start | bytes 12582916
  88.5 4.0 %collective-permute-start.32 = (bf16[384,512]{1,0:T(8,128)(2,1)S(1)}, bf16[384,512]{1,0:T(8,128)(2,1)S(1)}, u32[]{:S(2)}, u32[]{:S(2)}) collective-permute-start(bf16[384,512]{1,0:T(8,128)(2,1)S(1)} %attend.3.refs_0_), channel_id=1, source_target_pairs={{0,1},{1,0},{2,3},{3,2},{4,5},{5,4},{6,7},{7,6},{8,9},{9,8},{10,11... | collective-permute-start | bytes 1179656 | tf_op jit(solution)/shard_map/ppermute | solution.py:49
  92.4 1.8 %collective-permute-start.22 = (bf16[384,512]{1,0:T(8,128)(2,1)S(1)}, bf16[384,512]{1,0:T(8,128)(2,1)S(1)}, u32[]{:S(2)}, u32[]{:S(2)}) collective-permute-start(bf16[384,512]{1,0:T(8,128)(2,1)S(1)} %attend.2.refs_2_), channel_id=1, source_target_pairs={{0,1},{1,0},{2,3},{3,2},{4,5},{5,4},{6,7},{7,6},{8,9},{9,8},{10,11... | collective-permute-start | bytes 1179656 | tf_op jit(solution)/shard_map/ppermute | solution.py:49
